TPU v7x, 32 devices: a whole 2x2x4 slice. The times are simulated.
32 devices in a mesh: sp: 16 (over z, y, x), tp: 2 (over core).
Axes of the slice: x: 2, y: 2, z: 4, core: 2. Of those that a mesh axis runs over, the one named last changes fastest.
Arguments:
- query_rows: bfloat16 [4096, 1024], P('sp', 'tp'), may hold values from -26 to 26
- key_rows: bfloat16 [4096, 128], P('sp', 'tp'), may hold values from -26 to 26
- value_head_rows: bfloat16 [4096, 128], P('sp', 'tp'), may hold values from -6 to 6
- sink_logit_head: float32 [16], P('tp'), may hold values from -6 to 6
- out_weight: bfloat16 [1024, 2048], P('tp'), may hold values from -0.1875 to 0.1875
- residual: bfloat16 [4096, 2048], P(('sp', 'tp')), may hold values from -6 to 6
- norm_gain: float32 [2048], replicated, may hold values from 0.1 to 1.9
- routes: int32 [4096, 2], P(('sp', 'tp')), may hold values from 0 to 15, all different within a row; in each aligned block of 128 rows (0 to 127, 128 to 255, ...) at most 24 rows name the same one
- route_weights: float32 [4096, 2], P(('sp', 'tp')), may hold values from 0.1 to 1
- gate_proj: bfloat16 [16, 2048, 3584], P('sp', None, 'tp'), may hold values from -0.125 to 0.125
- up_proj: bfloat16 [16, 2048, 3584], P('sp', None, 'tp'), may hold values from -0.125 to 0.125
- down_proj: bfloat16 [16, 3584, 2048], P('sp', 'tp'), may hold values from -0.09375 to 0.09375
Outputs:
- output: bfloat16 [4096, 2048], P(('sp', 'tp'))
Inputs may be any that keep to these rules, and one draw needn't show every extreme that they name: `routes`: A row names 2 different experts. Among the rows of one device no expert is named more than 24 times, a bound that some block reaches on some devices.
All inputs are finite; a program needn't handle non-finite values.
Results may differ from a plain program's by a relative error of at most 0.0055.
Values may be sent and summed in bfloat16 or wider, within the bound.
No kernel may reach another device: no remote copies, remote signals or barrier semaphores. Data moves between devices by JAX's collectives and lax.ppermute only.
A program may use at most 128 MiB of HBM per device.

v0:
```python
import jax
import jax.numpy as jnp
from jax import lax
from jax.sharding import PartitionSpec as P

QUERY_HEADS = 16
KEY_VALUE_HEADS = 2
HEAD_SIZE = 64
TOP = 2
WINDOW_KEYS = 128


def from_behind(block, axis, distance):
    devices = range(lax.axis_size(axis))
    route = [(i - distance, i) for i in devices if i - distance in devices]
    return lax.ppermute(block, axis, route)


def on_device(
    query_rows,
    key_rows,
    value_head_rows,
    sink_logit_head,
    out_weight,
    residual,
    norm_gain,
    routes,
    route_weights,
    gate_proj,
    up_proj,
    down_proj,
):
    length = query_rows.shape[0]
    query_group = QUERY_HEADS // KEY_VALUE_HEADS
    width = key_rows.shape[1]
    local_kv = width // HEAD_SIZE
    local_heads = local_kv * query_group
    sp_index = lax.axis_index("sp")
    tp_index = lax.axis_index("tp")
    tail = jnp.concatenate(
        [key_rows[length - WINDOW_KEYS :], value_head_rows[length - WINDOW_KEYS :]], axis=1
    )
    before = from_behind(tail, "sp", 1)
    key_all = jnp.concatenate([before[:, :width], key_rows], axis=0)
    value_all = jnp.concatenate([before[:, width:], value_head_rows], axis=0)
    score_matrix = jnp.einsum(
        "rjwh,cjh->jwrc",
        query_rows.reshape(length, local_kv, query_group, HEAD_SIZE),
        key_all.reshape(-1, local_kv, HEAD_SIZE),
        preferred_element_type=jnp.float32,
    ) * HEAD_SIZE ** (-0.5)
    query_pos = sp_index * length + jnp.arange(length, dtype=jnp.int32)
    key_pos = sp_index * length - WINDOW_KEYS + jnp.arange(length + WINDOW_KEYS, dtype=jnp.int32)
    distance = query_pos[:, None] - key_pos[None, :]
    inside = (distance >= 0) & (distance < WINDOW_KEYS) & (key_pos[None, :] >= 0)
    head_ids = (tp_index * local_heads + jnp.arange(local_heads, dtype=jnp.int32)).astype(
        jnp.float32
    )
    slope_values = jnp.exp2(-8.0 * (head_ids + 1.0) / QUERY_HEADS).reshape(local_kv, query_group)
    score_matrix = (
        score_matrix - slope_values[:, :, None, None] * distance.astype(jnp.float32)[None, None]
    )
    score_matrix = jnp.where(inside[None, None], score_matrix, -jnp.inf)
    sink_portion = sink_logit_head.reshape(local_kv, query_group)[:, :, None]
    peak = jnp.maximum(jnp.max(score_matrix, axis=-1), sink_portion)
    expd = jnp.exp(score_matrix - peak[..., None])
    denom = jnp.sum(expd, axis=-1) + jnp.exp(sink_portion - peak)
    probabilities = (expd / denom[..., None]).astype(jnp.bfloat16)
    attended = (
        jnp.einsum(
            "wfbt,twj->bwfj",
            probabilities,
            value_all.reshape(-1, local_kv, HEAD_SIZE),
            preferred_element_type=jnp.float32,
        )
        .reshape(length, local_heads * HEAD_SIZE)
        .astype(jnp.bfloat16)
    )
    own_rows = length // lax.axis_size("tp")
    projected = lax.psum_scatter(
        jnp.dot(attended, out_weight, preferred_element_type=jnp.float32),
        "tp",
        scatter_dimension=0,
        tiled=True,
    )
    mixed = residual.astype(jnp.float32) + projected
    scale = lax.rsqrt(jnp.mean(mixed * mixed, axis=-1, keepdims=True) + 1e-05)
    normed = (mixed * scale * norm_gain).astype(jnp.bfloat16)
    n_sp = lax.axis_size("sp")
    n_tp = lax.axis_size("tp")
    capacity = 3 * own_rows * TOP // (2 * n_sp)
    chosen = routes.reshape(-1)
    onehot = (chosen[:, None] == jnp.arange(n_sp, dtype=jnp.int32)[None, :]).astype(jnp.int32)
    running = jnp.cumsum(onehot, axis=0)
    rank_in = jnp.sum(onehot * running, axis=1) - 1
    slot_index = chosen * capacity + rank_in
    slot_ids = jnp.arange(n_sp * capacity, dtype=jnp.int32)
    select = jnp.any(
        slot_index.reshape(own_rows, TOP)[None, :, :] == slot_ids[:, None, None], axis=-1
    )
    dispatch = jnp.dot(
        select.astype(jnp.bfloat16), normed, preferred_element_type=jnp.float32
    ).astype(jnp.bfloat16)
    model_width = dispatch.shape[1]
    landed = lax.all_to_all(
        dispatch.reshape(n_sp, capacity, model_width), "sp", split_axis=0, concat_axis=0, tiled=True
    )
    arrived = lax.all_gather(
        landed.reshape(n_sp, 1, capacity, model_width), "tp", axis=1, tiled=True
    )
    rows_in = arrived.reshape(-1, model_width)
    gate = jnp.dot(rows_in, gate_proj[0], preferred_element_type=jnp.float32)
    upper = jnp.dot(rows_in, up_proj[0], preferred_element_type=jnp.float32)
    hidden = (jax.nn.silu(gate) * upper).astype(jnp.bfloat16)
    partial_out = jnp.dot(hidden, down_proj[0], preferred_element_type=jnp.float32)
    partial_out = partial_out.reshape(n_sp, n_tp, capacity, model_width)
    summed = lax.psum_scatter(
        partial_out.astype(jnp.bfloat16), "tp", scatter_dimension=1, tiled=True
    )
    expert_out = summed.reshape(n_sp, capacity, model_width)
    returned = lax.all_to_all(expert_out, "sp", split_axis=0, concat_axis=0, tiled=True)
    picked = returned.reshape(n_sp * capacity, model_width)[slot_index].reshape(
        own_rows, TOP, model_width
    )
    moe_sum = jnp.sum(route_weights[:, :, None] * picked.astype(jnp.float32), axis=1)
    return (mixed + moe_sum).astype(jnp.bfloat16)


def solution(mesh):
    placed = (
        P("sp", "tp"),
        P("sp", "tp"),
        P("sp", "tp"),
        P("tp"),
        P("tp", None),
        P(("sp", "tp"), None),
        P(),
        P(("sp", "tp"), None),
        P(("sp", "tp"), None),
        P("sp", None, "tp"),
        P("sp", None, "tp"),
        P("sp", "tp", None),
    )
    return jax.shard_map(
        on_device, mesh=mesh, in_specs=placed, out_specs=P(("sp", "tp"), None), check_vma=False
    )
```

profile of v0, /device:TPU:12, one launch (start us, length us, event | category | flops | bytes accessed | tf_op | source)
XLA Modules:
  0.0 209.4 jit_solution(3881032120100905958)
XLA Ops:
  6.5 0.0 copy-start
  6.5 0.0 reduce-scatter.3.cloned.1.call-start
  6.5 0.9 slice.18
  7.4 0.7 slice.19
  8.1 3.4 %collective-permute-start = (bf16[128,128]{0,1:T(8,128)(2,1)S(1)}, bf16[128,128]{0,1:T(8,128)(2,1)S(1)}, u32[]{:S(2)}, u32[]{:S(2)}) collective-permute-start(bf16[128,128]{0,1:T(8,128)(2,1)S(1)} %pad_maximum_fusion), channel_id=1, source_target_pairs={{0,2},{2,4},{4,6},{6,8},{8,10},{10,12},{12,14},{14,16},{16,18},{18... | collective-permute-start | bytes 98312 | tf_op jit(solution)/shard_map/ppermute | solution.py:16
  11.6 0.1 subtract_convert_fusion
  11.7 0.2 fusion.22
  11.9 1.1 copy.31
  13.0 1.8 collective-permute-done
  14.8 1.6 fusion.34
  16.4 0.0 copy-done.6
  16.4 0.1 broadcast_maximum_fusion
  16.5 0.4 fusion.12
  16.9 0.1 exponential_add_fusion
  17.0 0.0 copy-done.5
  17.0 0.7 fusion.15
  17.7 0.0 copy-done
  17.7 0.0 copy-start.7
  17.7 0.0 copy-start.2
  17.8 2.1 fusion.35
  19.8 0.0 reduce-scatter.3.cloned.1.call-update
  19.9 0.0 all-gather.3.cloned.1.call-start
  19.9 0.0 copy-done.7
  19.9 0.1 copy.34
  20.0 0.1 eq.42
  20.2 0.1 eq.38
  20.3 0.6 reduce-window.6
  20.9 0.2 slice_reduce_fusion
  21.1 0.1 fusion.28
  21.2 0.1 sub.63
  21.4 0.1 copy.38
  21.5 0.1 fusion.20
  21.5 8.8 %reduce-scatter.3.cloned.1.call-done = f32[128,2048]{1,0:T(8,128)} async-done(((f32[256,2048]{1,0:T(8,128)}), f32[128,2048]{1,0:T(8,128)}) %reduce-scatter.3.cloned.1.call-update) | async-done | bytes 1048592 | tf_op jit(solution)/shard_map/reduce_scatter | solution.py:80
  30.4 0.0 copy-done.2
  30.4 1.4 multiply_reduce_fusion.1
  31.8 0.0 copy-done.4
  31.8 1.9 convolution_convert_fusion
  33.7 43.6 %all_to_all.10 = bf16[16,24,2048]{2,1,0:T(8,128)(2,1)} all-to-all(bf16[16,24,2048]{2,1,0:T(8,128)(2,1)S(1)} %bitcast.75), channel_id=1, replica_groups=mesh['sp'=16,'tp'=2] {'sp'}, dimensions={0} | all-to-all | bytes 3145728 | tf_op jit(solution)/shard_map/all_to_all | solution.py:105
  77.3 0.0 all-gather.3.cloned.1.call-update
  77.3 0.2 all-reduce.3.cloned.1.call-start
  77.5 11.4 %all-gather.3.cloned.1.call-done = bf16[16,48,2048]{2,1,0:T(8,128)(2,1)} async-done(((bf16[16,24,2048]{2,1,0:T(8,128)(2,1)}), bf16[16,48,2048]{2,1,0:T(8,128)(2,1)}) %all-gather.3.cloned.1.call-update) | async-done | bytes 3145744 | tf_op jit(solution)/shard_map/all_gather | solution.py:108
  88.9 10.0 %fusion.4 = f32[768,1792]{1,0:T(8,128)S(1)} fusion(bf16[768,2048]{1,0:T(8,128)(2,1)} %bitcast.82, bf16[1,2048,1792]{2,1,0:T(8,128)(2,1)} %param.21), kind=kOutput, calls=%fused_computation.5 | convolution fusion | flops 5637144576 | bytes 15990784 | tf_op jit(solution)/shard_map/dot_general | solution.py:112
  98.9 0.0 copy-done.9
  98.9 0.0 slice-start.1
  98.9 9.7 %multiply_convert_fusion = bf16[768,1792]{1,0:T(8,128)(2,1)S(1)} fusion(f32[768,1792]{1,0:T(8,128)S(1)} %fusion.4, bf16[768,2048]{1,0:T(8,128)(2,1)S(1)} %bitcast.83, bf16[1,2048,1792]{2,1,0:T(8,128)(2,1)} %param.22), kind=kOutput, calls=%fused_computation.7 | convolution fusion | flops 5645402112 | bytes 18743296 | tf_op jit(solution)/shard_map/dot_general | solution.py:113
  108.7 0.0 slice-done
  108.7 0.0 slice-done.1
  108.7 7.3 %fusion.8 = bf16[16,2,24,2048]{3,2,1,0:T(8,128)(2,1)} fusion(bf16[16,2,24,1792]{3,2,1,0:T(8,128)(2,1)S(1)} %bitcast.84, bf16[1,1792,2048]{2,1,0:T(8,128)(2,1)S(1)} %bitcast.81), kind=kOutput, calls=%fused_computation.8 | convolution fusion | flops 5638717440 | bytes 13238272 | tf_op jit(solution)/shard_map/dot_general | solution.py:115
  116.0 0.0 all-reduce.3.cloned.1.call-update
  116.1 0.6 copy-done.10
  116.7 0.6 dynamic-slice
  117.3 23.4 %all-reduce.3.cloned.1.call-done = bf16[16,2,24,2048]{3,2,1,0:T(8,128)(2,1)} async-done(((bf16[16,2,24,2048]{3,2,1,0:T(8,128)(2,1)}), bf16[16,2,24,2048]{3,2,1,0:T(8,128)(2,1)}) %all-reduce.3.cloned.1.call-update) | async-done | bytes 3145744
  140.7 3.4 %dynamic-slice_bitcast_fusion = bf16[16,24,2048]{2,1,0:T(8,128)(2,1)} fusion(bf16[16,2,24,2048]{3,2,1,0:T(8,128)(2,1)} %all-reduce.3.cloned.1.call-done, u32[]{:T(128)} %bitcast.29), kind=kLoop, calls=%fused_computation.16 | loop fusion | bytes 3145732 | tf_op jit(solution)/shard_map/reshape | solution.py:120
  144.1 7.0 %all-to-all-start.1 = ((bf16[16,24,2048]{2,1,0:T(8,128)(2,1)}), bf16[16,24,2048]{2,1,0:T(8,128)(2,1)}, u32[]{:S(2)}, u32[]{:S(2)}) async-start(bf16[16,24,2048]{2,1,0:T(8,128)(2,1)} %dynamic-slice_bitcast_fusion), calls=%async_computation.2 | async-start | bytes 3145728 | tf_op jit(solution)/shard_map/all_to_all | solution.py:121
  151.1 0.1 mul.117
  151.2 0.0 copy-done.8
  151.2 0.1 copy.33
  151.3 37.2 %all-to-all-done.1 = bf16[16,24,2048]{2,1,0:T(8,128)(2,1)} async-done(((bf16[16,24,2048]{2,1,0:T(8,128)(2,1)}), bf16[16,24,2048]{2,1,0:T(8,128)(2,1)}, u32[]{:S(2)}, u32[]{:S(2)}) %all-to-all-start.1) | async-done | bytes 1572896 | tf_op jit(solution)/shard_map/all_to_all | solution.py:121
  188.5 5.0 %gather_fusion = bf16[256,2048]{1,0:T(8,128)(2,1)} fusion(bf16[384,2048]{1,0:T(8,128)(2,1)} %bitcast.19, s32[1024]{0:T(1024)S(1)} %pad_clamp_fusion), kind=kCustom, calls=%fused_computation | custom fusion | bytes 2098176 | tf_op jit(solution)/shard_map/gather | solution.py:122
  193.5 3.5 %reshape.286 = f32[128,2,2048]{2,1,0:T(2,128)} reshape(bf16[256,2048]{1,0:T(8,128)(2,1)} %gather_fusion) | data formatting | bytes 3145728 | tf_op jit(solution)/shard_map/convert_element_type | solution.py:125
  197.0 4.9 %multiply_reduce_fusion = f32[128,2048]{1,0:T(8,128)S(1)} fusion(f32[128,2,2048]{2,1,0:T(2,128)} %reshape.286, f32[128,2]{1,0:T(8,128)S(1)} %copy.33), kind=kLoop, calls=%fused_computation.15 | loop fusion | flops 786432 | bytes 3146752 | tf_op jit(solution)/shard_map/reduce_sum | solution.py:125
  201.9 0.0 copy-done.1
  201.9 0.0 copy-done.3
  201.9 1.0 add_convert_fusion
  (24 shorter events, 0.1 us)
Async XLA Ops:
  6.5 11.2 %copy-start = (bf16[512,2048]{1,0:T(8,128)(2,1)S(1)}, bf16[512,2048]{1,0:T(8,128)(2,1)}, u32[]{:S(2)}) copy-start(bf16[512,2048]{1,0:T(8,128)(2,1)} %param.16) | copy-start | bytes 6291460
  6.5 9.9 %copy-start.6 = (f32[8]{0:T(128)S(1)}, f32[8]{0:T(128)}, u32[]{:S(2)}) copy-start(f32[8]{0:T(128)} %param.15) | copy-start | bytes 100
  6.5 23.8 %reduce-scatter.3.cloned.1.call-start = ((), (), s32[]{:S(2)}) async-start(), calls=%async_computation.3 | async-start | bytes 3145728 | tf_op jit(solution)/shard_map/reduce_scatter | solution.py:80
  8.1 6.7 %collective-permute-start = (bf16[128,128]{0,1:T(8,128)(2,1)S(1)}, bf16[128,128]{0,1:T(8,128)(2,1)S(1)}, u32[]{:S(2)}, u32[]{:S(2)}) collective-permute-start(bf16[128,128]{0,1:T(8,128)(2,1)S(1)} %pad_maximum_fusion), channel_id=1, source_target_pairs={{0,2},{2,4},{4,6},{6,8},{8,10},{10,12},{12,14},{14,16},{16,18},{18... | collective-permute-start | bytes 98312 | tf_op jit(solution)/shard_map/ppermute | solution.py:16
  14.8 2.2 %copy-start.5 = (bf16[256,64]{0,1:T(8,128)(2,1)S(1)}, bf16[256,64]{0,1:T(8,128)(2,1)}, u32[]{:S(2)}) copy-start(bf16[256,64]{0,1:T(8,128)(2,1)} %param.14) | copy-start | bytes 98308
  17.7 2.2 %copy-start.7 = (s32[128,2]{0,1:T(2,128)S(1)}, s32[128,2]{0,1:T(2,128)}, u32[]{:S(2)}) copy-start(s32[128,2]{0,1:T(2,128)} %param.19) | copy-start | bytes 3076
  17.7 12.6 %copy-start.2 = (bf16[128,2048]{1,0:T(8,128)(2,1)S(1)}, bf16[128,2048]{1,0:T(8,128)(2,1)}, u32[]{:S(2)}) copy-start(bf16[128,2048]{1,0:T(8,128)(2,1)} %param.17) | copy-start | bytes 1572868
  19.8 12.0 %copy-start.4 = (f32[2048]{0:T(1024)S(1)}, f32[2048]{0:T(1024)}, u32[]{:S(2)}) copy-start(f32[2048]{0:T(1024)} %param.18) | copy-start | bytes 24580
  19.9 69.0 %all-gather.3.cloned.1.call-start = ((), (), s32[]{:S(2)}) async-start(), calls=%async_computation.4 | async-start | bytes 4718592 | tf_op jit(solution)/shard_map/all_gather | solution.py:108
  77.3 63.4 %all-reduce.3.cloned.1.call-start = ((), (), s32[]{:S(2)}) async-start(), calls=%async_computation.5 | async-start | bytes 6291456
  88.9 10.0 %copy-start.9 = (bf16[16,48,2048]{2,1,0:T(8,128)(2,1)S(1)}, bf16[16,48,2048]{2,1,0:T(8,128)(2,1)}, u32[]{:S(2)}) copy-start(bf16[16,48,2048]{2,1,0:T(8,128)(2,1)} %all-gather.3.cloned.1.call-done) | copy-start | bytes 9437188
  88.9 19.8 %slice-start = ((s8[7340032]{0:T(1024)(128)(4,1)}), s8[4194304]{0:T(1024)(128)(4,1)S(1)}, s32[]{:S(2)}) async-start(s8[7340032]{0:T(1024)(128)(4,1)} %bitcast.80), calls=%async_computation.6 | async-start | bytes 8388608
  98.9 9.7 %slice-start.1 = ((s8[7340032]{0:T(1024)(128)(4,1)}), s8[3145728]{0:T(1024)(128)(4,1)S(1)}, s32[]{:S(2)}) async-start(s8[7340032]{0:T(1024)(128)(4,1)} %bitcast.80), calls=%async_computation.7 | async-start | bytes 6291456
  116.0 0.7 copy-start.10
  140.7 10.5 %copy-start.8 = (f32[128,2]{0,1:T(2,128)S(1)}, f32[128,2]{0,1:T(2,128)}, u32[]{:S(2)}) copy-start(f32[128,2]{0,1:T(2,128)} %param.20) | copy-start | bytes 3076
  144.1 44.5 %all-to-all-start.1 = ((bf16[16,24,2048]{2,1,0:T(8,128)(2,1)}), bf16[16,24,2048]{2,1,0:T(8,128)(2,1)}, u32[]{:S(2)}, u32[]{:S(2)}) async-start(bf16[16,24,2048]{2,1,0:T(8,128)(2,1)} %dynamic-slice_bitcast_fusion), calls=%async_computation.2 | async-start | bytes 3145728 | tf_op jit(solution)/shard_map/all_to_all | solution.py:121
  193.5 8.4 %copy-start.1 = (f32[128,2048]{1,0:T(8,128)S(1)}, f32[128,2048]{1,0:T(8,128)}, u32[]{:S(2)}) copy-start(f32[128,2048]{1,0:T(8,128)} %reduce-scatter.3.cloned.1.call-done) | copy-start | bytes 3145732
  197.0 4.9 %copy-start.3 = (bf16[128,2048]{1,0:T(8,128)(2,1)S(1)}, bf16[128,2048]{1,0:T(8,128)(2,1)}, u32[]{:S(2)}) copy-start(bf16[128,2048]{1,0:T(8,128)(2,1)} %param.17) | copy-start | bytes 1572868
Sparse Core Ops, SparseCore 0:
  20.0 10.3 reduce-scatter.2
  77.4 11.4 all-gather.2
  116.2 24.4 all-reduce.2
where the time goes:
time: 210 us; the launch traced here: 209 us
  waiting for transfers between devices  82.7 us (39%)
  blocking collectives  43.6 us (21%)
  matrix products  33.3 us (16%)
  local copies, waits for them, and re-layouts  16.8 us (8%)
  between operations  13.4 us (6%)
  starting transfers between devices  10.6 us (5%)
  other arithmetic  9.03 us (4%)
    all_to_all x1, blocking collectives, on_device(): lax.all_to_all(dispatch.reshape(n_sp, capacity, model_width), 'sp', split...  43.6 us
    all_to_all x1, waiting for transfers between devices, on_device(): lax.all_to_all(expert_out, 'sp', split_axis=0, concat_axis=0, tiled=True)  37.2 us
    unnamed x4, waiting for transfers between devices  23.5 us
    all_gather x1, waiting for transfers between devices, on_device(): lax.all_gather(landed.reshape(n_sp, 1, capacity, model_width), 'tp', axis...  11.4 us
    dot_general x1, matrix products, on_device(): gate = jnp.dot(rows_in, gate_proj[0], preferred_element_type=jnp.float32)  10 us
    dot_general x1, matrix products, on_device(): upper = jnp.dot(rows_in, up_proj[0], preferred_element_type=jnp.float32)  9.71 us
    reduce_scatter x1, waiting for transfers between devices, on_device(): lax.psum_scatter(jnp.dot(attended, out_weight, preferred_element_type=jnp...  8.81 us
    dot_general x1, matrix products, on_device(): jnp.dot(hidden, down_proj[0], preferred_element_type=jnp.float32)  7.35 us
  transfers between devices with their start and end apart: 5, of which 5 were waited for; matrix products, arithmetic and copies ran while one was open for 2% of the time, Pallas kernels for 0%

commit v1 on v0

--- a/solution.py
+++ b/solution.py
@@ -16,20 +16,11 @@
     return lax.ppermute(block, axis, route)
 
 
-def on_device(
-    query_rows,
-    key_rows,
-    value_head_rows,
-    sink_logit_head,
-    out_weight,
-    residual,
-    norm_gain,
-    routes,
-    route_weights,
-    gate_proj,
-    up_proj,
-    down_proj,
-):
+def swap_cores(block):
+    return lax.ppermute(block, "tp", [(0, 1), (1, 0)])
+
+
+def attend(query_rows, key_rows, value_head_rows, sink_logit_head):
     length = query_rows.shape[0]
     query_group = QUERY_HEADS // KEY_VALUE_HEADS
     width = key_rows.shape[1]
@@ -66,7 +57,7 @@
     expd = jnp.exp(score_matrix - peak[..., None])
     denom = jnp.sum(expd, axis=-1) + jnp.exp(sink_portion - peak)
     probabilities = (expd / denom[..., None]).astype(jnp.bfloat16)
-    attended = (
+    return (
         jnp.einsum(
             "wfbt,twj->bwfj",
             probabilities,
@@ -76,54 +67,78 @@
         .reshape(length, local_heads * HEAD_SIZE)
         .astype(jnp.bfloat16)
     )
-    own_rows = length // lax.axis_size("tp")
-    projected = lax.psum_scatter(
-        jnp.dot(attended, out_weight, preferred_element_type=jnp.float32),
-        "tp",
-        scatter_dimension=0,
-        tiled=True,
+
+
+def on_device(
+    query_rows,
+    key_rows,
+    value_head_rows,
+    sink_logit_head,
+    out_weight,
+    residual,
+    norm_gain,
+    routes,
+    route_weights,
+    gate_proj,
+    up_proj,
+    down_proj,
+):
+    n_sp = lax.axis_size("sp")
+    tp_index = lax.axis_index("tp")
+    length = query_rows.shape[0]
+    own_rows = residual.shape[0]
+    width = residual.shape[1]
+    other_weight = swap_cores(out_weight)
+    attended = attend(query_rows, key_rows, value_head_rows, sink_logit_head)
+    mine = lax.dynamic_slice_in_dim(attended, tp_index * own_rows, own_rows, 0)
+    theirs = lax.dynamic_slice_in_dim(attended, (1 - tp_index) * own_rows, own_rows, 0)
+    from_other = swap_cores(theirs)
+    mixed = (
+        residual.astype(jnp.float32)
+        + jnp.dot(mine, out_weight, preferred_element_type=jnp.float32)
+        + jnp.dot(from_other, other_weight, preferred_element_type=jnp.float32)
     )
-    mixed = residual.astype(jnp.float32) + projected
     scale = lax.rsqrt(jnp.mean(mixed * mixed, axis=-1, keepdims=True) + 1e-05)
     normed = (mixed * scale * norm_gain).astype(jnp.bfloat16)
-    n_sp = lax.axis_size("sp")
-    n_tp = lax.axis_size("tp")
     capacity = 3 * own_rows * TOP // (2 * n_sp)
     chosen = routes.reshape(-1)
-    onehot = (chosen[:, None] == jnp.arange(n_sp, dtype=jnp.int32)[None, :]).astype(jnp.int32)
-    running = jnp.cumsum(onehot, axis=0)
-    rank_in = jnp.sum(onehot * running, axis=1) - 1
-    slot_index = chosen * capacity + rank_in
+    onehot = chosen[:, None] == jnp.arange(n_sp, dtype=jnp.int32)[None, :]
+    pairs = chosen.shape[0]
+    order = jnp.arange(pairs, dtype=jnp.int32)
+    lower = (order[:, None] > order[None, :]).astype(jnp.bfloat16)
+    ahead = jnp.dot(lower, onehot.astype(jnp.bfloat16), preferred_element_type=jnp.float32)
+    rank_in = jnp.sum(jnp.where(onehot, ahead, 0.0), axis=1).astype(jnp.int32)
+    slot_index = (chosen * capacity + rank_in).reshape(own_rows, TOP)
     slot_ids = jnp.arange(n_sp * capacity, dtype=jnp.int32)
-    select = jnp.any(
-        slot_index.reshape(own_rows, TOP)[None, :, :] == slot_ids[:, None, None], axis=-1
-    )
+    select = jnp.any(slot_index[None, :, :] == slot_ids[:, None, None], axis=-1)
     dispatch = jnp.dot(
         select.astype(jnp.bfloat16), normed, preferred_element_type=jnp.float32
     ).astype(jnp.bfloat16)
-    model_width = dispatch.shape[1]
     landed = lax.all_to_all(
-        dispatch.reshape(n_sp, capacity, model_width), "sp", split_axis=0, concat_axis=0, tiled=True
-    )
-    arrived = lax.all_gather(
-        landed.reshape(n_sp, 1, capacity, model_width), "tp", axis=1, tiled=True
-    )
-    rows_in = arrived.reshape(-1, model_width)
+        dispatch.reshape(n_sp, capacity, width), "sp", split_axis=0, concat_axis=0, tiled=True
+    ).reshape(n_sp * capacity, width)
+    rows_in = jnp.concatenate([landed, swap_cores(landed)], axis=0)
     gate = jnp.dot(rows_in, gate_proj[0], preferred_element_type=jnp.float32)
     upper = jnp.dot(rows_in, up_proj[0], preferred_element_type=jnp.float32)
     hidden = (jax.nn.silu(gate) * upper).astype(jnp.bfloat16)
-    partial_out = jnp.dot(hidden, down_proj[0], preferred_element_type=jnp.float32)
-    partial_out = partial_out.reshape(n_sp, n_tp, capacity, model_width)
-    summed = lax.psum_scatter(
-        partial_out.astype(jnp.bfloat16), "tp", scatter_dimension=1, tiled=True
-    )
-    expert_out = summed.reshape(n_sp, capacity, model_width)
-    returned = lax.all_to_all(expert_out, "sp", split_axis=0, concat_axis=0, tiled=True)
-    picked = returned.reshape(n_sp * capacity, model_width)[slot_index].reshape(
-        own_rows, TOP, model_width
-    )
-    moe_sum = jnp.sum(route_weights[:, :, None] * picked.astype(jnp.float32), axis=1)
-    return (mixed + moe_sum).astype(jnp.bfloat16)
+    half = n_sp * capacity
+    part_other = jnp.dot(
+        hidden[half:], down_proj[0], preferred_element_type=jnp.float32
+    ).astype(jnp.bfloat16)
+    part_sent = swap_cores(part_other)
+    part_own = jnp.dot(
+        hidden[:half], down_proj[0], preferred_element_type=jnp.float32
+    ).astype(jnp.bfloat16)
+    expert_out = (part_own.astype(jnp.float32) + part_sent.astype(jnp.float32)).astype(jnp.bfloat16)
+    returned = lax.all_to_all(
+        expert_out.reshape(n_sp, capacity, width), "sp", split_axis=0, concat_axis=0, tiled=True
+    ).reshape(half, width)
+    result = mixed
+    for choice in range(TOP):
+        pick = (slot_index[:, choice : choice + 1] == slot_ids[None, :]).astype(jnp.bfloat16)
+        picked = jnp.dot(pick, returned, preferred_element_type=jnp.float32)
+        result = result + route_weights[:, choice : choice + 1] * picked
+    return result.astype(jnp.bfloat16)
 
 
 def solution(mesh):

time: 210 us -> 136 us (0.65)
  waiting for transfers between devices: 82.7 us -> 44.1 us
  between operations: 13.4 us -> 0.31 us
  local copies, waits for them, and re-layouts: 16.8 us -> 4.11 us
  other arithmetic: 9.03 us -> 1.67 us
    unnamed x4 -> x0, waiting for transfers between devices: 23.5 us -> none
    all_gather x1 -> x0, waiting for transfers between devices: 11.4 us -> none  [on_device(): lax.all_gather(landed.reshape(n_sp, 1, capacity, model_width), 'tp', axis...]
    reduce_scatter x1 -> x0, waiting for transfers between devices: 8.81 us -> none  [on_device(): lax.psum_scatter(jnp.dot(attended, out_weight, preferred_element_type=jnp...]
    ppermute x0 -> x4, waiting for transfers between devices: none -> 6.79 us  [swap_cores(): return lax.ppermute(block, 'tp', [(0, 1), (1, 0)])]
    reduce_sum x4 -> x1, other arithmetic: 6.84 us -> 0.43 us  [attend(): denom = jnp.sum(expd, axis=-1) + jnp.exp(sink_portion - peak)]
    gather x1 -> x0, local copies, waits for them, and re-layouts: 4.96 us -> none  [on_device(): returned.reshape(n_sp * capacity, model_width)[slot_index]]
    reshape x1 -> x0, local copies, waits for them, and re-layouts: 3.39 us -> none  [on_device(): expert_out = summed.reshape(n_sp, capacity, model_width)]
    convert_element_type x1 -> x2, local copies, waits for them, and re-layouts: 3.48 us -> 0.19 us  [on_device(): rank_in = jnp.sum(jnp.where(onehot, ahead, 0.0), axis=1).astype(jnp.int32)]
  transfers between devices with their start and end apart: 5 -> 6, of which waited for: 5 -> 4; matrix products, arithmetic and copies ran while one was open for 2% -> 5% of each run, Pallas kernels for 0% -> 0%
where the time goes in v1:
time: 136 us
  waiting for transfers between devices  44.1 us (32%)
  blocking collectives  43 us (32%)
  matrix products  33.3 us (24%)
  starting transfers between devices  9.44 us (7%)
  local copies, waits for them, and re-layouts  4.11 us (3%)
  other arithmetic  1.67 us (1%)
    all_to_all x1, blocking collectives, on_device(): lax.all_to_all(dispatch.reshape(n_sp, capacity, width), 'sp', split_axis=...  43 us
    all_to_all x1, waiting for transfers between devices, on_device(): lax.all_to_all(expert_out.reshape(n_sp, capacity, width), 'sp', split_axi...  37.3 us
    dot_general x1, matrix products, on_device(): upper = jnp.dot(rows_in, up_proj[0], preferred_element_type=jnp.float32)  9.46 us
    dot_general x1, matrix products, on_device(): gate = jnp.dot(rows_in, gate_proj[0], preferred_element_type=jnp.float32)  8.84 us
    ppermute x4, waiting for transfers between devices, swap_cores(): return lax.ppermute(block, 'tp', [(0, 1), (1, 0)])  6.79 us
    all_to_all x1, starting transfers between devices, on_device(): lax.all_to_all(expert_out.reshape(n_sp, capacity, width), 'sp', split_axi...  5.24 us
    dot_general x1, matrix products, on_device(): jnp.dot(hidden[:half], down_proj[0], preferred_element_type=jnp.float32)  4.09 us
    ppermute x1, starting transfers between devices, from_behind(): return lax.ppermute(block, axis, route)  3.39 us
  transfers between devices with their start and end apart: 6, of which 4 were waited for; matrix products, arithmetic and copies ran while one was open for 5% of the time, Pallas kernels for 0%

profile of v1, /device:TPU:12, one launch (start us, length us, event | category | flops | bytes accessed | tf_op | source)
XLA Modules:
  0.0 135.8 jit_solution(3354390552146733387)
XLA Ops:
  0.0 0.7 slice.30
  0.7 0.7 slice.31
  1.4 3.4 %collective-permute-start = (bf16[128,128]{0,1:T(8,128)(2,1)S(1)}, bf16[128,128]{0,1:T(8,128)(2,1)S(1)}, u32[]{:S(2)}, u32[]{:S(2)}) collective-permute-start(bf16[128,128]{0,1:T(8,128)(2,1)S(1)} %pad_maximum_fusion.5), channel_id=1, source_target_pairs={{0,2},{2,4},{4,6},{6,8},{8,10},{10,12},{12,14},{14,16},{16,18},{18... | collective-permute-start | bytes 98312 | tf_op jit(solution)/shard_map/ppermute | solution.py:16
  4.8 0.1 collective-permute-start.2
  5.0 0.0 copy-start.4
  5.0 0.1 subtract_convert_fusion
  5.1 0.2 fusion.35
  5.3 0.8 copy.34
  6.1 0.1 eq.58
  6.2 0.2 fusion.30
  6.4 0.1 convert_element_type.82
  6.6 0.1 copy.35
  6.6 0.7 multiply_add_fusion
  7.4 1.1 copy.32
  8.5 0.0 collective-permute-done
  8.5 0.0 copy-start.3
  8.5 1.6 %fusion.50 = (f32[8,256]{1,0:T(8,128)S(1)}, f32[1,8,256,384]{2,3,1,0:T(8,128)S(1)}) fusion(f32[256,384]{0,1:T(8,128)S(1)} %subtract_convert_fusion, f32[8]{0:T(128)S(1)} %multiply_exponential_fusion, bf16[256,8,64]{0,2,1:T(8,128)(2,1)S(1)} %bitcast.72, bf16[256,64]{0,1:T(8,128)(2,1)} %param.13, bf16[128,64]{0,1:T(8,128)(2,1)S(1)} %get-tuple-element.6, ...), kind=kOutput, calls=%fused_computation.78 | convolution fusion | flops 104691712 | bytes 3956768 | tf_op jit(solution)/shard_map/rjwh,cjh->jwrc/dot_general | solution.py:37
  10.1 0.0 copy-done.4
  10.1 0.1 broadcast_maximum_fusion
  10.2 0.4 fusion.15
  10.6 0.1 exponential_add_fusion
  10.7 0.0 copy-done.3
  10.7 0.0 copy-start
  10.7 0.0 copy-start.1
  10.7 0.7 fusion.27
  11.5 0.0 copy-start.2
  11.5 0.5 collective-permute-start.1
  12.0 0.3 copy-done
  12.3 0.1 copy-done.1
  12.4 0.0 slice-start
  12.4 0.5 convolution_add_fusion.1
  12.9 0.0 slice-start.1
  12.9 0.1 collective-permute-done.1
  13.0 0.0 collective-permute-done.2
  13.0 2.4 %multiply_reduce_fusion = (f32[128]{0:T(128)S(1)}, f32[128,2048]{1,0:T(8,128)S(1)}) fusion(f32[128,2048]{1,0:T(8,128)S(1)} %convolution_add_fusion.1, bf16[128,512]{0,1:T(8,128)(2,1)S(1)} %collective-permute-done.1, bf16[512,2048]{1,0:T(8,128)(2,1)} %collective-permute-done.2), kind=kOutput, calls=%fused_computation.34 | convolution fusion | flops 269221760 | bytes 4325888 | tf_op jit(solution)/shard_map/dot_general | solution.py:99
  15.4 0.0 copy-done.2
  15.5 0.6 convolution_convert_fusion
  16.1 43.0 %all_to_all.10 = bf16[16,24,2048]{2,1,0:T(8,128)(2,1)S(1)} all-to-all(bf16[16,24,2048]{2,1,0:T(8,128)(2,1)S(1)} %bitcast.65), channel_id=1, replica_groups=mesh['sp'=16,'tp'=2] {'sp'}, dimensions={0} | all-to-all | bytes 3145728 | tf_op jit(solution)/shard_map/all_to_all | solution.py:117
  59.1 0.0 slice-start.2
  59.1 0.0 slice-start.3
  59.1 0.0 collective-permute-start.3
  59.1 3.4 %collective-permute-done.3 = bf16[384,2048]{1,0:T(8,128)(2,1)S(1)} collective-permute-done((bf16[384,2048]{1,0:T(8,128)(2,1)S(1)}, bf16[384,2048]{1,0:T(8,128)(2,1)S(1)}, u32[]{:S(2)}, u32[]{:S(2)}) %collective-permute-start.3) | collective-permute-done | bytes 1572896 | tf_op jit(solution)/shard_map/ppermute | solution.py:20
  62.5 0.0 slice-done
  62.5 0.0 slice-done.1
  62.5 0.0 slice-start.4
  62.5 8.8 %fusion.6 = f32[768,1792]{1,0:T(8,128)} fusion(bf16[1,2048,1792]{2,1,0:T(8,128)(2,1)S(1)} %bitcast.74, bf16[384,2048]{1,0:T(8,128)(2,1)S(1)} %collective-permute-done.3, bf16[384,2048]{1,0:T(8,128)(2,1)S(1)} %bitcast.68), kind=kOutput, calls=%fused_computation.6 | convolution fusion | flops 5643436032 | bytes 15990784 | tf_op jit(solution)/shard_map/dot_general | solution.py:121
  71.3 0.0 slice-done.2
  71.3 0.0 slice-done.3
  71.3 0.0 slice-start.5
  71.3 9.5 %multiply_convert_fusion = bf16[768,1792]{1,0:T(8,128)(2,1)S(1)} fusion(f32[768,1792]{1,0:T(8,128)} %fusion.6, bf16[1,2048,1792]{2,1,0:T(8,128)(2,1)S(1)} %bitcast.76, bf16[384,2048]{1,0:T(8,128)(2,1)S(1)} %collective-permute-done.3, bf16[384,2048]{1,0:T(8,128)(2,1)S(1)} %bitcast.69), kind=kOutput, calls=%fused_computation.8 | convolution fusion | flops 5651693568 | bytes 18743296 | tf_op jit(solution)/shard_map/dot_general | solution.py:122
  80.8 0.0 slice-done.4
  80.8 0.0 slice-done.5
  80.8 3.0 %fusion.12 = bf16[384,2048]{1,0:T(8,128)(2,1)S(1)} fusion(bf16[1,1792,2048]{2,1,0:T(8,128)(2,1)S(1)} %bitcast.78, bf16[768,1792]{1,0:T(8,128)(2,1)S(1)} %multiply_convert_fusion), kind=kOutput, calls=%fused_computation.16 | convolution fusion | flops 2819358720 | bytes 10289152 | tf_op jit(solution)/shard_map/dot_general | solution.py:125
  83.9 0.2 collective-permute-start.4
  84.1 3.3 %collective-permute-done.4 = bf16[384,2048]{1,0:T(8,128)(2,1)S(1)} collective-permute-done((bf16[384,2048]{1,0:T(8,128)(2,1)S(1)}, bf16[384,2048]{1,0:T(8,128)(2,1)S(1)}, u32[]{:S(2)}, u32[]{:S(2)}) %collective-permute-start.4) | collective-permute-done | bytes 1572896 | tf_op jit(solution)/shard_map/ppermute | solution.py:20
  87.3 4.1 %add_convert_fusion = bf16[384,2048]{1,0:T(8,128)(2,1)} fusion(bf16[384,2048]{1,0:T(8,128)(2,1)S(1)} %collective-permute-done.4, bf16[1,1792,2048]{2,1,0:T(8,128)(2,1)S(1)} %bitcast.78, bf16[768,1792]{1,0:T(8,128)(2,1)S(1)} %multiply_convert_fusion), kind=kOutput, calls=%fused_computation.12 | convolution fusion | flops 2822504448 | bytes 11862016 | tf_op jit(solution)/shard_map/dot_general | solution.py:129
  91.4 0.0 copy-start.5
  91.4 5.2 %all-to-all-start.1 = ((bf16[16,24,2048]{2,1,0:T(8,128)(2,1)}), bf16[16,24,2048]{2,1,0:T(8,128)(2,1)S(1)}, u32[]{:S(2)}, u32[]{:S(2)}) async-start(bf16[16,24,2048]{2,1,0:T(8,128)(2,1)} %bitcast.66), calls=%async_computation.1 | async-start | bytes 3145728 | tf_op jit(solution)/shard_map/all_to_all | solution.py:133
  96.7 0.0 copy-done.5
  96.7 37.3 %all-to-all-done.1 = bf16[16,24,2048]{2,1,0:T(8,128)(2,1)S(1)} async-done(((bf16[16,24,2048]{2,1,0:T(8,128)(2,1)}), bf16[16,24,2048]{2,1,0:T(8,128)(2,1)S(1)}, u32[]{:S(2)}, u32[]{:S(2)}) %all-to-all-start.1) | async-done | bytes 1572896 | tf_op jit(solution)/shard_map/all_to_all | solution.py:133
  134.0 0.5 convolution_multiply_fusion
  134.5 1.3 fusion.20
  (15 shorter events, 0.1 us)
Async XLA Ops:
  1.4 7.1 %collective-permute-start = (bf16[128,128]{0,1:T(8,128)(2,1)S(1)}, bf16[128,128]{0,1:T(8,128)(2,1)S(1)}, u32[]{:S(2)}, u32[]{:S(2)}) collective-permute-start(bf16[128,128]{0,1:T(8,128)(2,1)S(1)} %pad_maximum_fusion.5), channel_id=1, source_target_pairs={{0,2},{2,4},{4,6},{6,8},{8,10},{10,12},{12,14},{14,16},{16,18},{18... | collective-permute-start | bytes 98312 | tf_op jit(solution)/shard_map/ppermute | solution.py:16
  4.8 8.2 %collective-permute-start.2 = (bf16[512,2048]{1,0:T(8,128)(2,1)}, bf16[512,2048]{1,0:T(8,128)(2,1)}, u32[]{:S(2)}, u32[]{:S(2)}) collective-permute-start(bf16[512,2048]{1,0:T(8,128)(2,1)} %param.16), channel_id=1, source_target_pairs={{0,1},{1,0},{2,3},{3,2},{4,5},{5,4},{6,7},{7,6},{8,9},{9,8},{10,11... | collective-permute-start | bytes 6291464 | tf_op jit(solution)/shard_map/ppermute | solution.py:20
  5.0 5.2 %copy-start.4 = (f32[8]{0:T(128)S(1)}, f32[8]{0:T(128)}, u32[]{:S(2)}) copy-start(f32[8]{0:T(128)} %param.15) | copy-start | bytes 100
  8.5 2.2 %copy-start.3 = (bf16[256,64]{0,1:T(8,128)(2,1)S(1)}, bf16[256,64]{0,1:T(8,128)(2,1)}, u32[]{:S(2)}) copy-start(bf16[256,64]{0,1:T(8,128)(2,1)} %param.14) | copy-start | bytes 98308
  10.7 1.6 %copy-start = (bf16[512,2048]{1,0:T(8,128)(2,1)S(1)}, bf16[512,2048]{1,0:T(8,128)(2,1)}, u32[]{:S(2)}) copy-start(bf16[512,2048]{1,0:T(8,128)(2,1)} %param.16) | copy-start | bytes 6291460
  10.7 1.7 %copy-start.1 = (bf16[128,2048]{1,0:T(8,128)(2,1)S(1)}, bf16[128,2048]{1,0:T(8,128)(2,1)}, u32[]{:S(2)}) copy-start(bf16[128,2048]{1,0:T(8,128)(2,1)} %param.17) | copy-start | bytes 1572868
  11.5 4.0 %copy-start.2 = (f32[2048]{0:T(1024)S(1)}, f32[2048]{0:T(1024)}, u32[]{:S(2)}) copy-start(f32[2048]{0:T(1024)} %param.18) | copy-start | bytes 24580
  11.5 1.5 %collective-permute-start.1 = (bf16[128,512]{0,1:T(8,128)(2,1)S(1)}, bf16[128,512]{0,1:T(8,128)(2,1)S(1)}, u32[]{:S(2)}, u32[]{:S(2)}) collective-permute-start(bf16[128,512]{0,1:T(8,128)(2,1)S(1)} %constant_dynamic-slice_fusion), channel_id=1, source_target_pairs={{0,1},{1,0},{2,3},{3,2},{4,5},{5,4},{6,7},{7,6},{8,9},{9,8},{10,11... | collective-permute-start | bytes 393224 | tf_op jit(solution)/shard_map/ppermute | solution.py:20
  12.4 50.1 %slice-start = ((s8[7340032]{0:T(1024)(128)(4,1)}), s8[4194304]{0:T(1024)(128)(4,1)S(1)}, s32[]{:S(2)}) async-start(s8[7340032]{0:T(1024)(128)(4,1)} %bitcast.73), calls=%async_computation.2 | async-start | bytes 8388608
  12.9 49.6 %slice-start.1 = ((s8[7340032]{0:T(1024)(128)(4,1)}), s8[3145728]{0:T(1024)(128)(4,1)S(1)}, s32[]{:S(2)}) async-start(s8[7340032]{0:T(1024)(128)(4,1)} %bitcast.73), calls=%async_computation.3 | async-start | bytes 6291456
  59.1 12.3 %slice-start.2 = ((s8[7340032]{0:T(1024)(128)(4,1)}), s8[4194304]{0:T(1024)(128)(4,1)S(1)}, s32[]{:S(2)}) async-start(s8[7340032]{0:T(1024)(128)(4,1)} %bitcast.75), calls=%async_computation.4 | async-start | bytes 8388608
  59.1 12.3 %slice-start.3 = ((s8[7340032]{0:T(1024)(128)(4,1)}), s8[3145728]{0:T(1024)(128)(4,1)S(1)}, s32[]{:S(2)}) async-start(s8[7340032]{0:T(1024)(128)(4,1)} %bitcast.75), calls=%async_computation.5 | async-start | bytes 6291456
  59.1 3.4 %collective-permute-start.3 = (bf16[384,2048]{1,0:T(8,128)(2,1)S(1)}, bf16[384,2048]{1,0:T(8,128)(2,1)S(1)}, u32[]{:S(2)}, u32[]{:S(2)}) collective-permute-start(bf16[384,2048]{1,0:T(8,128)(2,1)S(1)} %bitcast.67), channel_id=1, source_target_pairs={{0,1},{1,0},{2,3},{3,2},{4,5},{5,4},{6,7},{7,6},{8,9},{9,8},{10,11... | collective-permute-start | bytes 4718600 | tf_op jit(solution)/shard_map/ppermute | solution.py:20
  62.5 18.3 %slice-start.4 = ((s8[7340032]{0:T(1024)(128)(4,1)}), s8[4194304]{0:T(1024)(128)(4,1)S(1)}, s32[]{:S(2)}) async-start(s8[7340032]{0:T(1024)(128)(4,1)} %bitcast.77), calls=%async_computation.6 | async-start | bytes 8388608
  71.3 9.5 %slice-start.5 = ((s8[7340032]{0:T(1024)(128)(4,1)}), s8[3145728]{0:T(1024)(128)(4,1)S(1)}, s32[]{:S(2)}) async-start(s8[7340032]{0:T(1024)(128)(4,1)} %bitcast.77), calls=%async_computation.7 | async-start | bytes 6291456
  83.9 3.5 %collective-permute-start.4 = (bf16[384,2048]{1,0:T(8,128)(2,1)S(1)}, bf16[384,2048]{1,0:T(8,128)(2,1)S(1)}, u32[]{:S(2)}, u32[]{:S(2)}) collective-permute-start(bf16[384,2048]{1,0:T(8,128)(2,1)S(1)} %fusion.12), channel_id=1, source_target_pairs={{0,1},{1,0},{2,3},{3,2},{4,5},{5,4},{6,7},{7,6},{8,9},{9,8},{10,11... | collective-permute-start | bytes 4718600 | tf_op jit(solution)/shard_map/ppermute | solution.py:20
  91.4 5.3 %copy-start.5 = (f32[128,2]{0,1:T(2,128)S(1)}, f32[128,2]{0,1:T(2,128)}, u32[]{:S(2)}) copy-start(f32[128,2]{0,1:T(2,128)} %param.20) | copy-start | bytes 3076
  91.4 42.6 %all-to-all-start.1 = ((bf16[16,24,2048]{2,1,0:T(8,128)(2,1)}), bf16[16,24,2048]{2,1,0:T(8,128)(2,1)S(1)}, u32[]{:S(2)}, u32[]{:S(2)}) async-start(bf16[16,24,2048]{2,1,0:T(8,128)(2,1)} %bitcast.66), calls=%async_computation.1 | async-start | bytes 3145728 | tf_op jit(solution)/shard_map/all_to_all | solution.py:133

commit v2 on v1

--- a/solution.py
+++ b/solution.py
@@ -1,13 +1,19 @@
+import functools
+
 import jax
 import jax.numpy as jnp
 from jax import lax
+from jax.experimental import pallas as pl
+from jax.experimental.pallas import tpu as pltpu
 from jax.sharding import PartitionSpec as P
+
 
 QUERY_HEADS = 16
 KEY_VALUE_HEADS = 2
 HEAD_SIZE = 64
 TOP = 2
 WINDOW_KEYS = 128
+PLANES = 4
 
 
 def from_behind(block, axis, distance):
@@ -67,6 +73,63 @@
         .reshape(length, local_heads * HEAD_SIZE)
         .astype(jnp.bfloat16)
     )
+
+
+BLOCK = 256
+
+
+def gather_rows(pieces, rows_ref):
+    start = 0
+    for piece in pieces:
+        rows_ref[start : start + piece.shape[0], :] = piece[...]
+        start += piece.shape[0]
+
+
+def expert_body(*refs, count):
+    pieces, (gate_ref, up_ref, down_ref, own_ref, other_ref, rows_ref, hidden_ref) = (
+        refs[:count],
+        refs[count:],
+    )
+    gather_rows(pieces, rows_ref)
+    for start in range(0, gate_ref.shape[1], BLOCK):
+        units = slice(start, start + BLOCK)
+        rows = rows_ref[...]
+        gate = jnp.dot(rows, gate_ref[:, units], preferred_element_type=jnp.float32)
+        upper = jnp.dot(rows, up_ref[:, units], preferred_element_type=jnp.float32)
+        hidden_ref[:, units] = (gate / (1.0 + jnp.exp(-gate)) * upper).astype(jnp.bfloat16)
+    half = own_ref.shape[0]
+    for start in range(0, down_ref.shape[1], BLOCK):
+        units = slice(start, start + BLOCK)
+        part = jnp.dot(
+            hidden_ref[...], down_ref[:, units], preferred_element_type=jnp.float32
+        ).astype(jnp.bfloat16)
+        own_ref[:, units] = part[:half]
+        other_ref[:, units] = part[half:]
+
+
+def expert_parts(pieces, weights):
+    width, hidden_units = weights[0].shape
+    if any(piece.shape[0] % 8 for piece in pieces):
+        pieces = [jnp.concatenate(pieces, axis=0)]
+    rows = sum(piece.shape[0] for piece in pieces)
+    half = jax.ShapeDtypeStruct((rows // 2, width), jnp.bfloat16)
+    inside = pl.BlockSpec(memory_space=pltpu.VMEM)
+    return pl.pallas_call(
+        functools.partial(expert_body, count=len(pieces)),
+        in_specs=[inside] * (len(pieces) + 3),
+        out_specs=[inside] * 2,
+        out_shape=[half, half],
+        scratch_shapes=[
+            pltpu.VMEM((rows, width), jnp.bfloat16),
+            pltpu.VMEM((rows, hidden_units), jnp.bfloat16),
+        ],
+        compiler_params=pltpu.CompilerParams(vmem_limit_bytes=8 * 2**20),
+        cost_estimate=pl.CostEstimate(
+            flops=6 * rows * width * hidden_units,
+            transcendentals=rows * hidden_units,
+            bytes_accessed=6 * width * hidden_units,
+        ),
+    )(*pieces, *weights)
 
 
 def on_device(
@@ -85,7 +148,6 @@
 ):
     n_sp = lax.axis_size("sp")
     tp_index = lax.axis_index("tp")
-    length = query_rows.shape[0]
     own_rows = residual.shape[0]
     width = residual.shape[1]
     other_weight = swap_cores(out_weight)
@@ -100,7 +162,9 @@
     )
     scale = lax.rsqrt(jnp.mean(mixed * mixed, axis=-1, keepdims=True) + 1e-05)
     normed = (mixed * scale * norm_gain).astype(jnp.bfloat16)
+    plane = n_sp // PLANES
     capacity = 3 * own_rows * TOP // (2 * n_sp)
+    group = plane * capacity
     chosen = routes.reshape(-1)
     onehot = chosen[:, None] == jnp.arange(n_sp, dtype=jnp.int32)[None, :]
     pairs = chosen.shape[0]
@@ -108,37 +172,65 @@
     lower = (order[:, None] > order[None, :]).astype(jnp.bfloat16)
     ahead = jnp.dot(lower, onehot.astype(jnp.bfloat16), preferred_element_type=jnp.float32)
     rank_in = jnp.sum(jnp.where(onehot, ahead, 0.0), axis=1).astype(jnp.int32)
-    slot_index = (chosen * capacity + rank_in).reshape(own_rows, TOP)
-    slot_ids = jnp.arange(n_sp * capacity, dtype=jnp.int32)
-    select = jnp.any(slot_index[None, :, :] == slot_ids[:, None, None], axis=-1)
-    dispatch = jnp.dot(
-        select.astype(jnp.bfloat16), normed, preferred_element_type=jnp.float32
-    ).astype(jnp.bfloat16)
-    landed = lax.all_to_all(
-        dispatch.reshape(n_sp, capacity, width), "sp", split_axis=0, concat_axis=0, tiled=True
-    ).reshape(n_sp * capacity, width)
-    rows_in = jnp.concatenate([landed, swap_cores(landed)], axis=0)
-    gate = jnp.dot(rows_in, gate_proj[0], preferred_element_type=jnp.float32)
-    upper = jnp.dot(rows_in, up_proj[0], preferred_element_type=jnp.float32)
-    hidden = (jax.nn.silu(gate) * upper).astype(jnp.bfloat16)
-    half = n_sp * capacity
-    part_other = jnp.dot(
-        hidden[half:], down_proj[0], preferred_element_type=jnp.float32
-    ).astype(jnp.bfloat16)
-    part_sent = swap_cores(part_other)
-    part_own = jnp.dot(
-        hidden[:half], down_proj[0], preferred_element_type=jnp.float32
-    ).astype(jnp.bfloat16)
-    expert_out = (part_own.astype(jnp.float32) + part_sent.astype(jnp.float32)).astype(jnp.bfloat16)
-    returned = lax.all_to_all(
-        expert_out.reshape(n_sp, capacity, width), "sp", split_axis=0, concat_axis=0, tiled=True
-    ).reshape(half, width)
-    result = mixed
-    for choice in range(TOP):
-        pick = (slot_index[:, choice : choice + 1] == slot_ids[None, :]).astype(jnp.bfloat16)
-        picked = jnp.dot(pick, returned, preferred_element_type=jnp.float32)
-        result = result + route_weights[:, choice : choice + 1] * picked
-    return result.astype(jnp.bfloat16)
+    relative = jnp.bitwise_xor(chosen, lax.axis_index("sp"))
+    slot_index = (relative * capacity + rank_in).reshape(own_rows, TOP)
+
+    def ids(number):
+        return number * group + jnp.arange(group, dtype=jnp.int32)
+
+    weights = [
+        pltpu.with_memory_space_constraint(w[0], pltpu.VMEM)
+        for w in (gate_proj, up_proj, down_proj)
+    ]
+
+    def selected(number):
+        select = jnp.any(slot_index[None, :, :] == ids(number)[:, None, None], axis=-1)
+        return jnp.dot(
+            select.astype(jnp.bfloat16), normed, preferred_element_type=jnp.float32
+        ).astype(jnp.bfloat16)
+
+    def across(block, distance):
+        return lax.ppermute(block, "sp", [(i, i ^ distance) for i in range(n_sp)])
+
+    def pieces(block):
+        rows = block.shape[0] // plane
+        return [block[rows * j : rows * (j + 1)] for j in range(plane)]
+
+    def in_plane(parts):
+        return [parts[0]] + [across(parts[j], j) for j in range(1, plane)]
+
+    def expert(parts):
+        rows = jnp.concatenate(parts, axis=0) if len(parts) > 1 else parts[0]
+        other = swap_cores(rows)
+        own_part, other_part = expert_parts([rows, other], weights)
+        added = swap_cores(other_part)
+        return (own_part.astype(jnp.float32) + added.astype(jnp.float32)).astype(jnp.bfloat16)
+
+    arrived = {number: across(selected(number), number * plane) for number in (3, 1, 2)}
+    arrived[0] = selected(0)
+    out = {number: expert(in_plane(pieces(arrived[number]))) for number in (0, 3, 1, 2)}
+    far_back = in_plane(pieces(across(out[3], 3 * plane)))
+    one_back = across(out[1], plane)
+    near = [jnp.concatenate(two, axis=0) for two in zip(pieces(out[0]), pieces(one_back))]
+    near_back = in_plane(near)
+    mid_back = [across(p, 2 * plane + j) for j, p in enumerate(pieces(out[2]))]
+
+    total = jnp.zeros((TOP * own_rows, width), jnp.float32)
+    slots = slot_index.T.reshape(-1, 1)
+    near_ids = jnp.arange(2 * group, dtype=jnp.int32)
+    near_ids = (
+        near_ids // capacity % 2 * group
+        + near_ids // (2 * capacity) * capacity
+        + near_ids % capacity
+    )
+    groups = ((near_ids, near_back), (ids(3), far_back), (ids(2), mid_back))
+    for numbers, back in groups:
+        pick = (slots == numbers[None, :]).astype(jnp.bfloat16)
+        total = total + jnp.dot(
+            pick, jnp.concatenate(back, axis=0), preferred_element_type=jnp.float32
+        )
+    weighted = route_weights.T.reshape(-1, 1) * total
+    return (mixed + jnp.sum(weighted.reshape(TOP, own_rows, width), axis=0)).astype(jnp.bfloat16)
 
 
 def solution(mesh):
@@ -156,6 +248,7 @@
         P("sp", None, "tp"),
         P("sp", "tp", None),
     )
+
     return jax.shard_map(
         on_device, mesh=mesh, in_specs=placed, out_specs=P(("sp", "tp"), None), check_vma=False
     )

time: 136 us -> 143 us (1.051); the launches traced: 136 us -> 141 us
  blocking collectives: 43 us -> 0 us
  starting transfers between devices: 9.44 us -> 41 us
  matrix products: 33.3 us -> 6.13 us
  waiting for transfers between devices: 44.1 us -> 64.6 us
  Pallas kernels: 0 us -> 18.7 us
  other arithmetic: 1.67 us -> 5.85 us
    ppermute x0 -> x27, waiting for transfers between devices: none -> 64.4 us  [across(): return lax.ppermute(block, 'sp', [(i, i ^ distance) for i in range(n_sp)])]
    all_to_all x1 -> x0, blocking collectives: 43 us -> none  [on_device(): lax.all_to_all(dispatch.reshape(n_sp, capacity, width), 'sp', split_axis=...]
    all_to_all x1 -> x0, waiting for transfers between devices: 37.3 us -> none  [on_device(): lax.all_to_all(expert_out.reshape(n_sp, capacity, width), 'sp', split_axi...]
    ppermute x0 -> x27, starting transfers between devices: none -> 35.2 us  [across(): return lax.ppermute(block, 'sp', [(i, i ^ distance) for i in range(n_sp)])]
    dot_general x7, matrix products: 27.9 us -> 2.51 us  [the longest x3 1.47 us: on_device(): jnp.dot(pick, jnp.concatenate(back, axis=0), preferred_element_type=jnp.f...]
    pallas_call x0 -> x4, Pallas kernels: none -> 18.7 us  [expert_parts(): pl.pallas_call(functools.partial(expert_body, count=len(pieces)), in_spec...]
    ppermute x4 -> x10, waiting for transfers between devices: 6.79 us -> 0.17 us  [swap_cores(): return lax.ppermute(block, 'tp', [(0, 1), (1, 0)])]
    all_to_all x1 -> x0, starting transfers between devices: 5.24 us -> none  [on_device(): lax.all_to_all(expert_out.reshape(n_sp, capacity, width), 'sp', split_axi...]
  transfers between devices with their start and end apart: 6 -> 38, of which waited for: 4 -> 17; matrix products, arithmetic and copies ran while one was open for 5% -> 7% of each run, Pallas kernels for 0% -> 13%
where the time goes in v2:
time: 143 us; the launch traced here: 141 us
  waiting for transfers between devices  64.6 us (45%)
  starting transfers between devices  41 us (29%)
  Pallas kernels  18.7 us (13%)
  matrix products  6.13 us (4%)
  other arithmetic  5.85 us (4%)
  local copies, waits for them, and re-layouts  4.35 us (3%)
    ppermute x27, waiting for transfers between devices, across(): return lax.ppermute(block, 'sp', [(i, i ^ distance) for i in range(n_sp)])  64.4 us
    ppermute x27, starting transfers between devices, across(): return lax.ppermute(block, 'sp', [(i, i ^ distance) for i in range(n_sp)])  35.2 us
    pallas_call x4, Pallas kernels, expert_parts(): pl.pallas_call(functools.partial(expert_body, count=len(pieces)), in_spec...  18.7 us
    ppermute x1, starting transfers between devices, from_behind(): return lax.ppermute(block, axis, route)  3.39 us
  transfers between devices with their start and end apart: 38, of which 17 were waited for; matrix products, arithmetic and copies ran while one was open for 7% of the time, Pallas kernels for 13%

profile of v2, /device:TPU:12, one launch (start us, length us, event | category | flops | bytes accessed | tf_op | source)
XLA Modules:
  0.0 141.3 jit_solution(1791772178883934998)
XLA Ops:
  0.0 0.7 slice.108
  0.7 0.7 slice.109
  1.4 3.4 %collective-permute-start = (bf16[128,128]{0,1:T(8,128)(2,1)S(1)}, bf16[128,128]{0,1:T(8,128)(2,1)S(1)}, u32[]{:S(2)}, u32[]{:S(2)}) collective-permute-start(bf16[128,128]{0,1:T(8,128)(2,1)S(1)} %pad_maximum_fusion.7), channel_id=1, source_target_pairs={{0,2},{2,4},{4,6},{6,8},{8,10},{10,12},{12,14},{14,16},{16,18},{18... | collective-permute-start | bytes 98312 | tf_op jit(solution)/shard_map/ppermute | solution.py:22
  5.3 0.8 copy.33
  6.7 0.7 multiply_add_fusion
  7.5 1.1 copy.31
  8.7 1.7 %fusion.66 = (f32[8,256]{1,0:T(8,128)S(1)}, f32[1,8,256,384]{2,3,1,0:T(8,128)S(1)}) fusion(f32[256,384]{0,1:T(8,128)S(1)} %subtract_convert_fusion, f32[8]{0:T(128)S(1)} %multiply_exponential_fusion, bf16[256,8,64]{0,2,1:T(8,128)(2,1)S(1)} %bitcast.69, bf16[256,64]{0,1:T(8,128)(2,1)} %param.13, bf16[128,64]{0,1:T(8,128)(2,1)S(1)} %get-tuple-element.58, ...), kind=kOutput, calls=%fused_computation.129 | convolution fusion | flops 104691712 | bytes 3956768 | tf_op jit(solution)/shard_map/rjwh,cjh->jwrc/dot_general | solution.py:43
  10.4 0.4 fusion.1
  11.0 0.7 fusion.6
  11.8 0.5 collective-permute-start.1
  12.7 0.5 convolution_add_fusion.2
  13.3 0.6 multiply_reduce_fusion
  14.3 1.6 %collective-permute-start.3 = (bf16[24,2048]{1,0:T(8,128)(2,1)S(1)}, bf16[24,2048]{1,0:T(8,128)(2,1)S(1)}, u32[]{:S(2)}, u32[]{:S(2)}) collective-permute-start(bf16[24,2048]{1,0:T(8,128)(2,1)S(1)} %get-tuple-element.40), channel_id=1, source_target_pairs={{0,2},{2,0},{4,6},{6,4},{8,10},{10,8},{12,14},{14,12},{16,18},{18,... | collective-permute-start | bytes 294920 | tf_op jit(solution)/shard_map/ppermute | solution.py:193
  15.9 0.5 collective-permute-start.4
  16.4 1.5 %collective-permute-start.5 = (bf16[24,2048]{1,0:T(8,128)(2,1)S(1)}, bf16[24,2048]{1,0:T(8,128)(2,1)S(1)}, u32[]{:S(2)}, u32[]{:S(2)}) collective-permute-start(bf16[24,2048]{1,0:T(8,128)(2,1)S(1)} %get-tuple-element.38), channel_id=1, source_target_pairs={{0,6},{2,4},{4,2},{6,0},{8,14},{10,12},{12,10},{14,8},{16,22},{18,... | collective-permute-start | bytes 294920 | tf_op jit(solution)/shard_map/ppermute | solution.py:193
  18.2 0.5 collective-permute-start.8
  19.0 2.8 %collective-permute-start.18 = (bf16[96,2048]{1,0:T(8,128)(2,1)S(1)}, bf16[96,2048]{1,0:T(8,128)(2,1)S(1)}, u32[]{:S(2)}, u32[]{:S(2)}) collective-permute-start(bf16[96,2048]{1,0:T(8,128)(2,1)S(1)} %convolution_convert_fusion.1), channel_id=1, source_target_pairs={{0,24},{2,26},{4,28},{6,30},{8,16},{10,18},{12,20},{14,22},{16,8},... | collective-permute-start | bytes 1179656 | tf_op jit(solution)/shard_map/ppermute | solution.py:193
  22.0 1.3 collective-permute-start.28
  23.4 6.8 %collective-permute-done.8 = bf16[96,2048]{1,0:T(8,128)(2,1)S(1)} collective-permute-done((bf16[96,2048]{1,0:T(8,128)(2,1)S(1)}, bf16[96,2048]{1,0:T(8,128)(2,1)S(1)}, u32[]{:S(2)}, u32[]{:S(2)}) %collective-permute-start.8) | collective-permute-done | bytes 393248 | tf_op jit(solution)/shard_map/ppermute | solution.py:193
  30.3 0.8 collective-permute-start.10
  31.1 2.2 %collective-permute-start.11 = (bf16[24,2048]{1,0:T(8,128)(2,1)S(1)}, bf16[24,2048]{1,0:T(8,128)(2,1)S(1)}, u32[]{:S(2)}, u32[]{:S(2)}) collective-permute-start(bf16[24,2048]{1,0:T(8,128)(2,1)S(1)} %get-tuple-element.34), channel_id=1, source_target_pairs={{0,6},{2,4},{4,2},{6,0},{8,14},{10,12},{12,10},{14,8},{16,22},{18,... | collective-permute-start | bytes 294920 | tf_op jit(solution)/shard_map/ppermute | solution.py:193
  33.3 15.3 %collective-permute-done.18 = bf16[96,2048]{1,0:T(8,128)(2,1)S(1)} collective-permute-done((bf16[96,2048]{1,0:T(8,128)(2,1)S(1)}, bf16[96,2048]{1,0:T(8,128)(2,1)S(1)}, u32[]{:S(2)}, u32[]{:S(2)}) %collective-permute-start.18) | collective-permute-done | bytes 393248 | tf_op jit(solution)/shard_map/ppermute | solution.py:193
  48.5 0.8 collective-permute-start.9
  49.4 5.4 %collective-permute-done.28 = bf16[96,2048]{1,0:T(8,128)(2,1)S(1)} collective-permute-done((bf16[96,2048]{1,0:T(8,128)(2,1)S(1)}, bf16[96,2048]{1,0:T(8,128)(2,1)S(1)}, u32[]{:S(2)}, u32[]{:S(2)}) %collective-permute-start.28) | collective-permute-done | bytes 393248 | tf_op jit(solution)/shard_map/ppermute | solution.py:193
  54.8 0.4 collective-permute-start.19
  55.2 1.7 %collective-permute-start.20 = (bf16[24,2048]{1,0:T(8,128)(2,1)S(1)}, bf16[24,2048]{1,0:T(8,128)(2,1)S(1)}, u32[]{:S(2)}, u32[]{:S(2)}) collective-permute-start(bf16[24,2048]{1,0:T(8,128)(2,1)S(1)} %get-tuple-element.47), channel_id=1, source_target_pairs={{0,4},{2,6},{4,0},{6,2},{8,12},{10,14},{12,8},{14,10},{16,20},{18,... | collective-permute-start | bytes 294920 | tf_op jit(solution)/shard_map/ppermute | solution.py:193
  56.9 4.6 %shard_map.118 = (bf16[96,2048]{1,0:T(8,128)(2,1)S(1)}, bf16[96,2048]{1,0:T(8,128)(2,1)S(1)}) custom-call(bf16[96,2048]{1,0:T(8,128)(2,1)S(1)} %pad_maximum_fusion.refs_0_, bf16[96,2048]{1,0:T(8,128)(2,1)S(1)} %collective-permute-done.6.refs_1_, bf16[2048,1792]{1,0:T(8,128)(2,1)S(1)} %bitcast.50, bf16[2048,1792]{1,0:T(8,128)(2,1)S(1)} %bitcast.56, ...), custom_call_target="tpu_custom_call" | custom-call | flops 4227858432 | bytes 22020096 | tf_op jit(solution)/shard_map/pallas_call | solution.py:117
  61.6 1.5 %collective-permute-start.21 = (bf16[24,2048]{1,0:T(8,128)(2,1)S(1)}, bf16[24,2048]{1,0:T(8,128)(2,1)S(1)}, u32[]{:S(2)}, u32[]{:S(2)}) collective-permute-start(bf16[24,2048]{1,0:T(8,128)(2,1)S(1)} %get-tuple-element.46), channel_id=1, source_target_pairs={{0,6},{2,4},{4,2},{6,0},{8,14},{10,12},{12,10},{14,8},{16,22},{18,... | collective-permute-start | bytes 294920 | tf_op jit(solution)/shard_map/ppermute | solution.py:193
  63.1 0.4 collective-permute-start.29
  63.5 1.6 %collective-permute-start.30 = (bf16[24,2048]{1,0:T(8,128)(2,1)S(1)}, bf16[24,2048]{1,0:T(8,128)(2,1)S(1)}, u32[]{:S(2)}, u32[]{:S(2)}) collective-permute-start(bf16[24,2048]{1,0:T(8,128)(2,1)S(1)} %get-tuple-element.55), channel_id=1, source_target_pairs={{0,4},{2,6},{4,0},{6,2},{8,12},{10,14},{12,8},{14,10},{16,20},{18,... | collective-permute-start | bytes 294920 | tf_op jit(solution)/shard_map/ppermute | solution.py:193
  65.2 1.5 %collective-permute-start.31 = (bf16[24,2048]{1,0:T(8,128)(2,1)S(1)}, bf16[24,2048]{1,0:T(8,128)(2,1)S(1)}, u32[]{:S(2)}, u32[]{:S(2)}) collective-permute-start(bf16[24,2048]{1,0:T(8,128)(2,1)S(1)} %get-tuple-element.54), channel_id=1, source_target_pairs={{0,6},{2,4},{4,2},{6,0},{8,14},{10,12},{12,10},{14,8},{16,22},{18,... | collective-permute-start | bytes 294920 | tf_op jit(solution)/shard_map/ppermute | solution.py:193
  66.7 1.2 collective-permute-done.21
  68.1 0.4 collective-permute-start.22
  68.5 0.4 collective-permute-done.30
  68.9 1.9 %collective-permute-done.31 = bf16[24,2048]{1,0:T(8,128)(2,1)S(1)} collective-permute-done((bf16[24,2048]{1,0:T(8,128)(2,1)S(1)}, bf16[24,2048]{1,0:T(8,128)(2,1)S(1)}, u32[]{:S(2)}, u32[]{:S(2)}) %collective-permute-start.31) | collective-permute-done | bytes 98336 | tf_op jit(solution)/shard_map/ppermute | solution.py:193
  70.9 4.8 %shard_map.119 = (bf16[96,2048]{1,0:T(8,128)(2,1)S(1)}, bf16[96,2048]{1,0:T(8,128)(2,1)S(1)}) custom-call(bf16[96,2048]{1,0:T(8,128)(2,1)S(1)} %pad_maximum_fusion.1.refs_0_, bf16[96,2048]{1,0:T(8,128)(2,1)S(1)} %collective-permute-done.12.refs_1_, bf16[2048,1792]{1,0:T(8,128)(2,1)S(1)} %bitcast.51, bf16[2048,1792]{1,0:T(8,128)(2,1)S(1)} %bitcast.57, ...), custom_call_target="tpu_custom_call" | custom-call | flops 4227858432 | bytes 22020096 | tf_op jit(solution)/shard_map/pallas_call | solution.py:117
  75.7 0.6 collective-permute-start.13
  76.3 4.6 %shard_map.120 = (bf16[96,2048]{1,0:T(8,128)(2,1)S(1)}, bf16[96,2048]{1,0:T(8,128)(2,1)S(1)}) custom-call(bf16[96,2048]{1,0:T(8,128)(2,1)S(1)} %pad_maximum_fusion.2.refs_0_, bf16[96,2048]{1,0:T(8,128)(2,1)S(1)} %collective-permute-done.22.refs_1_, bf16[2048,1792]{1,0:T(8,128)(2,1)S(1)} %bitcast.52, bf16[2048,1792]{1,0:T(8,128)(2,1)S(1)} %bitcast.58, ...), custom_call_target="tpu_custom_call" | custom-call | flops 4227858432 | bytes 22020096 | tf_op jit(solution)/shard_map/pallas_call | solution.py:117
  81.0 4.6 %shard_map.121 = (bf16[96,2048]{1,0:T(8,128)(2,1)S(1)}, bf16[96,2048]{1,0:T(8,128)(2,1)S(1)}) custom-call(bf16[96,2048]{1,0:T(8,128)(2,1)S(1)} %pad_maximum_fusion.3.refs_0_, bf16[96,2048]{1,0:T(8,128)(2,1)S(1)} %collective-permute-done.32.refs_1_, bf16[2048,1792]{1,0:T(8,128)(2,1)S(1)} %bitcast.53, bf16[2048,1792]{1,0:T(8,128)(2,1)S(1)} %bitcast.59, ...), custom_call_target="tpu_custom_call" | custom-call | flops 4227858432 | bytes 22020096 | tf_op jit(solution)/shard_map/pallas_call | solution.py:117
  85.6 0.6 collective-permute-start.33
  86.4 2.3 %collective-permute-start.14 = (bf16[96,2048]{1,0:T(8,128)(2,1)S(1)}, bf16[96,2048]{1,0:T(8,128)(2,1)S(1)}, u32[]{:S(2)}, u32[]{:S(2)}) collective-permute-start(bf16[96,2048]{1,0:T(8,128)(2,1)S(1)} %add_convert_fusion.3), channel_id=1, source_target_pairs={{0,8},{2,10},{4,12},{6,14},{8,0},{10,2},{12,4},{14,6},{16,24},{18,... | collective-permute-start | bytes 1179656 | tf_op jit(solution)/shard_map/ppermute | solution.py:193
  88.9 2.3 %collective-permute-start.34 = (bf16[24,2048]{1,0:T(8,128)(2,1)S(1)}, bf16[24,2048]{1,0:T(8,128)(2,1)S(1)}, u32[]{:S(2)}, u32[]{:S(2)}) collective-permute-start(bf16[24,2048]{1,0:T(8,128)(2,1)S(1)} %get-tuple-element.49), channel_id=1, source_target_pairs={{0,16},{2,18},{4,20},{6,22},{8,24},{10,26},{12,28},{14,30},{16,0},... | collective-permute-start | bytes 294920 | tf_op jit(solution)/shard_map/ppermute | solution.py:193
  91.1 0.8 collective-permute-start.35
  91.9 3.1 %collective-permute-start.36 = (bf16[24,2048]{1,0:T(8,128)(2,1)S(1)}, bf16[24,2048]{1,0:T(8,128)(2,1)S(1)}, u32[]{:S(2)}, u32[]{:S(2)}) collective-permute-start(bf16[24,2048]{1,0:T(8,128)(2,1)S(1)} %get-tuple-element.51), channel_id=1, source_target_pairs={{0,20},{2,22},{4,16},{6,18},{8,28},{10,30},{12,24},{14,26},{16,4},... | collective-permute-start | bytes 294920 | tf_op jit(solution)/shard_map/ppermute | solution.py:193
  95.0 1.6 %collective-permute-start.37 = (bf16[24,2048]{1,0:T(8,128)(2,1)S(1)}, bf16[24,2048]{1,0:T(8,128)(2,1)S(1)}, u32[]{:S(2)}, u32[]{:S(2)}) collective-permute-start(bf16[24,2048]{1,0:T(8,128)(2,1)S(1)} %get-tuple-element.50), channel_id=1, source_target_pairs={{0,22},{2,20},{4,18},{6,16},{8,30},{10,28},{12,26},{14,24},{16,6},... | collective-permute-start | bytes 294920 | tf_op jit(solution)/shard_map/ppermute | solution.py:193
  96.7 5.4 %collective-permute-done.34 = bf16[24,2048]{1,0:T(8,128)(2,1)S(1)} collective-permute-done((bf16[24,2048]{1,0:T(8,128)(2,1)S(1)}, bf16[24,2048]{1,0:T(8,128)(2,1)S(1)}, u32[]{:S(2)}, u32[]{:S(2)}) %collective-permute-start.34) | collective-permute-done | bytes 98336 | tf_op jit(solution)/shard_map/ppermute | solution.py:193
  102.3 1.9 %collective-permute-done.35 = bf16[24,2048]{1,0:T(8,128)(2,1)S(1)} collective-permute-done((bf16[24,2048]{1,0:T(8,128)(2,1)S(1)}, bf16[24,2048]{1,0:T(8,128)(2,1)S(1)}, u32[]{:S(2)}, u32[]{:S(2)}) %collective-permute-start.35) | collective-permute-done | bytes 98336 | tf_op jit(solution)/shard_map/ppermute | solution.py:193
  104.2 11.2 %collective-permute-done.36 = bf16[24,2048]{1,0:T(8,128)(2,1)S(1)} collective-permute-done((bf16[24,2048]{1,0:T(8,128)(2,1)S(1)}, bf16[24,2048]{1,0:T(8,128)(2,1)S(1)}, u32[]{:S(2)}, u32[]{:S(2)}) %collective-permute-start.36) | collective-permute-done | bytes 98336 | tf_op jit(solution)/shard_map/ppermute | solution.py:193
  115.4 2.1 %collective-permute-done.37 = bf16[24,2048]{1,0:T(8,128)(2,1)S(1)} collective-permute-done((bf16[24,2048]{1,0:T(8,128)(2,1)S(1)}, bf16[24,2048]{1,0:T(8,128)(2,1)S(1)}, u32[]{:S(2)}, u32[]{:S(2)}) %collective-permute-start.37) | collective-permute-done | bytes 98336 | tf_op jit(solution)/shard_map/ppermute | solution.py:193
  117.5 0.5 fusion.18
  118.1 1.5 %collective-permute-start.17 = (bf16[48,2048]{1,0:T(8,128)(2,1)S(1)}, bf16[48,2048]{1,0:T(8,128)(2,1)S(1)}, u32[]{:S(2)}, u32[]{:S(2)}) collective-permute-start(bf16[48,2048]{1,0:T(8,128)(2,1)S(1)} %pad_maximum_fusion.6), channel_id=1, source_target_pairs={{0,6},{2,4},{4,2},{6,0},{8,14},{10,12},{12,10},{14,8},{16,22},{18,... | collective-permute-start | bytes 589832 | tf_op jit(solution)/shard_map/ppermute | solution.py:193
  119.6 0.6 collective-permute-start.16
  120.3 5.8 %collective-permute-done.24 = bf16[96,2048]{1,0:T(8,128)(2,1)S(1)} collective-permute-done((bf16[96,2048]{1,0:T(8,128)(2,1)S(1)}, bf16[96,2048]{1,0:T(8,128)(2,1)S(1)}, u32[]{:S(2)}, u32[]{:S(2)}) %collective-permute-start.24) | collective-permute-done | bytes 393248 | tf_op jit(solution)/shard_map/ppermute | solution.py:193
  126.1 0.7 collective-permute-start.25
  126.8 1.4 %collective-permute-start.26 = (bf16[24,2048]{1,0:T(8,128)(2,1)S(1)}, bf16[24,2048]{1,0:T(8,128)(2,1)S(1)}, u32[]{:S(2)}, u32[]{:S(2)}) collective-permute-start(bf16[24,2048]{1,0:T(8,128)(2,1)S(1)} %get-tuple-element.43), channel_id=1, source_target_pairs={{0,4},{2,6},{4,0},{6,2},{8,12},{10,14},{12,8},{14,10},{16,20},{18,... | collective-permute-start | bytes 294920 | tf_op jit(solution)/shard_map/ppermute | solution.py:193
  128.2 1.4 %collective-permute-start.27 = (bf16[24,2048]{1,0:T(8,128)(2,1)S(1)}, bf16[24,2048]{1,0:T(8,128)(2,1)S(1)}, u32[]{:S(2)}, u32[]{:S(2)}) collective-permute-start(bf16[24,2048]{1,0:T(8,128)(2,1)S(1)} %get-tuple-element.42), channel_id=1, source_target_pairs={{0,6},{2,4},{4,2},{6,0},{8,14},{10,12},{12,10},{14,8},{16,22},{18,... | collective-permute-start | bytes 294920 | tf_op jit(solution)/shard_map/ppermute | solution.py:193
  129.7 1.9 %collective-permute-done.25 = bf16[24,2048]{1,0:T(8,128)(2,1)S(1)} collective-permute-done((bf16[24,2048]{1,0:T(8,128)(2,1)S(1)}, bf16[24,2048]{1,0:T(8,128)(2,1)S(1)}, u32[]{:S(2)}, u32[]{:S(2)}) %collective-permute-start.25) | collective-permute-done | bytes 98336 | tf_op jit(solution)/shard_map/ppermute | solution.py:193
  131.7 0.8 collective-permute-done.26
  132.5 2.3 %collective-permute-done.27 = bf16[24,2048]{1,0:T(8,128)(2,1)S(1)} collective-permute-done((bf16[24,2048]{1,0:T(8,128)(2,1)S(1)}, bf16[24,2048]{1,0:T(8,128)(2,1)S(1)}, u32[]{:S(2)}, u32[]{:S(2)}) %collective-permute-start.27) | collective-permute-done | bytes 98336 | tf_op jit(solution)/shard_map/ppermute | solution.py:193
  134.8 0.5 fusion.10
  135.3 2.0 %collective-permute-done.15 = bf16[48,2048]{1,0:T(8,128)(2,1)S(1)} collective-permute-done((bf16[48,2048]{1,0:T(8,128)(2,1)S(1)}, bf16[48,2048]{1,0:T(8,128)(2,1)S(1)}, u32[]{:S(2)}, u32[]{:S(2)}) %collective-permute-start.15) | collective-permute-done | bytes 196640 | tf_op jit(solution)/shard_map/ppermute | solution.py:193
  137.4 0.5 fusion.3
  137.9 1.2 reduce_sum.39
  139.2 2.1 %add_convert_fusion = bf16[128,2048]{1,0:T(8,128)(2,1)} fusion(f32[128,2048]{1,0:T(8,128)S(1)} %get-tuple-element.62, f32[128,2048]{1,0:T(8,128)} %reduce_sum.39), kind=kLoop, calls=%fused_computation.19 | loop fusion | flops 524288 | bytes 2621440 | tf_op jit(solution)/shard_map/convert_element_type | solution.py:233
  (106 shorter events, 4.6 us)
Async XLA Ops:
  1.4 7.2 %collective-permute-start = (bf16[128,128]{0,1:T(8,128)(2,1)S(1)}, bf16[128,128]{0,1:T(8,128)(2,1)S(1)}, u32[]{:S(2)}, u32[]{:S(2)}) collective-permute-start(bf16[128,128]{0,1:T(8,128)(2,1)S(1)} %pad_maximum_fusion.7), channel_id=1, source_target_pairs={{0,2},{2,4},{4,6},{6,8},{8,10},{10,12},{12,14},{14,16},{16,18},{18... | collective-permute-start | bytes 98312 | tf_op jit(solution)/shard_map/ppermute | solution.py:22
  4.8 8.5 %collective-permute-start.2 = (bf16[512,2048]{1,0:T(8,128)(2,1)}, bf16[512,2048]{1,0:T(8,128)(2,1)S(1)}, u32[]{:S(2)}, u32[]{:S(2)}) collective-permute-start(bf16[512,2048]{1,0:T(8,128)(2,1)} %param.16), channel_id=1, source_target_pairs={{0,1},{1,0},{2,3},{3,2},{4,5},{5,4},{6,7},{7,6},{8,9},{9,8},{10,11... | collective-permute-start | bytes 6291464 | tf_op jit(solution)/shard_map/ppermute | solution.py:26
  5.0 5.4 %copy-start.4 = (f32[8]{0:T(128)S(1)}, f32[8]{0:T(128)}, u32[]{:S(2)}) copy-start(f32[8]{0:T(128)} %param.15) | copy-start | bytes 100
  8.6 2.3 %copy-start.3 = (bf16[256,64]{0,1:T(8,128)(2,1)S(1)}, bf16[256,64]{0,1:T(8,128)(2,1)}, u32[]{:S(2)}) copy-start(bf16[256,64]{0,1:T(8,128)(2,1)} %param.14) | copy-start | bytes 98308
  8.6 48.2 %slice-start.4 = ((s8[7340032]{0:T(1024)(128)(4,1)}), s8[4194304]{0:T(1024)(128)(4,1)S(1)}, s32[]{:S(2)}) async-start(s8[7340032]{0:T(1024)(128)(4,1)} %bitcast.60), calls=%async_computation.4 | async-start | bytes 8388608
  11.0 1.6 %copy-start = (bf16[512,2048]{1,0:T(8,128)(2,1)S(1)}, bf16[512,2048]{1,0:T(8,128)(2,1)}, u32[]{:S(2)}) copy-start(bf16[512,2048]{1,0:T(8,128)(2,1)} %param.16) | copy-start | bytes 6291460
  11.0 1.7 %copy-start.1 = (bf16[128,2048]{1,0:T(8,128)(2,1)S(1)}, bf16[128,2048]{1,0:T(8,128)(2,1)}, u32[]{:S(2)}) copy-start(bf16[128,2048]{1,0:T(8,128)(2,1)} %param.17) | copy-start | bytes 1572868
  11.0 45.9 %slice-start.2 = ((s8[7340032]{0:T(1024)(128)(4,1)}), s8[4194304]{0:T(1024)(128)(4,1)S(1)}, s32[]{:S(2)}) async-start(s8[7340032]{0:T(1024)(128)(4,1)} %bitcast.54), calls=%async_computation.2 | async-start | bytes 8388608
  11.0 45.9 %slice-start.5 = ((s8[7340032]{0:T(1024)(128)(4,1)}), s8[3145728]{0:T(1024)(128)(4,1)S(1)}, s32[]{:S(2)}) async-start(s8[7340032]{0:T(1024)(128)(4,1)} %bitcast.60), calls=%async_computation.5 | async-start | bytes 6291456
  11.7 2.1 %copy-start.2 = (f32[2048]{0:T(1024)S(1)}, f32[2048]{0:T(1024)}, u32[]{:S(2)}) copy-start(f32[2048]{0:T(1024)} %param.18) | copy-start | bytes 24580
  11.7 45.1 %slice-start.3 = ((s8[7340032]{0:T(1024)(128)(4,1)}), s8[3145728]{0:T(1024)(128)(4,1)S(1)}, s32[]{:S(2)}) async-start(s8[7340032]{0:T(1024)(128)(4,1)} %bitcast.54), calls=%async_computation.3 | async-start | bytes 6291456
  11.8 1.5 %collective-permute-start.1 = (bf16[128,512]{0,1:T(8,128)(2,1)S(1)}, bf16[128,512]{0,1:T(8,128)(2,1)S(1)}, u32[]{:S(2)}, u32[]{:S(2)}) collective-permute-start(bf16[128,512]{0,1:T(8,128)(2,1)S(1)} %constant_dynamic-slice_fusion), channel_id=1, source_target_pairs={{0,1},{1,0},{2,3},{3,2},{4,5},{5,4},{6,7},{7,6},{8,9},{9,8},{10,11... | collective-permute-start | bytes 393224 | tf_op jit(solution)/shard_map/ppermute | solution.py:26
  13.3 43.6 %slice-start = ((s8[7340032]{0:T(1024)(128)(4,1)}), s8[4194304]{0:T(1024)(128)(4,1)S(1)}, s32[]{:S(2)}) async-start(s8[7340032]{0:T(1024)(128)(4,1)} %bitcast.48), calls=%async_computation | async-start | bytes 8388608
  14.0 42.9 %slice-start.1 = ((s8[7340032]{0:T(1024)(128)(4,1)}), s8[3145728]{0:T(1024)(128)(4,1)S(1)}, s32[]{:S(2)}) async-start(s8[7340032]{0:T(1024)(128)(4,1)} %bitcast.48), calls=%async_computation.1 | async-start | bytes 6291456
  14.3 7.6 %collective-permute-start.3 = (bf16[24,2048]{1,0:T(8,128)(2,1)S(1)}, bf16[24,2048]{1,0:T(8,128)(2,1)S(1)}, u32[]{:S(2)}, u32[]{:S(2)}) collective-permute-start(bf16[24,2048]{1,0:T(8,128)(2,1)S(1)} %get-tuple-element.40), channel_id=1, source_target_pairs={{0,2},{2,0},{4,6},{6,4},{8,10},{10,8},{12,14},{14,12},{16,18},{18,... | collective-permute-start | bytes 294920 | tf_op jit(solution)/shard_map/ppermute | solution.py:193
  15.9 7.4 %collective-permute-start.4 = (bf16[24,2048]{1,0:T(8,128)(2,1)S(1)}, bf16[24,2048]{1,0:T(8,128)(2,1)S(1)}, u32[]{:S(2)}, u32[]{:S(2)}) collective-permute-start(bf16[24,2048]{1,0:T(8,128)(2,1)S(1)} %get-tuple-element.39), channel_id=1, source_target_pairs={{0,4},{2,6},{4,0},{6,2},{8,12},{10,14},{12,8},{14,10},{16,20},{18,... | collective-permute-start | bytes 294920 | tf_op jit(solution)/shard_map/ppermute | solution.py:193
  16.4 6.9 %collective-permute-start.5 = (bf16[24,2048]{1,0:T(8,128)(2,1)S(1)}, bf16[24,2048]{1,0:T(8,128)(2,1)S(1)}, u32[]{:S(2)}, u32[]{:S(2)}) collective-permute-start(bf16[24,2048]{1,0:T(8,128)(2,1)S(1)} %get-tuple-element.38), channel_id=1, source_target_pairs={{0,6},{2,4},{4,2},{6,0},{8,14},{10,12},{12,10},{14,8},{16,22},{18,... | collective-permute-start | bytes 294920 | tf_op jit(solution)/shard_map/ppermute | solution.py:193
  18.2 12.1 %collective-permute-start.8 = (bf16[96,2048]{1,0:T(8,128)(2,1)S(1)}, bf16[96,2048]{1,0:T(8,128)(2,1)S(1)}, u32[]{:S(2)}, u32[]{:S(2)}) collective-permute-start(bf16[96,2048]{1,0:T(8,128)(2,1)S(1)} %convolution_convert_fusion.2), channel_id=1, source_target_pairs={{0,8},{2,10},{4,12},{6,14},{8,0},{10,2},{12,4},{14,6},{16,24},{18,... | collective-permute-start | bytes 1179656 | tf_op jit(solution)/shard_map/ppermute | solution.py:193
  19.0 29.6 %collective-permute-start.18 = (bf16[96,2048]{1,0:T(8,128)(2,1)S(1)}, bf16[96,2048]{1,0:T(8,128)(2,1)S(1)}, u32[]{:S(2)}, u32[]{:S(2)}) collective-permute-start(bf16[96,2048]{1,0:T(8,128)(2,1)S(1)} %convolution_convert_fusion.1), channel_id=1, source_target_pairs={{0,24},{2,26},{4,28},{6,30},{8,16},{10,18},{12,20},{14,22},{16,8},... | collective-permute-start | bytes 1179656 | tf_op jit(solution)/shard_map/ppermute | solution.py:193
  22.0 32.8 %collective-permute-start.28 = (bf16[96,2048]{1,0:T(8,128)(2,1)S(1)}, bf16[96,2048]{1,0:T(8,128)(2,1)S(1)}, u32[]{:S(2)}, u32[]{:S(2)}) collective-permute-start(bf16[96,2048]{1,0:T(8,128)(2,1)S(1)} %convolution_convert_fusion), channel_id=1, source_target_pairs={{0,16},{2,18},{4,20},{6,22},{8,24},{10,26},{12,28},{14,30},{16,0},... | collective-permute-start | bytes 1179656 | tf_op jit(solution)/shard_map/ppermute | solution.py:193
  23.3 31.8 %collective-permute-start.6 = (bf16[96,2048]{1,0:T(8,128)(2,1)S(1)}, bf16[96,2048]{1,0:T(8,128)(2,1)S(1)}, u32[]{:S(2)}, u32[]{:S(2)}) collective-permute-start(bf16[96,2048]{1,0:T(8,128)(2,1)S(1)} %pad_maximum_fusion.refs_0_), channel_id=1, source_target_pairs={{0,1},{1,0},{2,3},{3,2},{4,5},{5,4},{6,7},{7,6},{8,9},{9,8},{10,11... | collective-permute-start | bytes 1179656 | tf_op jit(solution)/shard_map/ppermute | solution.py:26
  30.3 31.3 %collective-permute-start.10 = (bf16[24,2048]{1,0:T(8,128)(2,1)S(1)}, bf16[24,2048]{1,0:T(8,128)(2,1)S(1)}, u32[]{:S(2)}, u32[]{:S(2)}) collective-permute-start(bf16[24,2048]{1,0:T(8,128)(2,1)S(1)} %get-tuple-element.35), channel_id=1, source_target_pairs={{0,4},{2,6},{4,0},{6,2},{8,12},{10,14},{12,8},{14,10},{16,20},{18,... | collective-permute-start | bytes 294920 | tf_op jit(solution)/shard_map/ppermute | solution.py:193
  31.1 32.0 %collective-permute-start.11 = (bf16[24,2048]{1,0:T(8,128)(2,1)S(1)}, bf16[24,2048]{1,0:T(8,128)(2,1)S(1)}, u32[]{:S(2)}, u32[]{:S(2)}) collective-permute-start(bf16[24,2048]{1,0:T(8,128)(2,1)S(1)} %get-tuple-element.34), channel_id=1, source_target_pairs={{0,6},{2,4},{4,2},{6,0},{8,14},{10,12},{12,10},{14,8},{16,22},{18,... | collective-permute-start | bytes 294920 | tf_op jit(solution)/shard_map/ppermute | solution.py:193
  48.5 15.0 %collective-permute-start.9 = (bf16[24,2048]{1,0:T(8,128)(2,1)S(1)}, bf16[24,2048]{1,0:T(8,128)(2,1)S(1)}, u32[]{:S(2)}, u32[]{:S(2)}) collective-permute-start(bf16[24,2048]{1,0:T(8,128)(2,1)S(1)} %get-tuple-element.36), channel_id=1, source_target_pairs={{0,2},{2,0},{4,6},{6,4},{8,10},{10,8},{12,14},{14,12},{16,18},{18,... | collective-permute-start | bytes 294920 | tf_op jit(solution)/shard_map/ppermute | solution.py:193
  54.8 10.4 %collective-permute-start.19 = (bf16[24,2048]{1,0:T(8,128)(2,1)S(1)}, bf16[24,2048]{1,0:T(8,128)(2,1)S(1)}, u32[]{:S(2)}, u32[]{:S(2)}) collective-permute-start(bf16[24,2048]{1,0:T(8,128)(2,1)S(1)} %get-tuple-element.48), channel_id=1, source_target_pairs={{0,2},{2,0},{4,6},{6,4},{8,10},{10,8},{12,14},{14,12},{16,18},{18,... | collective-permute-start | bytes 294920 | tf_op jit(solution)/shard_map/ppermute | solution.py:193
  55.2 11.6 %collective-permute-start.20 = (bf16[24,2048]{1,0:T(8,128)(2,1)S(1)}, bf16[24,2048]{1,0:T(8,128)(2,1)S(1)}, u32[]{:S(2)}, u32[]{:S(2)}) collective-permute-start(bf16[24,2048]{1,0:T(8,128)(2,1)S(1)} %get-tuple-element.47), channel_id=1, source_target_pairs={{0,4},{2,6},{4,0},{6,2},{8,12},{10,14},{12,8},{14,10},{16,20},{18,... | collective-permute-start | bytes 294920 | tf_op jit(solution)/shard_map/ppermute | solution.py:193
  61.6 6.3 %collective-permute-start.21 = (bf16[24,2048]{1,0:T(8,128)(2,1)S(1)}, bf16[24,2048]{1,0:T(8,128)(2,1)S(1)}, u32[]{:S(2)}, u32[]{:S(2)}) collective-permute-start(bf16[24,2048]{1,0:T(8,128)(2,1)S(1)} %get-tuple-element.46), channel_id=1, source_target_pairs={{0,6},{2,4},{4,2},{6,0},{8,14},{10,12},{12,10},{14,8},{16,22},{18,... | collective-permute-start | bytes 294920 | tf_op jit(solution)/shard_map/ppermute | solution.py:193
  63.1 5.0 %collective-permute-start.29 = (bf16[24,2048]{1,0:T(8,128)(2,1)S(1)}, bf16[24,2048]{1,0:T(8,128)(2,1)S(1)}, u32[]{:S(2)}, u32[]{:S(2)}) collective-permute-start(bf16[24,2048]{1,0:T(8,128)(2,1)S(1)} %get-tuple-element.56), channel_id=1, source_target_pairs={{0,2},{2,0},{4,6},{6,4},{8,10},{10,8},{12,14},{14,12},{16,18},{18,... | collective-permute-start | bytes 294920 | tf_op jit(solution)/shard_map/ppermute | solution.py:193
  63.5 5.4 %collective-permute-start.30 = (bf16[24,2048]{1,0:T(8,128)(2,1)S(1)}, bf16[24,2048]{1,0:T(8,128)(2,1)S(1)}, u32[]{:S(2)}, u32[]{:S(2)}) collective-permute-start(bf16[24,2048]{1,0:T(8,128)(2,1)S(1)} %get-tuple-element.55), channel_id=1, source_target_pairs={{0,4},{2,6},{4,0},{6,2},{8,12},{10,14},{12,8},{14,10},{16,20},{18,... | collective-permute-start | bytes 294920 | tf_op jit(solution)/shard_map/ppermute | solution.py:193
  65.2 5.6 %collective-permute-start.31 = (bf16[24,2048]{1,0:T(8,128)(2,1)S(1)}, bf16[24,2048]{1,0:T(8,128)(2,1)S(1)}, u32[]{:S(2)}, u32[]{:S(2)}) collective-permute-start(bf16[24,2048]{1,0:T(8,128)(2,1)S(1)} %get-tuple-element.54), channel_id=1, source_target_pairs={{0,6},{2,4},{4,2},{6,0},{8,14},{10,12},{12,10},{14,8},{16,22},{18,... | collective-permute-start | bytes 294920 | tf_op jit(solution)/shard_map/ppermute | solution.py:193
  66.7 19.4 %collective-permute-start.7 = (bf16[96,2048]{1,0:T(8,128)(2,1)S(1)}, bf16[96,2048]{1,0:T(8,128)(2,1)S(1)}, u32[]{:S(2)}, u32[]{:S(2)}) collective-permute-start(bf16[96,2048]{1,0:T(8,128)(2,1)S(1)} %get-tuple-element.14), channel_id=1, source_target_pairs={{0,1},{1,0},{2,3},{3,2},{4,5},{5,4},{6,7},{7,6},{8,9},{9,8},{10,11... | collective-permute-start | bytes 1179656 | tf_op jit(solution)/shard_map/ppermute | solution.py:26
  67.9 3.0 %collective-permute-start.12 = (bf16[96,2048]{1,0:T(8,128)(2,1)S(1)}, bf16[96,2048]{1,0:T(8,128)(2,1)S(1)}, u32[]{:S(2)}, u32[]{:S(2)}) collective-permute-start(bf16[96,2048]{1,0:T(8,128)(2,1)S(1)} %pad_maximum_fusion.1.refs_0_), channel_id=1, source_target_pairs={{0,1},{1,0},{2,3},{3,2},{4,5},{5,4},{6,7},{7,6},{8,9},{9,8},{10,11... | collective-permute-start | bytes 1179656 | tf_op jit(solution)/shard_map/ppermute | solution.py:26
  68.1 8.2 %collective-permute-start.22 = (bf16[96,2048]{1,0:T(8,128)(2,1)S(1)}, bf16[96,2048]{1,0:T(8,128)(2,1)S(1)}, u32[]{:S(2)}, u32[]{:S(2)}) collective-permute-start(bf16[96,2048]{1,0:T(8,128)(2,1)S(1)} %pad_maximum_fusion.2.refs_0_), channel_id=1, source_target_pairs={{0,1},{1,0},{2,3},{3,2},{4,5},{5,4},{6,7},{7,6},{8,9},{9,8},{10,11... | collective-permute-start | bytes 1179656 | tf_op jit(solution)/shard_map/ppermute | solution.py:26
  70.8 10.2 %collective-permute-start.32 = (bf16[96,2048]{1,0:T(8,128)(2,1)S(1)}, bf16[96,2048]{1,0:T(8,128)(2,1)S(1)}, u32[]{:S(2)}, u32[]{:S(2)}) collective-permute-start(bf16[96,2048]{1,0:T(8,128)(2,1)S(1)} %pad_maximum_fusion.3.refs_0_), channel_id=1, source_target_pairs={{0,1},{1,0},{2,3},{3,2},{4,5},{5,4},{6,7},{7,6},{8,9},{9,8},{10,11... | collective-permute-start | bytes 1179656 | tf_op jit(solution)/shard_map/ppermute | solution.py:26
  75.7 10.6 %collective-permute-start.13 = (bf16[96,2048]{1,0:T(8,128)(2,1)S(1)}, bf16[96,2048]{1,0:T(8,128)(2,1)S(1)}, u32[]{:S(2)}, u32[]{:S(2)}) collective-permute-start(bf16[96,2048]{1,0:T(8,128)(2,1)S(1)} %get-tuple-element.16), channel_id=1, source_target_pairs={{0,1},{1,0},{2,3},{3,2},{4,5},{5,4},{6,7},{7,6},{8,9},{9,8},{10,11... | collective-permute-start | bytes 1179656 | tf_op jit(solution)/shard_map/ppermute | solution.py:26
  80.9 14.1 %collective-permute-start.23 = (bf16[96,2048]{1,0:T(8,128)(2,1)S(1)}, bf16[96,2048]{1,0:T(8,128)(2,1)S(1)}, u32[]{:S(2)}, u32[]{:S(2)}) collective-permute-start(bf16[96,2048]{1,0:T(8,128)(2,1)S(1)} %get-tuple-element.18), channel_id=1, source_target_pairs={{0,1},{1,0},{2,3},{3,2},{4,5},{5,4},{6,7},{7,6},{8,9},{9,8},{10,11... | collective-permute-start | bytes 1179656 | tf_op jit(solution)/shard_map/ppermute | solution.py:26
  85.6 3.1 %collective-permute-start.33 = (bf16[96,2048]{1,0:T(8,128)(2,1)S(1)}, bf16[96,2048]{1,0:T(8,128)(2,1)S(1)}, u32[]{:S(2)}, u32[]{:S(2)}) collective-permute-start(bf16[96,2048]{1,0:T(8,128)(2,1)S(1)} %get-tuple-element.20), channel_id=1, source_target_pairs={{0,1},{1,0},{2,3},{3,2},{4,5},{5,4},{6,7},{7,6},{8,9},{9,8},{10,11... | collective-permute-start | bytes 1179656 | tf_op jit(solution)/shard_map/ppermute | solution.py:26
  86.4 31.6 %collective-permute-start.14 = (bf16[96,2048]{1,0:T(8,128)(2,1)S(1)}, bf16[96,2048]{1,0:T(8,128)(2,1)S(1)}, u32[]{:S(2)}, u32[]{:S(2)}) collective-permute-start(bf16[96,2048]{1,0:T(8,128)(2,1)S(1)} %add_convert_fusion.3), channel_id=1, source_target_pairs={{0,8},{2,10},{4,12},{6,14},{8,0},{10,2},{12,4},{14,6},{16,24},{18,... | collective-permute-start | bytes 1179656 | tf_op jit(solution)/shard_map/ppermute | solution.py:193
  88.9 13.2 %collective-permute-start.34 = (bf16[24,2048]{1,0:T(8,128)(2,1)S(1)}, bf16[24,2048]{1,0:T(8,128)(2,1)S(1)}, u32[]{:S(2)}, u32[]{:S(2)}) collective-permute-start(bf16[24,2048]{1,0:T(8,128)(2,1)S(1)} %get-tuple-element.49), channel_id=1, source_target_pairs={{0,16},{2,18},{4,20},{6,22},{8,24},{10,26},{12,28},{14,30},{16,0},... | collective-permute-start | bytes 294920 | tf_op jit(solution)/shard_map/ppermute | solution.py:193
  91.1 13.1 %collective-permute-start.35 = (bf16[24,2048]{1,0:T(8,128)(2,1)S(1)}, bf16[24,2048]{1,0:T(8,128)(2,1)S(1)}, u32[]{:S(2)}, u32[]{:S(2)}) collective-permute-start(bf16[24,2048]{1,0:T(8,128)(2,1)S(1)} %get-tuple-element.52), channel_id=1, source_target_pairs={{0,18},{2,16},{4,22},{6,20},{8,26},{10,24},{12,30},{14,28},{16,2},... | collective-permute-start | bytes 294920 | tf_op jit(solution)/shard_map/ppermute | solution.py:193
  91.9 23.5 %collective-permute-start.36 = (bf16[24,2048]{1,0:T(8,128)(2,1)S(1)}, bf16[24,2048]{1,0:T(8,128)(2,1)S(1)}, u32[]{:S(2)}, u32[]{:S(2)}) collective-permute-start(bf16[24,2048]{1,0:T(8,128)(2,1)S(1)} %get-tuple-element.51), channel_id=1, source_target_pairs={{0,20},{2,22},{4,16},{6,18},{8,28},{10,30},{12,24},{14,26},{16,4},... | collective-permute-start | bytes 294920 | tf_op jit(solution)/shard_map/ppermute | solution.py:193
  95.0 22.6 %collective-permute-start.37 = (bf16[24,2048]{1,0:T(8,128)(2,1)S(1)}, bf16[24,2048]{1,0:T(8,128)(2,1)S(1)}, u32[]{:S(2)}, u32[]{:S(2)}) collective-permute-start(bf16[24,2048]{1,0:T(8,128)(2,1)S(1)} %get-tuple-element.50), channel_id=1, source_target_pairs={{0,22},{2,20},{4,18},{6,16},{8,30},{10,28},{12,26},{14,24},{16,6},... | collective-permute-start | bytes 294920 | tf_op jit(solution)/shard_map/ppermute | solution.py:193
  102.1 24.0 %collective-permute-start.24 = (bf16[96,2048]{1,0:T(8,128)(2,1)S(1)}, bf16[96,2048]{1,0:T(8,128)(2,1)S(1)}, u32[]{:S(2)}, u32[]{:S(2)}) collective-permute-start(bf16[96,2048]{1,0:T(8,128)(2,1)S(1)} %add_convert_fusion.2), channel_id=1, source_target_pairs={{0,24},{2,26},{4,28},{6,30},{8,16},{10,18},{12,20},{14,22},{16,8},... | collective-permute-start | bytes 1179656 | tf_op jit(solution)/shard_map/ppermute | solution.py:193
  118.0 19.4 %copy-start.5 = (f32[128,2]{0,1:T(2,128)S(1)}, f32[128,2]{0,1:T(2,128)}, u32[]{:S(2)}) copy-start(f32[128,2]{0,1:T(2,128)} %param.20) | copy-start | bytes 3076
  118.1 19.3 %collective-permute-start.17 = (bf16[48,2048]{1,0:T(8,128)(2,1)S(1)}, bf16[48,2048]{1,0:T(8,128)(2,1)S(1)}, u32[]{:S(2)}, u32[]{:S(2)}) collective-permute-start(bf16[48,2048]{1,0:T(8,128)(2,1)S(1)} %pad_maximum_fusion.6), channel_id=1, source_target_pairs={{0,6},{2,4},{4,2},{6,0},{8,14},{10,12},{12,10},{14,8},{16,22},{18,... | collective-permute-start | bytes 589832 | tf_op jit(solution)/shard_map/ppermute | solution.py:193
  119.6 17.7 %collective-permute-start.16 = (bf16[48,2048]{1,0:T(8,128)(2,1)S(1)}, bf16[48,2048]{1,0:T(8,128)(2,1)S(1)}, u32[]{:S(2)}, u32[]{:S(2)}) collective-permute-start(bf16[48,2048]{1,0:T(8,128)(2,1)S(1)} %pad_maximum_fusion.5), channel_id=1, source_target_pairs={{0,4},{2,6},{4,0},{6,2},{8,12},{10,14},{12,8},{14,10},{16,20},{18,... | collective-permute-start | bytes 589832 | tf_op jit(solution)/shard_map/ppermute | solution.py:193
  126.1 5.5 %collective-permute-start.25 = (bf16[24,2048]{1,0:T(8,128)(2,1)S(1)}, bf16[24,2048]{1,0:T(8,128)(2,1)S(1)}, u32[]{:S(2)}, u32[]{:S(2)}) collective-permute-start(bf16[24,2048]{1,0:T(8,128)(2,1)S(1)} %get-tuple-element.44), channel_id=1, source_target_pairs={{0,2},{2,0},{4,6},{6,4},{8,10},{10,8},{12,14},{14,12},{16,18},{18,... | collective-permute-start | bytes 294920 | tf_op jit(solution)/shard_map/ppermute | solution.py:193
  126.8 5.7 %collective-permute-start.26 = (bf16[24,2048]{1,0:T(8,128)(2,1)S(1)}, bf16[24,2048]{1,0:T(8,128)(2,1)S(1)}, u32[]{:S(2)}, u32[]{:S(2)}) collective-permute-start(bf16[24,2048]{1,0:T(8,128)(2,1)S(1)} %get-tuple-element.43), channel_id=1, source_target_pairs={{0,4},{2,6},{4,0},{6,2},{8,12},{10,14},{12,8},{14,10},{16,20},{18,... | collective-permute-start | bytes 294920 | tf_op jit(solution)/shard_map/ppermute | solution.py:193
  128.2 6.6 %collective-permute-start.27 = (bf16[24,2048]{1,0:T(8,128)(2,1)S(1)}, bf16[24,2048]{1,0:T(8,128)(2,1)S(1)}, u32[]{:S(2)}, u32[]{:S(2)}) collective-permute-start(bf16[24,2048]{1,0:T(8,128)(2,1)S(1)} %get-tuple-element.42), channel_id=1, source_target_pairs={{0,6},{2,4},{4,2},{6,0},{8,14},{10,12},{12,10},{14,8},{16,22},{18,... | collective-permute-start | bytes 294920 | tf_op jit(solution)/shard_map/ppermute | solution.py:193
  131.6 5.7 %collective-permute-start.15 = (bf16[48,2048]{1,0:T(8,128)(2,1)S(1)}, bf16[48,2048]{1,0:T(8,128)(2,1)S(1)}, u32[]{:S(2)}, u32[]{:S(2)}) collective-permute-start(bf16[48,2048]{1,0:T(8,128)(2,1)S(1)} %pad_maximum_fusion.4), channel_id=1, source_target_pairs={{0,2},{2,0},{4,6},{6,4},{8,10},{10,8},{12,14},{14,12},{16,18},{18,... | collective-permute-start | bytes 589832 | tf_op jit(solution)/shard_map/ppermute | solution.py:193

commit v3 on v2

v3 whole, which is shorter than its diff:
```python
import functools

import jax
import jax.numpy as jnp
from jax import lax
from jax.experimental import pallas as pl
from jax.experimental.pallas import tpu as pltpu
from jax.sharding import PartitionSpec as P


QUERY_HEADS = 16
HEAD_SIZE = 64
TOP = 2
WINDOW_KEYS = 128
PLANES = 4


def from_behind(block, axis, distance):
    devices = range(lax.axis_size(axis))
    route = [(i - distance, i) for i in devices if i - distance in devices]
    return lax.ppermute(block, axis, route)


def swap_cores(block):
    return lax.ppermute(block, "tp", [(0, 1), (1, 0)])


INSIDE = pl.BlockSpec(memory_space=pltpu.VMEM)
OUTSIDE = pl.BlockSpec(memory_space=pltpu.HBM)


def fetch(sources, targets, semaphores):
    copies = [
        pltpu.make_async_copy(source, target, semaphores.at[k])
        for k, (source, target) in enumerate(zip(sources, targets))
    ]
    for copy in copies:
        copy.start()
    return copies


def prepare_body(*refs, capacity):
    sources, outs = refs[:4], refs[4:]
    tail_ref, slots_ref, keys_ref, values_ref, query_ref, routes_ref, semaphores = outs
    targets = (keys_ref, values_ref, routes_ref, query_ref)
    copies = fetch(sources, targets, semaphores)
    for copy in copies:
        copy.wait()
    width, length = keys_ref.shape
    tail_ref[:width, :] = keys_ref[:, length - WINDOW_KEYS :]
    tail_ref[width:, :] = values_ref[:, length - WINDOW_KEYS :]
    experts = lax.axis_size("sp")
    tokens = routes_ref.shape[1]
    numbers = lax.broadcasted_iota(jnp.int32, (experts, tokens), 0)
    named = numbers == routes_ref[0:1, :]
    for choice in range(1, TOP):
        named = named | (numbers == routes_ref[choice : choice + 1, :])
    earlier = lax.broadcasted_iota(jnp.int32, (tokens, tokens), 0) < lax.broadcasted_iota(
        jnp.int32, (tokens, tokens), 1
    )
    ahead = jnp.dot(
        jnp.where(named, 1.0, 0.0).astype(jnp.bfloat16),
        jnp.where(earlier, 1.0, 0.0).astype(jnp.bfloat16),
        preferred_element_type=jnp.float32,
    )
    for choice in range(TOP):
        chosen = routes_ref[choice : choice + 1, :]
        rank = jnp.sum(jnp.where(numbers == chosen, ahead, 0.0), axis=0, keepdims=True)
        relative = chosen ^ lax.axis_index("sp")
        slots_ref[choice : choice + 1, :] = relative * capacity + rank.astype(jnp.int32)


def prepare(keys, values, routes, queries, capacity):
    return pl.pallas_call(
        functools.partial(prepare_body, capacity=capacity),
        in_specs=[OUTSIDE] * 4,
        out_specs=[INSIDE] * 5,
        out_shape=[
            pltpu.VMEM((2 * keys.shape[0], WINDOW_KEYS), keys.dtype),
            pltpu.VMEM(routes.shape, jnp.int32),
            pltpu.VMEM(keys.shape, keys.dtype),
            pltpu.VMEM(values.shape, values.dtype),
            pltpu.VMEM(queries.shape, queries.dtype),
        ],
        scratch_shapes=[
            pltpu.VMEM(routes.shape, routes.dtype),
            pltpu.SemaphoreType.DMA((4,)),
        ],
        compiler_params=pltpu.CompilerParams(vmem_limit_bytes=8 * 2**20),
    )(keys, values, routes, queries)


def attend_block(block, query_ref, before_ref, keys_ref, values_ref, sinks_ref, store):
    width, length = keys_ref.shape
    own = length // lax.axis_size("tp")
    local_heads = query_ref.shape[1] // HEAD_SIZE
    local_kv = width // HEAD_SIZE
    span = own + WINDOW_KEYS
    queries = query_ref[block * own : (block + 1) * own, :]
    if before_ref is None:
        keys, values = keys_ref[:, length - span :], values_ref[:, length - span :]
    else:
        keys, values = [
            jnp.concatenate([before_ref[part * width : (part + 1) * width, :], ref[:, :own]], axis=1)
            for part, ref in enumerate((keys_ref, values_ref))
        ]
    shape = (own, span)
    place = lax.broadcasted_iota(jnp.int32, shape, 1)
    distance = lax.broadcasted_iota(jnp.int32, shape, 0) - place + WINDOW_KEYS
    first = jnp.where(block + lax.axis_index("sp") == 0, WINDOW_KEYS, 0)
    inside = (distance >= 0) & (distance < WINDOW_KEYS) & (place >= first)
    distance = distance.astype(jnp.float32)
    for head in range(local_heads):
        columns = slice(head * HEAD_SIZE, (head + 1) * HEAD_SIZE)
        kv = head * local_kv // local_heads
        rows = slice(kv * HEAD_SIZE, (kv + 1) * HEAD_SIZE)
        slope = jnp.float32(0.0)
        for core in range(lax.axis_size("tp")):
            own_slope = 2.0 ** (-8.0 * (core * local_heads + head + 1.0) / QUERY_HEADS)
            slope = jnp.where(lax.axis_index("tp") == core, jnp.float32(own_slope), slope)
        score = jnp.dot(queries[:, columns], keys[rows, :], preferred_element_type=jnp.float32)
        score = jnp.where(inside, score * HEAD_SIZE ** (-0.5) - slope * distance, -jnp.inf)
        sink = sinks_ref[head]
        peak = jnp.maximum(jnp.max(score, axis=1, keepdims=True), sink)
        weight = jnp.exp(score - peak)
        total = jnp.sum(weight, axis=1, keepdims=True) + jnp.exp(sink - peak)
        probs = (weight / total).astype(jnp.bfloat16)
        store(
            columns,
            lax.dot_general(
                probs,
                values[rows, :],
                (((1,), (1,)), ((), ())),
                preferred_element_type=jnp.float32,
            ).astype(jnp.bfloat16),
        )


def attend_inside_body(*refs):
    query_ref, keys_ref, values_ref, sinks_hbm = refs[:4]
    later, (out_ref, *kept), (sinks_ref, semaphores) = refs[4:8], refs[8:13], refs[13:]
    later = (*later[:-1], later[-1].at[0])
    first, *copies = fetch((sinks_hbm, *later), (sinks_ref, *kept), semaphores)
    first.wait()

    def store(columns, value):
        out_ref[:, columns] = value

    attend_block(1, query_ref, None, keys_ref, values_ref, sinks_ref, store)
    for copy in copies:
        copy.wait()


def attend_border_body(*refs):
    query_ref, before_ref, keys_ref, values_ref, sinks_hbm, inside_ref = refs[:6]
    theirs_ref, mine_ref, sinks_ref, semaphores = refs[6:]
    fetch((sinks_hbm,), (sinks_ref,), semaphores)[0].wait()
    low = lax.axis_index("tp") == 0

    def store(columns, value):
        other = inside_ref[:, columns]
        mine_ref[:, columns] = jnp.where(low, value, other)
        theirs_ref[:, columns] = jnp.where(low, other, value)

    attend_block(0, query_ref, before_ref, keys_ref, values_ref, sinks_ref, store)


def partial_body(rows_ref, weight_ref, residual_ref, sum_ref):
    sum_ref[...] = residual_ref[...].astype(jnp.float32) + jnp.dot(
        rows_ref[...], weight_ref[...], preferred_element_type=jnp.float32
    )


def attend_inside(queries, keys, values, sinks, later, own_rows):
    return pl.pallas_call(
        attend_inside_body,
        in_specs=[INSIDE] * 3 + [OUTSIDE] * 5,
        out_specs=[INSIDE] * 5,
        out_shape=[pltpu.VMEM((own_rows, queries.shape[1]), jnp.bfloat16)]
        + [pltpu.VMEM(x.shape[-2:], x.dtype) for x in later],
        scratch_shapes=[pltpu.SMEM(sinks.shape, sinks.dtype), pltpu.SemaphoreType.DMA((5,))],
        compiler_params=pltpu.CompilerParams(vmem_limit_bytes=16 * 2**20),
    )(queries, keys, values, sinks, *later)


def attend_border(queries, before, keys, values, sinks, inside):
    return pl.pallas_call(
        attend_border_body,
        in_specs=[INSIDE] * 4 + [OUTSIDE, INSIDE],
        out_specs=[INSIDE] * 2,
        out_shape=[jax.ShapeDtypeStruct(inside.shape, inside.dtype)] * 2,
        scratch_shapes=[pltpu.SMEM(sinks.shape, sinks.dtype), pltpu.SemaphoreType.DMA((1,))],
        compiler_params=pltpu.CompilerParams(vmem_limit_bytes=16 * 2**20),
    )(queries, before, keys, values, sinks, inside)


def partial_sum(rows, weight, residual):
    return pl.pallas_call(
        partial_body,
        in_specs=[INSIDE] * 3,
        out_specs=INSIDE,
        out_shape=jax.ShapeDtypeStruct(residual.shape, jnp.float32),
        compiler_params=pltpu.CompilerParams(vmem_limit_bytes=16 * 2**20),
    )(rows, weight, residual)


def project_body(sum_ref, rows_ref, weight_ref, gain_ref, slots_ref, mixed_ref, *out_refs):
    mixed = sum_ref[...] + jnp.dot(
        rows_ref[...], weight_ref[...], preferred_element_type=jnp.float32
    )
    mixed_ref[...] = mixed
    scale = lax.rsqrt(jnp.mean(mixed * mixed, axis=-1, keepdims=True) + 1e-05)
    normed = (mixed * scale * gain_ref[...]).astype(jnp.bfloat16)
    for number, out_ref in enumerate(out_refs):
        shape = (out_ref.shape[0], mixed.shape[0])
        numbers = number * shape[0] + lax.broadcasted_iota(jnp.int32, shape, 0)
        select = numbers == slots_ref[0:1, :]
        for choice in range(1, TOP):
            select = select | (numbers == slots_ref[choice : choice + 1, :])
        out_ref[...] = jnp.dot(
            jnp.where(select, 1.0, 0.0).astype(jnp.bfloat16),
            normed,
            preferred_element_type=jnp.float32,
        ).astype(jnp.bfloat16)


def project(total, rows, weight, gain, slots, group):
    picked = jax.ShapeDtypeStruct((group, total.shape[1]), jnp.bfloat16)
    return pl.pallas_call(
        project_body,
        in_specs=[INSIDE] * 5,
        out_specs=[INSIDE] * (1 + PLANES),
        out_shape=[jax.ShapeDtypeStruct(total.shape, jnp.float32)] + [picked] * PLANES,
        compiler_params=pltpu.CompilerParams(vmem_limit_bytes=16 * 2**20),
    )(total, rows, weight, gain, slots)


BLOCK = 256


def gather_rows(pieces, rows_ref):
    start = 0
    for piece in pieces:
        rows_ref[start : start + piece.shape[0], :] = piece[...]
        start += piece.shape[0]


def load_body(*refs):
    count = len(refs) // 2
    sources = [ref.at[0] for ref in refs[:count]]
    for copy in fetch(sources, refs[count : 2 * count], refs[-1]):
        copy.wait()


def load(*weights):
    return pl.pallas_call(
        load_body,
        in_specs=[OUTSIDE] * len(weights),
        out_specs=[INSIDE] * len(weights),
        out_shape=[pltpu.VMEM(w.shape[1:], w.dtype) for w in weights],
        scratch_shapes=[pltpu.SemaphoreType.DMA((len(weights),))],
        compiler_params=pltpu.CompilerParams(vmem_limit_bytes=4 * 2**20),
    )(*weights)


def expert_body(*refs, count):
    pieces, (gate_ref, up_ref, down_ref, own_ref, other_ref, rows_ref, hidden_ref) = (
        refs[:count],
        refs[count:],
    )
    gather_rows(pieces, rows_ref)
    for start in range(0, gate_ref.shape[1], BLOCK):
        units = slice(start, start + BLOCK)
        rows = rows_ref[...]
        gate = jnp.dot(rows, gate_ref[:, units], preferred_element_type=jnp.float32)
        upper = jnp.dot(rows, up_ref[:, units], preferred_element_type=jnp.float32)
        hidden_ref[:, units] = (gate / (1.0 + jnp.exp(-gate)) * upper).astype(jnp.bfloat16)
    half = own_ref.shape[0]
    for start in range(0, down_ref.shape[1], BLOCK):
        units = slice(start, start + BLOCK)
        part = jnp.dot(
            hidden_ref[...], down_ref[:, units], preferred_element_type=jnp.float32
        ).astype(jnp.bfloat16)
        own_ref[:, units] = part[:half]
        other_ref[:, units] = part[half:]


def expert_parts(pieces, weights):
    width, hidden_units = weights[0].shape
    if any(piece.shape[0] % 8 for piece in pieces):
        pieces = [jnp.concatenate(pieces, axis=0)]
    rows = sum(piece.shape[0] for piece in pieces)
    half = jax.ShapeDtypeStruct((rows // 2, width), jnp.bfloat16)
    inside = pl.BlockSpec(memory_space=pltpu.VMEM)
    return pl.pallas_call(
        functools.partial(expert_body, count=len(pieces)),
        in_specs=[inside] * (len(pieces) + 3),
        out_specs=[inside] * 2,
        out_shape=[half, half],
        scratch_shapes=[
            pltpu.VMEM((rows, width), jnp.bfloat16),
            pltpu.VMEM((rows, hidden_units), jnp.bfloat16),
        ],
        compiler_params=pltpu.CompilerParams(vmem_limit_bytes=8 * 2**20),
        cost_estimate=pl.CostEstimate(
            flops=6 * rows * width * hidden_units,
            transcendentals=rows * hidden_units,
            bytes_accessed=6 * width * hidden_units,
        ),
    )(*pieces, *weights)


def combine_body(*refs, count, base):
    sum_ref, slots_ref, weights_ref = refs[:3]
    pieces, (result_ref, rows_ref) = refs[3 : 3 + count], refs[3 + count :]
    gather_rows(pieces, rows_ref)
    shape = (rows_ref.shape[0], slots_ref.shape[1])
    numbers = base + lax.broadcasted_iota(jnp.int32, shape, 0)
    result = sum_ref[...]
    for choice in range(TOP):
        pick = slots_ref[choice : choice + 1, :] == numbers
        picked = lax.dot_general(
            jnp.where(pick, 1.0, 0.0).astype(jnp.bfloat16),
            rows_ref[...],
            (((0,), (0,)), ((), ())),
            preferred_element_type=jnp.float32,
        )
        result = result + weights_ref[:, choice : choice + 1] * picked
    result_ref[...] = result.astype(result_ref.dtype)


def combine(total, slots, weights, pieces, base, dtype):
    if any(piece.shape[0] % 8 for piece in pieces):
        pieces = [jnp.concatenate(pieces, axis=0)]
    rows = sum(piece.shape[0] for piece in pieces)
    inside = pl.BlockSpec(memory_space=pltpu.VMEM)
    return pl.pallas_call(
        functools.partial(combine_body, count=len(pieces), base=base),
        in_specs=[inside] * (3 + len(pieces)),
        out_specs=inside,
        out_shape=jax.ShapeDtypeStruct(total.shape, dtype),
        scratch_shapes=[pltpu.VMEM((rows, total.shape[1]), jnp.bfloat16)],
        compiler_params=pltpu.CompilerParams(vmem_limit_bytes=8 * 2**20),
        cost_estimate=pl.CostEstimate(
            flops=4 * rows * total.shape[0] * total.shape[1],
            transcendentals=0,
            bytes_accessed=8 * total.shape[0] * total.shape[1],
        ),
    )(total, slots, weights, *pieces)


def on_device(
    query_rows,
    key_rows,
    value_head_rows,
    sink_logit_head,
    out_weight,
    residual,
    norm_gain,
    routes,
    route_weights,
    gate_proj,
    up_proj,
    down_proj,
):
    n_sp = lax.axis_size("sp")
    own_rows = residual.shape[0]
    plane = n_sp // PLANES
    capacity = 3 * own_rows * TOP // (2 * n_sp)
    group = plane * capacity
    outside = [
        pltpu.with_memory_space_constraint(x, pltpu.HBM)
        for x in (
            key_rows.T,
            value_head_rows.T,
            routes.T,
            query_rows,
            sink_logit_head,
        )
    ]
    sinks = outside[4]
    tail, slot_index, keys, values, queries = prepare(*outside[:4], capacity)
    before = from_behind(tail, "sp", 1)
    other_weight = swap_cores(out_weight)
    later = [
        pltpu.with_memory_space_constraint(x, pltpu.HBM)
        for x in (out_weight, residual, norm_gain.reshape(1, -1), gate_proj)
    ]
    inside, own_weight, own_residual, gain, gate_kept = attend_inside(
        queries, keys, values, sinks, later, own_rows
    )
    theirs, mine = attend_border(queries, before, keys, values, sinks, inside)
    from_other = swap_cores(theirs)
    partial = partial_sum(mine, own_weight, own_residual)
    mixed, *selected = project(partial, from_other, other_weight, gain, slot_index, group)
    weights = load(
        *[
            pltpu.with_memory_space_constraint(w, pltpu.HBM)
            for w in (up_proj, down_proj)
        ]
    )
    weights = [pltpu.with_memory_space_constraint(w, pltpu.VMEM) for w in (gate_kept, *weights)]

    def across(block, distance):
        return lax.ppermute(block, "sp", [(i, i ^ distance) for i in range(n_sp)])

    def pieces(block):
        rows = block.shape[0] // plane
        return [block[rows * j : rows * (j + 1)] for j in range(plane)]

    def in_plane(parts):
        return [parts[0]] + [across(parts[j], j) for j in range(1, plane)]

    def expert(parts):
        rows = jnp.concatenate(parts, axis=0)
        other = swap_cores(rows)
        own_part, other_part = expert_parts([rows, other], weights)
        added = swap_cores(other_part)
        return (own_part.astype(jnp.float32) + added.astype(jnp.float32)).astype(jnp.bfloat16)

    arrived = {number: across(selected[number], number * plane) for number in (3, 1, 2)}
    arrived[0] = selected[0]
    out = {number: expert(in_plane(pieces(arrived[number]))) for number in (0, 3, 1, 2)}
    far_back = in_plane(pieces(across(out[3], 3 * plane)))
    zero_back = in_plane(pieces(out[0]))
    one_back = in_plane(pieces(across(out[1], plane)))
    mid_back = [across(p, 2 * plane + j) for j, p in enumerate(pieces(out[2]))]

    total = mixed
    backs = (("zero", 0, zero_back), ("far", 3, far_back), ("one", 1, one_back), ("mid", 2, mid_back))
    for name, number, back in backs:
        dtype = jnp.bfloat16 if name == "mid" else jnp.float32
        total = combine(total, slot_index, route_weights, back, number * group, dtype)
    return total


def solution(mesh):
    placed = (
        P("sp", "tp"),
        P("sp", "tp"),
        P("sp", "tp"),
        P("tp"),
        P("tp", None),
        P(("sp", "tp"), None),
        P(),
        P(("sp", "tp"), None),
        P(("sp", "tp"), None),
        P("sp", None, "tp"),
        P("sp", None, "tp"),
        P("sp", "tp", None),
    )

    return jax.shard_map(
        on_device, mesh=mesh, in_specs=placed, out_specs=P(("sp", "tp"), None), check_vma=False
    )
```

time: 143 us -> 137 us (0.958)
  the two profiles are of different devices: /device:TPU:12 before, /device:TPU:0 now
where the time goes in v3:
time: 137 us
  starting transfers between devices  51.3 us (37%)
  waiting for transfers between devices  49.8 us (36%)
  Pallas kernels  34.4 us (25%)
    ppermute x30, waiting for transfers between devices, across(): return lax.ppermute(block, 'sp', [(i, i ^ distance) for i in range(n_sp)])  49.2 us
    ppermute x30, starting transfers between devices, across(): return lax.ppermute(block, 'sp', [(i, i ^ distance) for i in range(n_sp)])  44.7 us
    pallas_call x4, Pallas kernels, expert_parts(): pl.pallas_call(functools.partial(expert_body, count=len(pieces)), in_spec...  18 us
    pallas_call x1, Pallas kernels, load(): pl.pallas_call(load_body, in_specs=[OUTSIDE] * len(weights), out_specs=[I...  5.19 us
    ppermute x1, starting transfers between devices, from_behind(): return lax.ppermute(block, axis, route)  4.38 us
    pallas_call x1, Pallas kernels, attend_inside(): pl.pallas_call(attend_inside_body, in_specs=[INSIDE] * 3 + [OUTSIDE] * 5,...  3.95 us
    pallas_call x4, Pallas kernels, combine(): pl.pallas_call(functools.partial(combine_body, count=len(pieces), base=ba...  2.75 us
  transfers between devices with their start and end apart: 41, of which 15 were waited for; matrix products, arithmetic and copies ran while one was open for 1% of the time, Pallas kernels for 23%

profile of v3, /device:TPU:0, one launch (start us, length us, event | category | flops | bytes accessed | tf_op | source)
XLA Modules:
  0.0 136.7 jit_solution(15288122159045732476)
XLA Ops:
  0.0 0.5 collective-permute-start.2
  0.5 1.2 shard_map.118
  1.7 4.4 %collective-permute-start = (bf16[128,128]{1,0:T(8,128)(2,1)S(1)}, bf16[128,128]{1,0:T(8,128)(2,1)S(1)}, u32[]{:S(2)}, u32[]{:S(2)}) collective-permute-start(bf16[128,128]{1,0:T(8,128)(2,1)S(1)} %get-tuple-element.33), channel_id=1, source_target_pairs={{0,2},{2,4},{4,6},{6,8},{8,10},{10,12},{12,14},{14,16},{16,18},{18... | collective-permute-start | bytes 98312 | tf_op jit(solution)/shard_map/ppermute | solution.py:21
  6.1 3.9 %shard_map.119 = (bf16[128,512]{1,0:T(8,128)(2,1)S(1)}, bf16[512,2048]{1,0:T(8,128)(2,1)S(1)}, bf16[128,2048]{1,0:T(8,128)(2,1)S(1)}, f32[1,2048]{1,0:T(1,128)S(1)}, bf16[2048,1792]{1,0:T(8,128)(2,1)S(1)}) custom-call(bf16[256,512]{1,0:T(8,128)(2,1)S(1)} %get-tuple-element.32.refs_0_, bf16[64,256]{1,0:T(8,128)(2,1)S(1)} %get-tuple-element.34.refs_1_.refs_2_, ...), custom_call_target="tpu_custom_call" | custom-call | tf_op jit(solution)/shard_map/pallas_call | solution.py:175
  10.0 1.8 %shard_map.120 = (bf16[128,512]{1,0:T(8,128)(2,1)S(1)}, bf16[128,512]{1,0:T(8,128)(2,1)S(1)}) custom-call(bf16[256,512]{1,0:T(8,128)(2,1)S(1)} %get-tuple-element.32.refs_0_, bf16[128,128]{1,0:T(8,128)(2,1)S(1)} %collective-permute-done.refs_1_, bf16[64,256]{1,0:T(8,128)(2,1)S(1)} %get-tuple-element.34.refs_1_.refs_2_, ...), custom_call_target="tpu_custom_call" | custom-call | tf_op jit(solution)/shard_map/pallas_call | solution.py:187
  11.9 0.3 collective-permute-start.1
  12.2 0.5 shard_map.121.sum_ref
  12.6 0.7 collective-permute-done.1.rows_ref
  13.3 1.1 shard_map.122
  14.4 2.9 %collective-permute-start.31 = (bf16[96,2048]{1,0:T(8,128)(2,1)S(1)}, bf16[96,2048]{1,0:T(8,128)(2,1)S(1)}, u32[]{:S(2)}, u32[]{:S(2)}) collective-permute-start(bf16[96,2048]{1,0:T(8,128)(2,1)S(1)} %get-tuple-element.56), channel_id=1, source_target_pairs={{0,16},{2,18},{4,20},{6,22},{8,24},{10,26},{12,28},{14,30},{16,0},... | collective-permute-start | bytes 1179656 | tf_op jit(solution)/shard_map/ppermute | solution.py:405
  17.4 1.3 collective-permute-start.3
  18.7 1.5 %collective-permute-start.4 = (bf16[24,2048]{1,0:T(8,128)(2,1)S(1)}, bf16[24,2048]{1,0:T(8,128)(2,1)S(1)}, u32[]{:S(2)}, u32[]{:S(2)}) collective-permute-start(bf16[24,2048]{1,0:T(8,128)(2,1)S(1)} %get-tuple-element.89), channel_id=1, source_target_pairs={{0,4},{2,6},{4,0},{6,2},{8,12},{10,14},{12,8},{14,10},{16,20},{18,... | collective-permute-start | bytes 294920 | tf_op jit(solution)/shard_map/ppermute | solution.py:405
  20.2 0.7 collective-permute-start.5
  20.9 5.2 %shard_map.123 = (bf16[2048,1792]{1,0:T(8,128)(2,1)S(1)}, bf16[1792,2048]{1,0:T(8,128)(2,1)S(1)}) custom-call(bf16[1,2048,1792]{2,1,0:T(8,128)(2,1)} %refs_0_.1, bf16[1,1792,2048]{2,1,0:T(8,128)(2,1)} %refs_1_.1), custom_call_target="tpu_custom_call" | custom-call | tf_op jit(solution)/shard_map/pallas_call | solution.py:256
  26.1 1.6 %collective-permute-start.21 = (bf16[96,2048]{1,0:T(8,128)(2,1)S(1)}, bf16[96,2048]{1,0:T(8,128)(2,1)S(1)}, u32[]{:S(2)}, u32[]{:S(2)}) collective-permute-start(bf16[96,2048]{1,0:T(8,128)(2,1)S(1)} %get-tuple-element.53), channel_id=1, source_target_pairs={{0,8},{2,10},{4,12},{6,14},{8,0},{10,2},{12,4},{14,6},{16,24},{18,... | collective-permute-start | bytes 1179656 | tf_op jit(solution)/shard_map/ppermute | solution.py:405
  27.9 8.9 %collective-permute-done.31 = bf16[96,2048]{1,0:T(8,128)(2,1)S(1)} collective-permute-done((bf16[96,2048]{1,0:T(8,128)(2,1)S(1)}, bf16[96,2048]{1,0:T(8,128)(2,1)S(1)}, u32[]{:S(2)}, u32[]{:S(2)}) %collective-permute-start.31) | collective-permute-done | bytes 393248 | tf_op jit(solution)/shard_map/ppermute | solution.py:405
  36.9 1.9 %collective-permute-start.32 = (bf16[24,2048]{1,0:T(8,128)(2,1)S(1)}, bf16[24,2048]{1,0:T(8,128)(2,1)S(1)}, u32[]{:S(2)}, u32[]{:S(2)}) collective-permute-start(bf16[24,2048]{1,0:T(8,128)(2,1)S(1)} %get-tuple-element.66), channel_id=1, source_target_pairs={{0,2},{2,0},{4,6},{6,4},{8,10},{10,8},{12,14},{14,12},{16,18},{18,... | collective-permute-start | bytes 294920 | tf_op jit(solution)/shard_map/ppermute | solution.py:405
  38.8 1.5 %collective-permute-start.33 = (bf16[24,2048]{1,0:T(8,128)(2,1)S(1)}, bf16[24,2048]{1,0:T(8,128)(2,1)S(1)}, u32[]{:S(2)}, u32[]{:S(2)}) collective-permute-start(bf16[24,2048]{1,0:T(8,128)(2,1)S(1)} %get-tuple-element.65), channel_id=1, source_target_pairs={{0,4},{2,6},{4,0},{6,2},{8,12},{10,14},{12,8},{14,10},{16,20},{18,... | collective-permute-start | bytes 294920 | tf_op jit(solution)/shard_map/ppermute | solution.py:405
  40.2 11.6 %collective-permute-done.21 = bf16[96,2048]{1,0:T(8,128)(2,1)S(1)} collective-permute-done((bf16[96,2048]{1,0:T(8,128)(2,1)S(1)}, bf16[96,2048]{1,0:T(8,128)(2,1)S(1)}, u32[]{:S(2)}, u32[]{:S(2)}) %collective-permute-start.21) | collective-permute-done | bytes 393248 | tf_op jit(solution)/shard_map/ppermute | solution.py:405
  51.8 2.4 %collective-permute-start.34 = (bf16[24,2048]{1,0:T(8,128)(2,1)S(1)}, bf16[24,2048]{1,0:T(8,128)(2,1)S(1)}, u32[]{:S(2)}, u32[]{:S(2)}) collective-permute-start(bf16[24,2048]{1,0:T(8,128)(2,1)S(1)} %get-tuple-element.64), channel_id=1, source_target_pairs={{0,6},{2,4},{4,2},{6,0},{8,14},{10,12},{12,10},{14,8},{16,22},{18,... | collective-permute-start | bytes 294920 | tf_op jit(solution)/shard_map/ppermute | solution.py:405
  54.2 0.6 collective-permute-start.22
  54.9 0.6 collective-permute-start.23
  55.5 2.4 %collective-permute-start.24 = (bf16[24,2048]{1,0:T(8,128)(2,1)S(1)}, bf16[24,2048]{1,0:T(8,128)(2,1)S(1)}, u32[]{:S(2)}, u32[]{:S(2)}) collective-permute-start(bf16[24,2048]{1,0:T(8,128)(2,1)S(1)} %get-tuple-element.72), channel_id=1, source_target_pairs={{0,6},{2,4},{4,2},{6,0},{8,14},{10,12},{12,10},{14,8},{16,22},{18,... | collective-permute-start | bytes 294920 | tf_op jit(solution)/shard_map/ppermute | solution.py:405
  57.9 0.4 collective-permute-done.34
  58.3 1.6 %collective-permute-start.12 = (bf16[24,2048]{1,0:T(8,128)(2,1)S(1)}, bf16[24,2048]{1,0:T(8,128)(2,1)S(1)}, u32[]{:S(2)}, u32[]{:S(2)}) collective-permute-start(bf16[24,2048]{1,0:T(8,128)(2,1)S(1)} %get-tuple-element.82), channel_id=1, source_target_pairs={{0,2},{2,0},{4,6},{6,4},{8,10},{10,8},{12,14},{14,12},{16,18},{18,... | collective-permute-start | bytes 294920 | tf_op jit(solution)/shard_map/ppermute | solution.py:405
  59.9 0.4 collective-permute-done.22
  60.3 1.1 collective-permute-start.13
  61.4 2.0 %collective-permute-start.14 = (bf16[24,2048]{1,0:T(8,128)(2,1)S(1)}, bf16[24,2048]{1,0:T(8,128)(2,1)S(1)}, u32[]{:S(2)}, u32[]{:S(2)}) collective-permute-start(bf16[24,2048]{1,0:T(8,128)(2,1)S(1)} %get-tuple-element.80), channel_id=1, source_target_pairs={{0,6},{2,4},{4,2},{6,0},{8,14},{10,12},{12,10},{14,8},{16,22},{18,... | collective-permute-start | bytes 294920 | tf_op jit(solution)/shard_map/ppermute | solution.py:405
  63.5 1.0 collective-permute-done.12
  64.5 0.8 collective-permute-done.13
  65.3 1.6 %collective-permute-done.14 = bf16[24,2048]{1,0:T(8,128)(2,1)S(1)} collective-permute-done((bf16[24,2048]{1,0:T(8,128)(2,1)S(1)}, bf16[24,2048]{1,0:T(8,128)(2,1)S(1)}, u32[]{:S(2)}, u32[]{:S(2)}) %collective-permute-start.14) | collective-permute-done | bytes 98336 | tf_op jit(solution)/shard_map/ppermute | solution.py:405
  67.1 4.4 %shard_map.124 = (bf16[96,2048]{1,0:T(8,128)(2,1)S(1)}, bf16[96,2048]{1,0:T(8,128)(2,1)S(1)}) custom-call(bf16[96,2048]{1,0:T(8,128)(2,1)S(1)} %pad_maximum_fusion.refs_0_, bf16[96,2048]{1,0:T(8,128)(2,1)S(1)} %collective-permute-done.6.refs_1_, bf16[2048,1792]{1,0:T(8,128)(2,1)S(1)} %get-tuple-element.45.refs_2_, ...), custom_call_target="tpu_custom_call" | custom-call | flops 4227858432 | bytes 22020096 | tf_op jit(solution)/shard_map/pallas_call | solution.py:295
  71.5 0.6 collective-permute-start.7
  72.1 4.4 %shard_map.130 = (bf16[96,2048]{1,0:T(8,128)(2,1)S(1)}, bf16[96,2048]{1,0:T(8,128)(2,1)S(1)}) custom-call(bf16[96,2048]{1,0:T(8,128)(2,1)S(1)} %pad_maximum_fusion.3.refs_0_, bf16[96,2048]{1,0:T(8,128)(2,1)S(1)} %collective-permute-done.35.refs_1_, bf16[2048,1792]{1,0:T(8,128)(2,1)S(1)} %get-tuple-element.45.refs_2_, ...), custom_call_target="tpu_custom_call" | custom-call | flops 4227858432 | bytes 22020096 | tf_op jit(solution)/shard_map/pallas_call | solution.py:295
  76.6 4.6 %shard_map.128 = (bf16[96,2048]{1,0:T(8,128)(2,1)S(1)}, bf16[96,2048]{1,0:T(8,128)(2,1)S(1)}) custom-call(bf16[96,2048]{1,0:T(8,128)(2,1)S(1)} %pad_maximum_fusion.2.refs_0_, bf16[96,2048]{1,0:T(8,128)(2,1)S(1)} %collective-permute-done.25.refs_1_, bf16[2048,1792]{1,0:T(8,128)(2,1)S(1)} %get-tuple-element.45.refs_2_, ...), custom_call_target="tpu_custom_call" | custom-call | flops 4227858432 | bytes 22020096 | tf_op jit(solution)/shard_map/pallas_call | solution.py:295
  81.3 0.6 collective-permute-start.26
  81.8 4.4 %shard_map.126 = (bf16[96,2048]{1,0:T(8,128)(2,1)S(1)}, bf16[96,2048]{1,0:T(8,128)(2,1)S(1)}) custom-call(bf16[96,2048]{1,0:T(8,128)(2,1)S(1)} %pad_maximum_fusion.1.refs_0_, bf16[96,2048]{1,0:T(8,128)(2,1)S(1)} %collective-permute-done.15.refs_1_, bf16[2048,1792]{1,0:T(8,128)(2,1)S(1)} %get-tuple-element.45.refs_2_, ...), custom_call_target="tpu_custom_call" | custom-call | flops 4227858432 | bytes 22020096 | tf_op jit(solution)/shard_map/pallas_call | solution.py:295
  86.4 0.1 add_convert_fusion.3
  86.5 2.1 %collective-permute-start.10 = (bf16[24,2048]{1,0:T(8,128)(2,1)S(1)}, bf16[24,2048]{1,0:T(8,128)(2,1)S(1)}, u32[]{:S(2)}, u32[]{:S(2)}) collective-permute-start(bf16[24,2048]{1,0:T(8,128)(2,1)S(1)} %get-tuple-element.83), channel_id=1, source_target_pairs={{0,6},{2,4},{4,2},{6,0},{8,14},{10,12},{12,10},{14,8},{16,22},{18,... | collective-permute-start | bytes 294920 | tf_op jit(solution)/shard_map/ppermute | solution.py:405
  88.6 0.4 collective-permute-start.8
  89.0 1.1 collective-permute-start.9
  90.4 3.0 %collective-permute-start.17 = (bf16[96,2048]{1,0:T(8,128)(2,1)S(1)}, bf16[96,2048]{1,0:T(8,128)(2,1)S(1)}, u32[]{:S(2)}, u32[]{:S(2)}) collective-permute-start(bf16[96,2048]{1,0:T(8,128)(2,1)S(1)} %add_convert_fusion.2), channel_id=1, source_target_pairs={{0,24},{2,26},{4,28},{6,30},{8,16},{10,18},{12,20},{14,22},{16,8},... | collective-permute-start | bytes 1179656 | tf_op jit(solution)/shard_map/ppermute | solution.py:405
  93.5 7.5 %collective-permute-done.27 = bf16[96,2048]{1,0:T(8,128)(2,1)S(1)} collective-permute-done((bf16[96,2048]{1,0:T(8,128)(2,1)S(1)}, bf16[96,2048]{1,0:T(8,128)(2,1)S(1)}, u32[]{:S(2)}, u32[]{:S(2)}) %collective-permute-start.27) | collective-permute-done | bytes 393248 | tf_op jit(solution)/shard_map/ppermute | solution.py:405
  101.0 2.5 %collective-permute-start.28 = (bf16[24,2048]{1,0:T(8,128)(2,1)S(1)}, bf16[24,2048]{1,0:T(8,128)(2,1)S(1)}, u32[]{:S(2)}, u32[]{:S(2)}) collective-permute-start(bf16[24,2048]{1,0:T(8,128)(2,1)S(1)} %get-tuple-element.69), channel_id=1, source_target_pairs={{0,2},{2,0},{4,6},{6,4},{8,10},{10,8},{12,14},{14,12},{16,18},{18,... | collective-permute-start | bytes 294920 | tf_op jit(solution)/shard_map/ppermute | solution.py:405
  103.5 7.1 %collective-permute-done.17 = bf16[96,2048]{1,0:T(8,128)(2,1)S(1)} collective-permute-done((bf16[96,2048]{1,0:T(8,128)(2,1)S(1)}, bf16[96,2048]{1,0:T(8,128)(2,1)S(1)}, u32[]{:S(2)}, u32[]{:S(2)}) %collective-permute-start.17) | collective-permute-done | bytes 393248 | tf_op jit(solution)/shard_map/ppermute | solution.py:405
  110.6 0.3 collective-permute-start.29
  111.0 1.5 %collective-permute-start.30 = (bf16[24,2048]{1,0:T(8,128)(2,1)S(1)}, bf16[24,2048]{1,0:T(8,128)(2,1)S(1)}, u32[]{:S(2)}, u32[]{:S(2)}) collective-permute-start(bf16[24,2048]{1,0:T(8,128)(2,1)S(1)} %get-tuple-element.67), channel_id=1, source_target_pairs={{0,6},{2,4},{4,2},{6,0},{8,14},{10,12},{12,10},{14,8},{16,22},{18,... | collective-permute-start | bytes 294920 | tf_op jit(solution)/shard_map/ppermute | solution.py:405
  112.5 1.7 %collective-permute-start.18 = (bf16[24,2048]{1,0:T(8,128)(2,1)S(1)}, bf16[24,2048]{1,0:T(8,128)(2,1)S(1)}, u32[]{:S(2)}, u32[]{:S(2)}) collective-permute-start(bf16[24,2048]{1,0:T(8,128)(2,1)S(1)} %get-tuple-element.77), channel_id=1, source_target_pairs={{0,2},{2,0},{4,6},{6,4},{8,10},{10,8},{12,14},{14,12},{16,18},{18,... | collective-permute-start | bytes 294920 | tf_op jit(solution)/shard_map/ppermute | solution.py:405
  114.2 0.3 collective-permute-start.19
  114.6 1.4 %collective-permute-start.20 = (bf16[24,2048]{1,0:T(8,128)(2,1)S(1)}, bf16[24,2048]{1,0:T(8,128)(2,1)S(1)}, u32[]{:S(2)}, u32[]{:S(2)}) collective-permute-start(bf16[24,2048]{1,0:T(8,128)(2,1)S(1)} %get-tuple-element.75), channel_id=1, source_target_pairs={{0,6},{2,4},{4,2},{6,0},{8,14},{10,12},{12,10},{14,8},{16,22},{18,... | collective-permute-start | bytes 294920 | tf_op jit(solution)/shard_map/ppermute | solution.py:405
  116.0 1.7 %collective-permute-done.29.refs_5_ = bf16[24,2048]{1,0:T(8,128)(2,1)S(1)} collective-permute-done((bf16[24,2048]{1,0:T(8,128)(2,1)S(1)}, bf16[24,2048]{1,0:T(8,128)(2,1)S(1)}, u32[]{:S(2)}, u32[]{:S(2)}) %collective-permute-start.29) | collective-permute-done | bytes 98336 | tf_op jit(solution)/shard_map/ppermute | solution.py:405
  117.7 2.5 %collective-permute-start.37 = (bf16[24,2048]{1,0:T(8,128)(2,1)S(1)}, bf16[24,2048]{1,0:T(8,128)(2,1)S(1)}, u32[]{:S(2)}, u32[]{:S(2)}) collective-permute-start(bf16[24,2048]{1,0:T(8,128)(2,1)S(1)} %get-tuple-element.62), channel_id=1, source_target_pairs={{0,16},{2,18},{4,20},{6,22},{8,24},{10,26},{12,28},{14,30},{16,0},... | collective-permute-start | bytes 294920 | tf_op jit(solution)/shard_map/ppermute | solution.py:405
  120.2 1.5 %collective-permute-start.38 = (bf16[24,2048]{1,0:T(8,128)(2,1)S(1)}, bf16[24,2048]{1,0:T(8,128)(2,1)S(1)}, u32[]{:S(2)}, u32[]{:S(2)}) collective-permute-start(bf16[24,2048]{1,0:T(8,128)(2,1)S(1)} %get-tuple-element.61), channel_id=1, source_target_pairs={{0,18},{2,16},{4,22},{6,20},{8,26},{10,24},{12,30},{14,28},{16,2},... | collective-permute-start | bytes 294920 | tf_op jit(solution)/shard_map/ppermute | solution.py:405
  121.7 1.1 collective-permute-start.39
  122.7 3.0 %collective-permute-start.40 = (bf16[24,2048]{1,0:T(8,128)(2,1)S(1)}, bf16[24,2048]{1,0:T(8,128)(2,1)S(1)}, u32[]{:S(2)}, u32[]{:S(2)}) collective-permute-start(bf16[24,2048]{1,0:T(8,128)(2,1)S(1)} %get-tuple-element.59), channel_id=1, source_target_pairs={{0,22},{2,20},{4,18},{6,16},{8,30},{10,28},{12,26},{14,24},{16,6},... | collective-permute-start | bytes 294920 | tf_op jit(solution)/shard_map/ppermute | solution.py:405
  125.7 0.1 copy.13.refs_2_
  125.8 0.5 shard_map.125.refs_0_
  126.3 0.5 shard_map.127.refs_0_
  126.8 0.5 shard_map.129.refs_0_
  127.3 1.7 %collective-permute-done.37.refs_3_ = bf16[24,2048]{1,0:T(8,128)(2,1)S(1)} collective-permute-done((bf16[24,2048]{1,0:T(8,128)(2,1)S(1)}, bf16[24,2048]{1,0:T(8,128)(2,1)S(1)}, u32[]{:S(2)}, u32[]{:S(2)}) %collective-permute-start.37) | collective-permute-done | bytes 98336 | tf_op jit(solution)/shard_map/ppermute | solution.py:405
  129.0 3.6 %collective-permute-done.38.refs_4_ = bf16[24,2048]{1,0:T(8,128)(2,1)S(1)} collective-permute-done((bf16[24,2048]{1,0:T(8,128)(2,1)S(1)}, bf16[24,2048]{1,0:T(8,128)(2,1)S(1)}, u32[]{:S(2)}, u32[]{:S(2)}) %collective-permute-start.38) | collective-permute-done | bytes 98336 | tf_op jit(solution)/shard_map/ppermute | solution.py:405
  132.6 2.3 %collective-permute-done.39.refs_5_ = bf16[24,2048]{1,0:T(8,128)(2,1)S(1)} collective-permute-done((bf16[24,2048]{1,0:T(8,128)(2,1)S(1)}, bf16[24,2048]{1,0:T(8,128)(2,1)S(1)}, u32[]{:S(2)}, u32[]{:S(2)}) %collective-permute-start.39) | collective-permute-done | bytes 98336 | tf_op jit(solution)/shard_map/ppermute | solution.py:405
  134.9 0.5 collective-permute-done.40.refs_6_
  135.4 1.3 shard_map.131
  (51 shorter events, 1.1 us)
Async XLA Ops:
  0.0 13.3 %collective-permute-start.2 = (bf16[512,2048]{1,0:T(8,128)(2,1)}, bf16[512,2048]{1,0:T(8,128)(2,1)S(1)}, u32[]{:S(2)}, u32[]{:S(2)}) collective-permute-start(bf16[512,2048]{1,0:T(8,128)(2,1)} %refs_4_.2), channel_id=1, source_target_pairs={{0,1},{1,0},{2,3},{3,2},{4,5},{5,4},{6,7},{7,6},{8,9},{9,8},{10,11... | collective-permute-start | bytes 6291464 | tf_op jit(solution)/shard_map/ppermute | solution.py:25
  1.7 8.3 %collective-permute-start = (bf16[128,128]{1,0:T(8,128)(2,1)S(1)}, bf16[128,128]{1,0:T(8,128)(2,1)S(1)}, u32[]{:S(2)}, u32[]{:S(2)}) collective-permute-start(bf16[128,128]{1,0:T(8,128)(2,1)S(1)} %get-tuple-element.33), channel_id=1, source_target_pairs={{0,2},{2,4},{4,6},{6,8},{8,10},{10,12},{12,14},{14,16},{16,18},{18... | collective-permute-start | bytes 98312 | tf_op jit(solution)/shard_map/ppermute | solution.py:21
  11.9 1.4 %collective-permute-start.1 = (bf16[128,512]{1,0:T(8,128)(2,1)S(1)}, bf16[128,512]{1,0:T(8,128)(2,1)S(1)}, u32[]{:S(2)}, u32[]{:S(2)}) collective-permute-start(bf16[128,512]{1,0:T(8,128)(2,1)S(1)} %get-tuple-element.40), channel_id=1, source_target_pairs={{0,1},{1,0},{2,3},{3,2},{4,5},{5,4},{6,7},{7,6},{8,9},{9,8},{10,11... | collective-permute-start | bytes 393224 | tf_op jit(solution)/shard_map/ppermute | solution.py:25
  14.4 22.4 %collective-permute-start.31 = (bf16[96,2048]{1,0:T(8,128)(2,1)S(1)}, bf16[96,2048]{1,0:T(8,128)(2,1)S(1)}, u32[]{:S(2)}, u32[]{:S(2)}) collective-permute-start(bf16[96,2048]{1,0:T(8,128)(2,1)S(1)} %get-tuple-element.56), channel_id=1, source_target_pairs={{0,16},{2,18},{4,20},{6,22},{8,24},{10,26},{12,28},{14,30},{16,0},... | collective-permute-start | bytes 1179656 | tf_op jit(solution)/shard_map/ppermute | solution.py:405
  17.4 10.4 %collective-permute-start.3 = (bf16[24,2048]{1,0:T(8,128)(2,1)S(1)}, bf16[24,2048]{1,0:T(8,128)(2,1)S(1)}, u32[]{:S(2)}, u32[]{:S(2)}) collective-permute-start(bf16[24,2048]{1,0:T(8,128)(2,1)S(1)} %get-tuple-element.90), channel_id=1, source_target_pairs={{0,2},{2,0},{4,6},{6,4},{8,10},{10,8},{12,14},{14,12},{16,18},{18,... | collective-permute-start | bytes 294920 | tf_op jit(solution)/shard_map/ppermute | solution.py:405
  18.7 9.1 %collective-permute-start.4 = (bf16[24,2048]{1,0:T(8,128)(2,1)S(1)}, bf16[24,2048]{1,0:T(8,128)(2,1)S(1)}, u32[]{:S(2)}, u32[]{:S(2)}) collective-permute-start(bf16[24,2048]{1,0:T(8,128)(2,1)S(1)} %get-tuple-element.89), channel_id=1, source_target_pairs={{0,4},{2,6},{4,0},{6,2},{8,12},{10,14},{12,8},{14,10},{16,20},{18,... | collective-permute-start | bytes 294920 | tf_op jit(solution)/shard_map/ppermute | solution.py:405
  20.2 7.6 %collective-permute-start.5 = (bf16[24,2048]{1,0:T(8,128)(2,1)S(1)}, bf16[24,2048]{1,0:T(8,128)(2,1)S(1)}, u32[]{:S(2)}, u32[]{:S(2)}) collective-permute-start(bf16[24,2048]{1,0:T(8,128)(2,1)S(1)} %get-tuple-element.88), channel_id=1, source_target_pairs={{0,6},{2,4},{4,2},{6,0},{8,14},{10,12},{12,10},{14,8},{16,22},{18,... | collective-permute-start | bytes 294920 | tf_op jit(solution)/shard_map/ppermute | solution.py:405
  26.1 25.7 %collective-permute-start.21 = (bf16[96,2048]{1,0:T(8,128)(2,1)S(1)}, bf16[96,2048]{1,0:T(8,128)(2,1)S(1)}, u32[]{:S(2)}, u32[]{:S(2)}) collective-permute-start(bf16[96,2048]{1,0:T(8,128)(2,1)S(1)} %get-tuple-element.53), channel_id=1, source_target_pairs={{0,8},{2,10},{4,12},{6,14},{8,0},{10,2},{12,4},{14,6},{16,24},{18,... | collective-permute-start | bytes 1179656 | tf_op jit(solution)/shard_map/ppermute | solution.py:405
  27.8 26.5 %collective-permute-start.11 = (bf16[96,2048]{1,0:T(8,128)(2,1)S(1)}, bf16[96,2048]{1,0:T(8,128)(2,1)S(1)}, u32[]{:S(2)}, u32[]{:S(2)}) collective-permute-start(bf16[96,2048]{1,0:T(8,128)(2,1)S(1)} %get-tuple-element.50), channel_id=1, source_target_pairs={{0,24},{2,26},{4,28},{6,30},{8,16},{10,18},{12,20},{14,22},{16,8},... | collective-permute-start | bytes 1179656 | tf_op jit(solution)/shard_map/ppermute | solution.py:405
  27.8 39.3 %collective-permute-start.6 = (bf16[96,2048]{1,0:T(8,128)(2,1)S(1)}, bf16[96,2048]{1,0:T(8,128)(2,1)S(1)}, u32[]{:S(2)}, u32[]{:S(2)}) collective-permute-start(bf16[96,2048]{1,0:T(8,128)(2,1)S(1)} %pad_maximum_fusion.refs_0_), channel_id=1, source_target_pairs={{0,1},{1,0},{2,3},{3,2},{4,5},{5,4},{6,7},{7,6},{8,9},{9,8},{10,11... | collective-permute-start | bytes 1179656 | tf_op jit(solution)/shard_map/ppermute | solution.py:25
  36.9 18.0 %collective-permute-start.32 = (bf16[24,2048]{1,0:T(8,128)(2,1)S(1)}, bf16[24,2048]{1,0:T(8,128)(2,1)S(1)}, u32[]{:S(2)}, u32[]{:S(2)}) collective-permute-start(bf16[24,2048]{1,0:T(8,128)(2,1)S(1)} %get-tuple-element.66), channel_id=1, source_target_pairs={{0,2},{2,0},{4,6},{6,4},{8,10},{10,8},{12,14},{14,12},{16,18},{18,... | collective-permute-start | bytes 294920 | tf_op jit(solution)/shard_map/ppermute | solution.py:405
  38.8 16.8 %collective-permute-start.33 = (bf16[24,2048]{1,0:T(8,128)(2,1)S(1)}, bf16[24,2048]{1,0:T(8,128)(2,1)S(1)}, u32[]{:S(2)}, u32[]{:S(2)}) collective-permute-start(bf16[24,2048]{1,0:T(8,128)(2,1)S(1)} %get-tuple-element.65), channel_id=1, source_target_pairs={{0,4},{2,6},{4,0},{6,2},{8,12},{10,14},{12,8},{14,10},{16,20},{18,... | collective-permute-start | bytes 294920 | tf_op jit(solution)/shard_map/ppermute | solution.py:405
  51.8 6.5 %collective-permute-start.34 = (bf16[24,2048]{1,0:T(8,128)(2,1)S(1)}, bf16[24,2048]{1,0:T(8,128)(2,1)S(1)}, u32[]{:S(2)}, u32[]{:S(2)}) collective-permute-start(bf16[24,2048]{1,0:T(8,128)(2,1)S(1)} %get-tuple-element.64), channel_id=1, source_target_pairs={{0,6},{2,4},{4,2},{6,0},{8,14},{10,12},{12,10},{14,8},{16,22},{18,... | collective-permute-start | bytes 294920 | tf_op jit(solution)/shard_map/ppermute | solution.py:405
  54.2 6.1 %collective-permute-start.22 = (bf16[24,2048]{1,0:T(8,128)(2,1)S(1)}, bf16[24,2048]{1,0:T(8,128)(2,1)S(1)}, u32[]{:S(2)}, u32[]{:S(2)}) collective-permute-start(bf16[24,2048]{1,0:T(8,128)(2,1)S(1)} %get-tuple-element.74), channel_id=1, source_target_pairs={{0,2},{2,0},{4,6},{6,4},{8,10},{10,8},{12,14},{14,12},{16,18},{18,... | collective-permute-start | bytes 294920 | tf_op jit(solution)/shard_map/ppermute | solution.py:405
  54.9 6.6 %collective-permute-start.23 = (bf16[24,2048]{1,0:T(8,128)(2,1)S(1)}, bf16[24,2048]{1,0:T(8,128)(2,1)S(1)}, u32[]{:S(2)}, u32[]{:S(2)}) collective-permute-start(bf16[24,2048]{1,0:T(8,128)(2,1)S(1)} %get-tuple-element.73), channel_id=1, source_target_pairs={{0,4},{2,6},{4,0},{6,2},{8,12},{10,14},{12,8},{14,10},{16,20},{18,... | collective-permute-start | bytes 294920 | tf_op jit(solution)/shard_map/ppermute | solution.py:405
  55.5 7.9 %collective-permute-start.24 = (bf16[24,2048]{1,0:T(8,128)(2,1)S(1)}, bf16[24,2048]{1,0:T(8,128)(2,1)S(1)}, u32[]{:S(2)}, u32[]{:S(2)}) collective-permute-start(bf16[24,2048]{1,0:T(8,128)(2,1)S(1)} %get-tuple-element.72), channel_id=1, source_target_pairs={{0,6},{2,4},{4,2},{6,0},{8,14},{10,12},{12,10},{14,8},{16,22},{18,... | collective-permute-start | bytes 294920 | tf_op jit(solution)/shard_map/ppermute | solution.py:405
  58.3 6.2 %collective-permute-start.12 = (bf16[24,2048]{1,0:T(8,128)(2,1)S(1)}, bf16[24,2048]{1,0:T(8,128)(2,1)S(1)}, u32[]{:S(2)}, u32[]{:S(2)}) collective-permute-start(bf16[24,2048]{1,0:T(8,128)(2,1)S(1)} %get-tuple-element.82), channel_id=1, source_target_pairs={{0,2},{2,0},{4,6},{6,4},{8,10},{10,8},{12,14},{14,12},{16,18},{18,... | collective-permute-start | bytes 294920 | tf_op jit(solution)/shard_map/ppermute | solution.py:405
  60.3 5.0 %collective-permute-start.13 = (bf16[24,2048]{1,0:T(8,128)(2,1)S(1)}, bf16[24,2048]{1,0:T(8,128)(2,1)S(1)}, u32[]{:S(2)}, u32[]{:S(2)}) collective-permute-start(bf16[24,2048]{1,0:T(8,128)(2,1)S(1)} %get-tuple-element.81), channel_id=1, source_target_pairs={{0,4},{2,6},{4,0},{6,2},{8,12},{10,14},{12,8},{14,10},{16,20},{18,... | collective-permute-start | bytes 294920 | tf_op jit(solution)/shard_map/ppermute | solution.py:405
  61.4 5.5 %collective-permute-start.14 = (bf16[24,2048]{1,0:T(8,128)(2,1)S(1)}, bf16[24,2048]{1,0:T(8,128)(2,1)S(1)}, u32[]{:S(2)}, u32[]{:S(2)}) collective-permute-start(bf16[24,2048]{1,0:T(8,128)(2,1)S(1)} %get-tuple-element.80), channel_id=1, source_target_pairs={{0,6},{2,4},{4,2},{6,0},{8,14},{10,12},{12,10},{14,8},{16,22},{18,... | collective-permute-start | bytes 294920 | tf_op jit(solution)/shard_map/ppermute | solution.py:405
  63.4 8.6 %collective-permute-start.35 = (bf16[96,2048]{1,0:T(8,128)(2,1)S(1)}, bf16[96,2048]{1,0:T(8,128)(2,1)S(1)}, u32[]{:S(2)}, u32[]{:S(2)}) collective-permute-start(bf16[96,2048]{1,0:T(8,128)(2,1)S(1)} %pad_maximum_fusion.3.refs_0_), channel_id=1, source_target_pairs={{0,1},{1,0},{2,3},{3,2},{4,5},{5,4},{6,7},{7,6},{8,9},{9,8},{10,11... | collective-permute-start | bytes 1179656 | tf_op jit(solution)/shard_map/ppermute | solution.py:25
  64.5 12.1 %collective-permute-start.25 = (bf16[96,2048]{1,0:T(8,128)(2,1)S(1)}, bf16[96,2048]{1,0:T(8,128)(2,1)S(1)}, u32[]{:S(2)}, u32[]{:S(2)}) collective-permute-start(bf16[96,2048]{1,0:T(8,128)(2,1)S(1)} %pad_maximum_fusion.2.refs_0_), channel_id=1, source_target_pairs={{0,1},{1,0},{2,3},{3,2},{4,5},{5,4},{6,7},{7,6},{8,9},{9,8},{10,11... | collective-permute-start | bytes 1179656 | tf_op jit(solution)/shard_map/ppermute | solution.py:25
  67.0 14.8 %collective-permute-start.15 = (bf16[96,2048]{1,0:T(8,128)(2,1)S(1)}, bf16[96,2048]{1,0:T(8,128)(2,1)S(1)}, u32[]{:S(2)}, u32[]{:S(2)}) collective-permute-start(bf16[96,2048]{1,0:T(8,128)(2,1)S(1)} %pad_maximum_fusion.1.refs_0_), channel_id=1, source_target_pairs={{0,1},{1,0},{2,3},{3,2},{4,5},{5,4},{6,7},{7,6},{8,9},{9,8},{10,11... | collective-permute-start | bytes 1179656 | tf_op jit(solution)/shard_map/ppermute | solution.py:25
  71.5 14.9 %collective-permute-start.7 = (bf16[96,2048]{1,0:T(8,128)(2,1)S(1)}, bf16[96,2048]{1,0:T(8,128)(2,1)S(1)}, u32[]{:S(2)}, u32[]{:S(2)}) collective-permute-start(bf16[96,2048]{1,0:T(8,128)(2,1)S(1)} %get-tuple-element.49), channel_id=1, source_target_pairs={{0,1},{1,0},{2,3},{3,2},{4,5},{5,4},{6,7},{7,6},{8,9},{9,8},{10,11... | collective-permute-start | bytes 1179656 | tf_op jit(solution)/shard_map/ppermute | solution.py:25
  76.5 13.9 %collective-permute-start.36 = (bf16[96,2048]{1,0:T(8,128)(2,1)S(1)}, bf16[96,2048]{1,0:T(8,128)(2,1)S(1)}, u32[]{:S(2)}, u32[]{:S(2)}) collective-permute-start(bf16[96,2048]{1,0:T(8,128)(2,1)S(1)} %get-tuple-element.58), channel_id=1, source_target_pairs={{0,1},{1,0},{2,3},{3,2},{4,5},{5,4},{6,7},{7,6},{8,9},{9,8},{10,11... | collective-permute-start | bytes 1179656 | tf_op jit(solution)/shard_map/ppermute | solution.py:25
  81.3 7.7 %collective-permute-start.26 = (bf16[96,2048]{1,0:T(8,128)(2,1)S(1)}, bf16[96,2048]{1,0:T(8,128)(2,1)S(1)}, u32[]{:S(2)}, u32[]{:S(2)}) collective-permute-start(bf16[96,2048]{1,0:T(8,128)(2,1)S(1)} %get-tuple-element.55), channel_id=1, source_target_pairs={{0,1},{1,0},{2,3},{3,2},{4,5},{5,4},{6,7},{7,6},{8,9},{9,8},{10,11... | collective-permute-start | bytes 1179656 | tf_op jit(solution)/shard_map/ppermute | solution.py:25
  86.3 39.4 %copy-start = (f32[128,2]{0,1:T(2,128)S(1)}, f32[128,2]{0,1:T(2,128)}, u32[]{:S(2)}) copy-start(f32[128,2]{0,1:T(2,128)} %param.20) | copy-start | bytes 3076
  86.3 3.9 %collective-permute-start.16 = (bf16[96,2048]{1,0:T(8,128)(2,1)S(1)}, bf16[96,2048]{1,0:T(8,128)(2,1)S(1)}, u32[]{:S(2)}, u32[]{:S(2)}) collective-permute-start(bf16[96,2048]{1,0:T(8,128)(2,1)S(1)} %get-tuple-element.52), channel_id=1, source_target_pairs={{0,1},{1,0},{2,3},{3,2},{4,5},{5,4},{6,7},{7,6},{8,9},{9,8},{10,11... | collective-permute-start | bytes 1179656 | tf_op jit(solution)/shard_map/ppermute | solution.py:25
  86.5 24.5 %collective-permute-start.10 = (bf16[24,2048]{1,0:T(8,128)(2,1)S(1)}, bf16[24,2048]{1,0:T(8,128)(2,1)S(1)}, u32[]{:S(2)}, u32[]{:S(2)}) collective-permute-start(bf16[24,2048]{1,0:T(8,128)(2,1)S(1)} %get-tuple-element.83), channel_id=1, source_target_pairs={{0,6},{2,4},{4,2},{6,0},{8,14},{10,12},{12,10},{14,8},{16,22},{18,... | collective-permute-start | bytes 294920 | tf_op jit(solution)/shard_map/ppermute | solution.py:405
  88.6 23.9 %collective-permute-start.8 = (bf16[24,2048]{1,0:T(8,128)(2,1)S(1)}, bf16[24,2048]{1,0:T(8,128)(2,1)S(1)}, u32[]{:S(2)}, u32[]{:S(2)}) collective-permute-start(bf16[24,2048]{1,0:T(8,128)(2,1)S(1)} %get-tuple-element.85), channel_id=1, source_target_pairs={{0,2},{2,0},{4,6},{6,4},{8,10},{10,8},{12,14},{14,12},{16,18},{18,... | collective-permute-start | bytes 294920 | tf_op jit(solution)/shard_map/ppermute | solution.py:405
  89.0 25.3 %collective-permute-start.9 = (bf16[24,2048]{1,0:T(8,128)(2,1)S(1)}, bf16[24,2048]{1,0:T(8,128)(2,1)S(1)}, u32[]{:S(2)}, u32[]{:S(2)}) collective-permute-start(bf16[24,2048]{1,0:T(8,128)(2,1)S(1)} %get-tuple-element.84), channel_id=1, source_target_pairs={{0,4},{2,6},{4,0},{6,2},{8,12},{10,14},{12,8},{14,10},{16,20},{18,... | collective-permute-start | bytes 294920 | tf_op jit(solution)/shard_map/ppermute | solution.py:405
  90.2 10.7 %collective-permute-start.27 = (bf16[96,2048]{1,0:T(8,128)(2,1)S(1)}, bf16[96,2048]{1,0:T(8,128)(2,1)S(1)}, u32[]{:S(2)}, u32[]{:S(2)}) collective-permute-start(bf16[96,2048]{1,0:T(8,128)(2,1)S(1)} %add_convert_fusion.1), channel_id=1, source_target_pairs={{0,8},{2,10},{4,12},{6,14},{8,0},{10,2},{12,4},{14,6},{16,24},{18,... | collective-permute-start | bytes 1179656 | tf_op jit(solution)/shard_map/ppermute | solution.py:405
  90.4 20.2 %collective-permute-start.17 = (bf16[96,2048]{1,0:T(8,128)(2,1)S(1)}, bf16[96,2048]{1,0:T(8,128)(2,1)S(1)}, u32[]{:S(2)}, u32[]{:S(2)}) collective-permute-start(bf16[96,2048]{1,0:T(8,128)(2,1)S(1)} %add_convert_fusion.2), channel_id=1, source_target_pairs={{0,24},{2,26},{4,28},{6,30},{8,16},{10,18},{12,20},{14,22},{16,8},... | collective-permute-start | bytes 1179656 | tf_op jit(solution)/shard_map/ppermute | solution.py:405
  101.0 13.6 %collective-permute-start.28 = (bf16[24,2048]{1,0:T(8,128)(2,1)S(1)}, bf16[24,2048]{1,0:T(8,128)(2,1)S(1)}, u32[]{:S(2)}, u32[]{:S(2)}) collective-permute-start(bf16[24,2048]{1,0:T(8,128)(2,1)S(1)} %get-tuple-element.69), channel_id=1, source_target_pairs={{0,2},{2,0},{4,6},{6,4},{8,10},{10,8},{12,14},{14,12},{16,18},{18,... | collective-permute-start | bytes 294920 | tf_op jit(solution)/shard_map/ppermute | solution.py:405
  110.6 7.1 %collective-permute-start.29 = (bf16[24,2048]{1,0:T(8,128)(2,1)S(1)}, bf16[24,2048]{1,0:T(8,128)(2,1)S(1)}, u32[]{:S(2)}, u32[]{:S(2)}) collective-permute-start(bf16[24,2048]{1,0:T(8,128)(2,1)S(1)} %get-tuple-element.68), channel_id=1, source_target_pairs={{0,4},{2,6},{4,0},{6,2},{8,12},{10,14},{12,8},{14,10},{16,20},{18,... | collective-permute-start | bytes 294920 | tf_op jit(solution)/shard_map/ppermute | solution.py:405
  111.0 15.8 %collective-permute-start.30 = (bf16[24,2048]{1,0:T(8,128)(2,1)S(1)}, bf16[24,2048]{1,0:T(8,128)(2,1)S(1)}, u32[]{:S(2)}, u32[]{:S(2)}) collective-permute-start(bf16[24,2048]{1,0:T(8,128)(2,1)S(1)} %get-tuple-element.67), channel_id=1, source_target_pairs={{0,6},{2,4},{4,2},{6,0},{8,14},{10,12},{12,10},{14,8},{16,22},{18,... | collective-permute-start | bytes 294920 | tf_op jit(solution)/shard_map/ppermute | solution.py:405
  112.5 7.7 %collective-permute-start.18 = (bf16[24,2048]{1,0:T(8,128)(2,1)S(1)}, bf16[24,2048]{1,0:T(8,128)(2,1)S(1)}, u32[]{:S(2)}, u32[]{:S(2)}) collective-permute-start(bf16[24,2048]{1,0:T(8,128)(2,1)S(1)} %get-tuple-element.77), channel_id=1, source_target_pairs={{0,2},{2,0},{4,6},{6,4},{8,10},{10,8},{12,14},{14,12},{16,18},{18,... | collective-permute-start | bytes 294920 | tf_op jit(solution)/shard_map/ppermute | solution.py:405
  114.2 7.4 %collective-permute-start.19 = (bf16[24,2048]{1,0:T(8,128)(2,1)S(1)}, bf16[24,2048]{1,0:T(8,128)(2,1)S(1)}, u32[]{:S(2)}, u32[]{:S(2)}) collective-permute-start(bf16[24,2048]{1,0:T(8,128)(2,1)S(1)} %get-tuple-element.76), channel_id=1, source_target_pairs={{0,4},{2,6},{4,0},{6,2},{8,12},{10,14},{12,8},{14,10},{16,20},{18,... | collective-permute-start | bytes 294920 | tf_op jit(solution)/shard_map/ppermute | solution.py:405
  114.6 8.2 %collective-permute-start.20 = (bf16[24,2048]{1,0:T(8,128)(2,1)S(1)}, bf16[24,2048]{1,0:T(8,128)(2,1)S(1)}, u32[]{:S(2)}, u32[]{:S(2)}) collective-permute-start(bf16[24,2048]{1,0:T(8,128)(2,1)S(1)} %get-tuple-element.75), channel_id=1, source_target_pairs={{0,6},{2,4},{4,2},{6,0},{8,14},{10,12},{12,10},{14,8},{16,22},{18,... | collective-permute-start | bytes 294920 | tf_op jit(solution)/shard_map/ppermute | solution.py:405
  117.7 11.3 %collective-permute-start.37 = (bf16[24,2048]{1,0:T(8,128)(2,1)S(1)}, bf16[24,2048]{1,0:T(8,128)(2,1)S(1)}, u32[]{:S(2)}, u32[]{:S(2)}) collective-permute-start(bf16[24,2048]{1,0:T(8,128)(2,1)S(1)} %get-tuple-element.62), channel_id=1, source_target_pairs={{0,16},{2,18},{4,20},{6,22},{8,24},{10,26},{12,28},{14,30},{16,0},... | collective-permute-start | bytes 294920 | tf_op jit(solution)/shard_map/ppermute | solution.py:405
  120.2 12.4 %collective-permute-start.38 = (bf16[24,2048]{1,0:T(8,128)(2,1)S(1)}, bf16[24,2048]{1,0:T(8,128)(2,1)S(1)}, u32[]{:S(2)}, u32[]{:S(2)}) collective-permute-start(bf16[24,2048]{1,0:T(8,128)(2,1)S(1)} %get-tuple-element.61), channel_id=1, source_target_pairs={{0,18},{2,16},{4,22},{6,20},{8,26},{10,24},{12,30},{14,28},{16,2},... | collective-permute-start | bytes 294920 | tf_op jit(solution)/shard_map/ppermute | solution.py:405
  121.7 13.2 %collective-permute-start.39 = (bf16[24,2048]{1,0:T(8,128)(2,1)S(1)}, bf16[24,2048]{1,0:T(8,128)(2,1)S(1)}, u32[]{:S(2)}, u32[]{:S(2)}) collective-permute-start(bf16[24,2048]{1,0:T(8,128)(2,1)S(1)} %get-tuple-element.60), channel_id=1, source_target_pairs={{0,20},{2,22},{4,16},{6,18},{8,28},{10,30},{12,24},{14,26},{16,4},... | collective-permute-start | bytes 294920 | tf_op jit(solution)/shard_map/ppermute | solution.py:405
  122.7 12.7 %collective-permute-start.40 = (bf16[24,2048]{1,0:T(8,128)(2,1)S(1)}, bf16[24,2048]{1,0:T(8,128)(2,1)S(1)}, u32[]{:S(2)}, u32[]{:S(2)}) collective-permute-start(bf16[24,2048]{1,0:T(8,128)(2,1)S(1)} %get-tuple-element.59), channel_id=1, source_target_pairs={{0,22},{2,20},{4,18},{6,16},{8,30},{10,28},{12,26},{14,24},{16,6},... | collective-permute-start | bytes 294920 | tf_op jit(solution)/shard_map/ppermute | solution.py:405

commit v4 on v3

--- a/solution.py
+++ b/solution.py
@@ -317,7 +317,13 @@
     shape = (rows_ref.shape[0], slots_ref.shape[1])
     numbers = base + lax.broadcasted_iota(jnp.int32, shape, 0)
     result = sum_ref[...]
+    tokens = slots_ref.shape[1]
+    diagonal = lax.broadcasted_iota(jnp.int32, (tokens, tokens), 0) == lax.broadcasted_iota(
+        jnp.int32, (tokens, tokens), 1
+    )
     for choice in range(TOP):
+        spread = jnp.where(diagonal, weights_ref[choice : choice + 1, :], 0.0)
+        weight = jnp.sum(spread, axis=1, keepdims=True)
         pick = slots_ref[choice : choice + 1, :] == numbers
         picked = lax.dot_general(
             jnp.where(pick, 1.0, 0.0).astype(jnp.bfloat16),
@@ -325,7 +331,7 @@
             (((0,), (0,)), ((), ())),
             preferred_element_type=jnp.float32,
         )
-        result = result + weights_ref[:, choice : choice + 1] * picked
+        result = result + weight * picked
     result_ref[...] = result.astype(result_ref.dtype)
 
 
@@ -430,7 +436,7 @@
     backs = (("zero", 0, zero_back), ("far", 3, far_back), ("one", 1, one_back), ("mid", 2, mid_back))
     for name, number, back in backs:
         dtype = jnp.bfloat16 if name == "mid" else jnp.float32
-        total = combine(total, slot_index, route_weights, back, number * group, dtype)
+        total = combine(total, slot_index, route_weights.T, back, number * group, dtype)
     return total
 
 

time: 137 us -> 137 us (level)
  no operation moved by 1% of the time
where the time goes in v4:
time: 137 us
  starting transfers between devices  51.3 us (37%)
  waiting for transfers between devices  49.9 us (36%)
  Pallas kernels  34.5 us (25%)
    ppermute x30, waiting for transfers between devices, across(): return lax.ppermute(block, 'sp', [(i, i ^ distance) for i in range(n_sp)])  49.2 us
    ppermute x30, starting transfers between devices, across(): return lax.ppermute(block, 'sp', [(i, i ^ distance) for i in range(n_sp)])  44.7 us
    pallas_call x4, Pallas kernels, expert_parts(): pl.pallas_call(functools.partial(expert_body, count=len(pieces)), in_spec...  18 us
    pallas_call x1, Pallas kernels, load(): pl.pallas_call(load_body, in_specs=[OUTSIDE] * len(weights), out_specs=[I...  5.19 us
    ppermute x1, starting transfers between devices, from_behind(): return lax.ppermute(block, axis, route)  4.38 us
    pallas_call x1, Pallas kernels, attend_inside(): pl.pallas_call(attend_inside_body, in_specs=[INSIDE] * 3 + [OUTSIDE] * 5,...  3.95 us
    pallas_call x4, Pallas kernels, combine(): pl.pallas_call(functools.partial(combine_body, count=len(pieces), base=ba...  2.77 us
  transfers between devices with their start and end apart: 41, of which 15 were waited for; matrix products, arithmetic and copies ran while one was open for 1% of the time, Pallas kernels for 23%

profile of v4, /device:TPU:0, one launch (start us, length us, event | category | flops | bytes accessed | tf_op | source)
XLA Modules:
  0.0 136.7 jit_solution(14068489996703093884)
XLA Ops:
  0.0 0.5 collective-permute-start.2
  0.5 1.2 shard_map.118
  1.7 4.4 %collective-permute-start = (bf16[128,128]{1,0:T(8,128)(2,1)S(1)}, bf16[128,128]{1,0:T(8,128)(2,1)S(1)}, u32[]{:S(2)}, u32[]{:S(2)}) collective-permute-start(bf16[128,128]{1,0:T(8,128)(2,1)S(1)} %get-tuple-element.33), channel_id=1, source_target_pairs={{0,2},{2,4},{4,6},{6,8},{8,10},{10,12},{12,14},{14,16},{16,18},{18... | collective-permute-start | bytes 98312 | tf_op jit(solution)/shard_map/ppermute | solution.py:21
  6.1 3.9 %shard_map.119 = (bf16[128,512]{1,0:T(8,128)(2,1)S(1)}, bf16[512,2048]{1,0:T(8,128)(2,1)S(1)}, bf16[128,2048]{1,0:T(8,128)(2,1)S(1)}, f32[1,2048]{1,0:T(1,128)S(1)}, bf16[2048,1792]{1,0:T(8,128)(2,1)S(1)}) custom-call(bf16[256,512]{1,0:T(8,128)(2,1)S(1)} %get-tuple-element.32.refs_0_, bf16[64,256]{1,0:T(8,128)(2,1)S(1)} %get-tuple-element.34.refs_1_.refs_2_, ...), custom_call_target="tpu_custom_call" | custom-call | tf_op jit(solution)/shard_map/pallas_call | solution.py:175
  10.0 1.8 %shard_map.120 = (bf16[128,512]{1,0:T(8,128)(2,1)S(1)}, bf16[128,512]{1,0:T(8,128)(2,1)S(1)}) custom-call(bf16[256,512]{1,0:T(8,128)(2,1)S(1)} %get-tuple-element.32.refs_0_, bf16[128,128]{1,0:T(8,128)(2,1)S(1)} %collective-permute-done.refs_1_, bf16[64,256]{1,0:T(8,128)(2,1)S(1)} %get-tuple-element.34.refs_1_.refs_2_, ...), custom_call_target="tpu_custom_call" | custom-call | tf_op jit(solution)/shard_map/pallas_call | solution.py:187
  11.9 0.3 collective-permute-start.1
  12.2 0.5 shard_map.121.sum_ref
  12.6 0.7 collective-permute-done.1.rows_ref
  13.3 1.1 shard_map.122
  14.4 2.9 %collective-permute-start.31 = (bf16[96,2048]{1,0:T(8,128)(2,1)S(1)}, bf16[96,2048]{1,0:T(8,128)(2,1)S(1)}, u32[]{:S(2)}, u32[]{:S(2)}) collective-permute-start(bf16[96,2048]{1,0:T(8,128)(2,1)S(1)} %get-tuple-element.56), channel_id=1, source_target_pairs={{0,16},{2,18},{4,20},{6,22},{8,24},{10,26},{12,28},{14,30},{16,0},... | collective-permute-start | bytes 1179656 | tf_op jit(solution)/shard_map/ppermute | solution.py:411
  17.3 1.3 collective-permute-start.3
  18.7 1.5 %collective-permute-start.4 = (bf16[24,2048]{1,0:T(8,128)(2,1)S(1)}, bf16[24,2048]{1,0:T(8,128)(2,1)S(1)}, u32[]{:S(2)}, u32[]{:S(2)}) collective-permute-start(bf16[24,2048]{1,0:T(8,128)(2,1)S(1)} %get-tuple-element.89), channel_id=1, source_target_pairs={{0,4},{2,6},{4,0},{6,2},{8,12},{10,14},{12,8},{14,10},{16,20},{18,... | collective-permute-start | bytes 294920 | tf_op jit(solution)/shard_map/ppermute | solution.py:411
  20.2 0.7 collective-permute-start.5
  20.9 5.2 %shard_map.123 = (bf16[2048,1792]{1,0:T(8,128)(2,1)S(1)}, bf16[1792,2048]{1,0:T(8,128)(2,1)S(1)}) custom-call(bf16[1,2048,1792]{2,1,0:T(8,128)(2,1)} %refs_0_.1, bf16[1,1792,2048]{2,1,0:T(8,128)(2,1)} %refs_1_.1), custom_call_target="tpu_custom_call" | custom-call | tf_op jit(solution)/shard_map/pallas_call | solution.py:256
  26.1 1.7 %collective-permute-start.21 = (bf16[96,2048]{1,0:T(8,128)(2,1)S(1)}, bf16[96,2048]{1,0:T(8,128)(2,1)S(1)}, u32[]{:S(2)}, u32[]{:S(2)}) collective-permute-start(bf16[96,2048]{1,0:T(8,128)(2,1)S(1)} %get-tuple-element.53), channel_id=1, source_target_pairs={{0,8},{2,10},{4,12},{6,14},{8,0},{10,2},{12,4},{14,6},{16,24},{18,... | collective-permute-start | bytes 1179656 | tf_op jit(solution)/shard_map/ppermute | solution.py:411
  27.9 9.0 %collective-permute-done.31 = bf16[96,2048]{1,0:T(8,128)(2,1)S(1)} collective-permute-done((bf16[96,2048]{1,0:T(8,128)(2,1)S(1)}, bf16[96,2048]{1,0:T(8,128)(2,1)S(1)}, u32[]{:S(2)}, u32[]{:S(2)}) %collective-permute-start.31) | collective-permute-done | bytes 393248 | tf_op jit(solution)/shard_map/ppermute | solution.py:411
  36.9 1.9 %collective-permute-start.32 = (bf16[24,2048]{1,0:T(8,128)(2,1)S(1)}, bf16[24,2048]{1,0:T(8,128)(2,1)S(1)}, u32[]{:S(2)}, u32[]{:S(2)}) collective-permute-start(bf16[24,2048]{1,0:T(8,128)(2,1)S(1)} %get-tuple-element.66), channel_id=1, source_target_pairs={{0,2},{2,0},{4,6},{6,4},{8,10},{10,8},{12,14},{14,12},{16,18},{18,... | collective-permute-start | bytes 294920 | tf_op jit(solution)/shard_map/ppermute | solution.py:411
  38.7 1.5 %collective-permute-start.33 = (bf16[24,2048]{1,0:T(8,128)(2,1)S(1)}, bf16[24,2048]{1,0:T(8,128)(2,1)S(1)}, u32[]{:S(2)}, u32[]{:S(2)}) collective-permute-start(bf16[24,2048]{1,0:T(8,128)(2,1)S(1)} %get-tuple-element.65), channel_id=1, source_target_pairs={{0,4},{2,6},{4,0},{6,2},{8,12},{10,14},{12,8},{14,10},{16,20},{18,... | collective-permute-start | bytes 294920 | tf_op jit(solution)/shard_map/ppermute | solution.py:411
  40.2 11.6 %collective-permute-done.21 = bf16[96,2048]{1,0:T(8,128)(2,1)S(1)} collective-permute-done((bf16[96,2048]{1,0:T(8,128)(2,1)S(1)}, bf16[96,2048]{1,0:T(8,128)(2,1)S(1)}, u32[]{:S(2)}, u32[]{:S(2)}) %collective-permute-start.21) | collective-permute-done | bytes 393248 | tf_op jit(solution)/shard_map/ppermute | solution.py:411
  51.8 2.4 %collective-permute-start.34 = (bf16[24,2048]{1,0:T(8,128)(2,1)S(1)}, bf16[24,2048]{1,0:T(8,128)(2,1)S(1)}, u32[]{:S(2)}, u32[]{:S(2)}) collective-permute-start(bf16[24,2048]{1,0:T(8,128)(2,1)S(1)} %get-tuple-element.64), channel_id=1, source_target_pairs={{0,6},{2,4},{4,2},{6,0},{8,14},{10,12},{12,10},{14,8},{16,22},{18,... | collective-permute-start | bytes 294920 | tf_op jit(solution)/shard_map/ppermute | solution.py:411
  54.2 0.6 collective-permute-start.22
  54.9 0.6 collective-permute-start.23
  55.5 2.4 %collective-permute-start.24 = (bf16[24,2048]{1,0:T(8,128)(2,1)S(1)}, bf16[24,2048]{1,0:T(8,128)(2,1)S(1)}, u32[]{:S(2)}, u32[]{:S(2)}) collective-permute-start(bf16[24,2048]{1,0:T(8,128)(2,1)S(1)} %get-tuple-element.72), channel_id=1, source_target_pairs={{0,6},{2,4},{4,2},{6,0},{8,14},{10,12},{12,10},{14,8},{16,22},{18,... | collective-permute-start | bytes 294920 | tf_op jit(solution)/shard_map/ppermute | solution.py:411
  57.9 0.4 collective-permute-done.34
  58.3 1.6 %collective-permute-start.12 = (bf16[24,2048]{1,0:T(8,128)(2,1)S(1)}, bf16[24,2048]{1,0:T(8,128)(2,1)S(1)}, u32[]{:S(2)}, u32[]{:S(2)}) collective-permute-start(bf16[24,2048]{1,0:T(8,128)(2,1)S(1)} %get-tuple-element.82), channel_id=1, source_target_pairs={{0,2},{2,0},{4,6},{6,4},{8,10},{10,8},{12,14},{14,12},{16,18},{18,... | collective-permute-start | bytes 294920 | tf_op jit(solution)/shard_map/ppermute | solution.py:411
  59.9 0.4 collective-permute-done.22
  60.3 1.1 collective-permute-start.13
  61.4 2.0 %collective-permute-start.14 = (bf16[24,2048]{1,0:T(8,128)(2,1)S(1)}, bf16[24,2048]{1,0:T(8,128)(2,1)S(1)}, u32[]{:S(2)}, u32[]{:S(2)}) collective-permute-start(bf16[24,2048]{1,0:T(8,128)(2,1)S(1)} %get-tuple-element.80), channel_id=1, source_target_pairs={{0,6},{2,4},{4,2},{6,0},{8,14},{10,12},{12,10},{14,8},{16,22},{18,... | collective-permute-start | bytes 294920 | tf_op jit(solution)/shard_map/ppermute | solution.py:411
  63.5 1.0 collective-permute-done.12
  64.5 0.8 collective-permute-done.13
  65.3 1.7 %collective-permute-done.14 = bf16[24,2048]{1,0:T(8,128)(2,1)S(1)} collective-permute-done((bf16[24,2048]{1,0:T(8,128)(2,1)S(1)}, bf16[24,2048]{1,0:T(8,128)(2,1)S(1)}, u32[]{:S(2)}, u32[]{:S(2)}) %collective-permute-start.14) | collective-permute-done | bytes 98336 | tf_op jit(solution)/shard_map/ppermute | solution.py:411
  67.1 4.4 %shard_map.124 = (bf16[96,2048]{1,0:T(8,128)(2,1)S(1)}, bf16[96,2048]{1,0:T(8,128)(2,1)S(1)}) custom-call(bf16[96,2048]{1,0:T(8,128)(2,1)S(1)} %pad_maximum_fusion.refs_0_, bf16[96,2048]{1,0:T(8,128)(2,1)S(1)} %collective-permute-done.6.refs_1_, bf16[2048,1792]{1,0:T(8,128)(2,1)S(1)} %get-tuple-element.45.refs_2_, ...), custom_call_target="tpu_custom_call" | custom-call | flops 4227858432 | bytes 22020096 | tf_op jit(solution)/shard_map/pallas_call | solution.py:295
  71.5 0.6 collective-permute-start.7
  72.1 4.4 %shard_map.130 = (bf16[96,2048]{1,0:T(8,128)(2,1)S(1)}, bf16[96,2048]{1,0:T(8,128)(2,1)S(1)}) custom-call(bf16[96,2048]{1,0:T(8,128)(2,1)S(1)} %pad_maximum_fusion.3.refs_0_, bf16[96,2048]{1,0:T(8,128)(2,1)S(1)} %collective-permute-done.35.refs_1_, bf16[2048,1792]{1,0:T(8,128)(2,1)S(1)} %get-tuple-element.45.refs_2_, ...), custom_call_target="tpu_custom_call" | custom-call | flops 4227858432 | bytes 22020096 | tf_op jit(solution)/shard_map/pallas_call | solution.py:295
  76.6 4.6 %shard_map.128 = (bf16[96,2048]{1,0:T(8,128)(2,1)S(1)}, bf16[96,2048]{1,0:T(8,128)(2,1)S(1)}) custom-call(bf16[96,2048]{1,0:T(8,128)(2,1)S(1)} %pad_maximum_fusion.2.refs_0_, bf16[96,2048]{1,0:T(8,128)(2,1)S(1)} %collective-permute-done.25.refs_1_, bf16[2048,1792]{1,0:T(8,128)(2,1)S(1)} %get-tuple-element.45.refs_2_, ...), custom_call_target="tpu_custom_call" | custom-call | flops 4227858432 | bytes 22020096 | tf_op jit(solution)/shard_map/pallas_call | solution.py:295
  81.3 0.6 collective-permute-start.26
  81.8 4.4 %shard_map.126 = (bf16[96,2048]{1,0:T(8,128)(2,1)S(1)}, bf16[96,2048]{1,0:T(8,128)(2,1)S(1)}) custom-call(bf16[96,2048]{1,0:T(8,128)(2,1)S(1)} %pad_maximum_fusion.1.refs_0_, bf16[96,2048]{1,0:T(8,128)(2,1)S(1)} %collective-permute-done.15.refs_1_, bf16[2048,1792]{1,0:T(8,128)(2,1)S(1)} %get-tuple-element.45.refs_2_, ...), custom_call_target="tpu_custom_call" | custom-call | flops 4227858432 | bytes 22020096 | tf_op jit(solution)/shard_map/pallas_call | solution.py:295
  86.4 0.1 add_convert_fusion.3
  86.5 2.1 %collective-permute-start.10 = (bf16[24,2048]{1,0:T(8,128)(2,1)S(1)}, bf16[24,2048]{1,0:T(8,128)(2,1)S(1)}, u32[]{:S(2)}, u32[]{:S(2)}) collective-permute-start(bf16[24,2048]{1,0:T(8,128)(2,1)S(1)} %get-tuple-element.83), channel_id=1, source_target_pairs={{0,6},{2,4},{4,2},{6,0},{8,14},{10,12},{12,10},{14,8},{16,22},{18,... | collective-permute-start | bytes 294920 | tf_op jit(solution)/shard_map/ppermute | solution.py:411
  88.6 0.4 collective-permute-start.8
  89.0 1.1 collective-permute-start.9
  90.3 0.1 add_convert_fusion.2
  90.4 2.9 %collective-permute-start.17 = (bf16[96,2048]{1,0:T(8,128)(2,1)S(1)}, bf16[96,2048]{1,0:T(8,128)(2,1)S(1)}, u32[]{:S(2)}, u32[]{:S(2)}) collective-permute-start(bf16[96,2048]{1,0:T(8,128)(2,1)S(1)} %add_convert_fusion.2), channel_id=1, source_target_pairs={{0,24},{2,26},{4,28},{6,30},{8,16},{10,18},{12,20},{14,22},{16,8},... | collective-permute-start | bytes 1179656 | tf_op jit(solution)/shard_map/ppermute | solution.py:411
  93.5 7.5 %collective-permute-done.27 = bf16[96,2048]{1,0:T(8,128)(2,1)S(1)} collective-permute-done((bf16[96,2048]{1,0:T(8,128)(2,1)S(1)}, bf16[96,2048]{1,0:T(8,128)(2,1)S(1)}, u32[]{:S(2)}, u32[]{:S(2)}) %collective-permute-start.27) | collective-permute-done | bytes 393248 | tf_op jit(solution)/shard_map/ppermute | solution.py:411
  101.0 2.6 %collective-permute-start.28 = (bf16[24,2048]{1,0:T(8,128)(2,1)S(1)}, bf16[24,2048]{1,0:T(8,128)(2,1)S(1)}, u32[]{:S(2)}, u32[]{:S(2)}) collective-permute-start(bf16[24,2048]{1,0:T(8,128)(2,1)S(1)} %get-tuple-element.69), channel_id=1, source_target_pairs={{0,2},{2,0},{4,6},{6,4},{8,10},{10,8},{12,14},{14,12},{16,18},{18,... | collective-permute-start | bytes 294920 | tf_op jit(solution)/shard_map/ppermute | solution.py:411
  103.6 7.0 %collective-permute-done.17 = bf16[96,2048]{1,0:T(8,128)(2,1)S(1)} collective-permute-done((bf16[96,2048]{1,0:T(8,128)(2,1)S(1)}, bf16[96,2048]{1,0:T(8,128)(2,1)S(1)}, u32[]{:S(2)}, u32[]{:S(2)}) %collective-permute-start.17) | collective-permute-done | bytes 393248 | tf_op jit(solution)/shard_map/ppermute | solution.py:411
  110.6 0.3 collective-permute-start.29
  111.0 1.5 %collective-permute-start.30 = (bf16[24,2048]{1,0:T(8,128)(2,1)S(1)}, bf16[24,2048]{1,0:T(8,128)(2,1)S(1)}, u32[]{:S(2)}, u32[]{:S(2)}) collective-permute-start(bf16[24,2048]{1,0:T(8,128)(2,1)S(1)} %get-tuple-element.67), channel_id=1, source_target_pairs={{0,6},{2,4},{4,2},{6,0},{8,14},{10,12},{12,10},{14,8},{16,22},{18,... | collective-permute-start | bytes 294920 | tf_op jit(solution)/shard_map/ppermute | solution.py:411
  112.5 1.7 %collective-permute-start.18 = (bf16[24,2048]{1,0:T(8,128)(2,1)S(1)}, bf16[24,2048]{1,0:T(8,128)(2,1)S(1)}, u32[]{:S(2)}, u32[]{:S(2)}) collective-permute-start(bf16[24,2048]{1,0:T(8,128)(2,1)S(1)} %get-tuple-element.77), channel_id=1, source_target_pairs={{0,2},{2,0},{4,6},{6,4},{8,10},{10,8},{12,14},{14,12},{16,18},{18,... | collective-permute-start | bytes 294920 | tf_op jit(solution)/shard_map/ppermute | solution.py:411
  114.2 0.3 collective-permute-start.19
  114.5 1.4 %collective-permute-start.20 = (bf16[24,2048]{1,0:T(8,128)(2,1)S(1)}, bf16[24,2048]{1,0:T(8,128)(2,1)S(1)}, u32[]{:S(2)}, u32[]{:S(2)}) collective-permute-start(bf16[24,2048]{1,0:T(8,128)(2,1)S(1)} %get-tuple-element.75), channel_id=1, source_target_pairs={{0,6},{2,4},{4,2},{6,0},{8,14},{10,12},{12,10},{14,8},{16,22},{18,... | collective-permute-start | bytes 294920 | tf_op jit(solution)/shard_map/ppermute | solution.py:411
  116.0 1.7 %collective-permute-done.29.refs_5_ = bf16[24,2048]{1,0:T(8,128)(2,1)S(1)} collective-permute-done((bf16[24,2048]{1,0:T(8,128)(2,1)S(1)}, bf16[24,2048]{1,0:T(8,128)(2,1)S(1)}, u32[]{:S(2)}, u32[]{:S(2)}) %collective-permute-start.29) | collective-permute-done | bytes 98336 | tf_op jit(solution)/shard_map/ppermute | solution.py:411
  117.7 2.5 %collective-permute-start.37 = (bf16[24,2048]{1,0:T(8,128)(2,1)S(1)}, bf16[24,2048]{1,0:T(8,128)(2,1)S(1)}, u32[]{:S(2)}, u32[]{:S(2)}) collective-permute-start(bf16[24,2048]{1,0:T(8,128)(2,1)S(1)} %get-tuple-element.62), channel_id=1, source_target_pairs={{0,16},{2,18},{4,20},{6,22},{8,24},{10,26},{12,28},{14,30},{16,0},... | collective-permute-start | bytes 294920 | tf_op jit(solution)/shard_map/ppermute | solution.py:411
  120.2 1.5 %collective-permute-start.38 = (bf16[24,2048]{1,0:T(8,128)(2,1)S(1)}, bf16[24,2048]{1,0:T(8,128)(2,1)S(1)}, u32[]{:S(2)}, u32[]{:S(2)}) collective-permute-start(bf16[24,2048]{1,0:T(8,128)(2,1)S(1)} %get-tuple-element.61), channel_id=1, source_target_pairs={{0,18},{2,16},{4,22},{6,20},{8,26},{10,24},{12,30},{14,28},{16,2},... | collective-permute-start | bytes 294920 | tf_op jit(solution)/shard_map/ppermute | solution.py:411
  121.7 1.0 collective-permute-start.39
  122.7 3.0 %collective-permute-start.40 = (bf16[24,2048]{1,0:T(8,128)(2,1)S(1)}, bf16[24,2048]{1,0:T(8,128)(2,1)S(1)}, u32[]{:S(2)}, u32[]{:S(2)}) collective-permute-start(bf16[24,2048]{1,0:T(8,128)(2,1)S(1)} %get-tuple-element.59), channel_id=1, source_target_pairs={{0,22},{2,20},{4,18},{6,16},{8,30},{10,28},{12,26},{14,24},{16,6},... | collective-permute-start | bytes 294920 | tf_op jit(solution)/shard_map/ppermute | solution.py:411
  125.7 0.5 shard_map.125.refs_0_
  126.2 0.5 shard_map.127.refs_0_
  126.7 0.5 shard_map.129.refs_0_
  127.2 1.7 %collective-permute-done.37.refs_3_ = bf16[24,2048]{1,0:T(8,128)(2,1)S(1)} collective-permute-done((bf16[24,2048]{1,0:T(8,128)(2,1)S(1)}, bf16[24,2048]{1,0:T(8,128)(2,1)S(1)}, u32[]{:S(2)}, u32[]{:S(2)}) %collective-permute-start.37) | collective-permute-done | bytes 98336 | tf_op jit(solution)/shard_map/ppermute | solution.py:411
  129.0 3.7 %collective-permute-done.38.refs_4_ = bf16[24,2048]{1,0:T(8,128)(2,1)S(1)} collective-permute-done((bf16[24,2048]{1,0:T(8,128)(2,1)S(1)}, bf16[24,2048]{1,0:T(8,128)(2,1)S(1)}, u32[]{:S(2)}, u32[]{:S(2)}) %collective-permute-start.38) | collective-permute-done | bytes 98336 | tf_op jit(solution)/shard_map/ppermute | solution.py:411
  132.6 2.4 %collective-permute-done.39.refs_5_ = bf16[24,2048]{1,0:T(8,128)(2,1)S(1)} collective-permute-done((bf16[24,2048]{1,0:T(8,128)(2,1)S(1)}, bf16[24,2048]{1,0:T(8,128)(2,1)S(1)}, u32[]{:S(2)}, u32[]{:S(2)}) %collective-permute-start.39) | collective-permute-done | bytes 98336 | tf_op jit(solution)/shard_map/ppermute | solution.py:411
  135.0 0.5 collective-permute-done.40.refs_6_
  135.4 1.3 shard_map.131
  (50 shorter events, 1.0 us)
Async XLA Ops:
  0.0 13.3 %collective-permute-start.2 = (bf16[512,2048]{1,0:T(8,128)(2,1)}, bf16[512,2048]{1,0:T(8,128)(2,1)S(1)}, u32[]{:S(2)}, u32[]{:S(2)}) collective-permute-start(bf16[512,2048]{1,0:T(8,128)(2,1)} %refs_4_.2), channel_id=1, source_target_pairs={{0,1},{1,0},{2,3},{3,2},{4,5},{5,4},{6,7},{7,6},{8,9},{9,8},{10,11... | collective-permute-start | bytes 6291464 | tf_op jit(solution)/shard_map/ppermute | solution.py:25
  1.7 8.3 %collective-permute-start = (bf16[128,128]{1,0:T(8,128)(2,1)S(1)}, bf16[128,128]{1,0:T(8,128)(2,1)S(1)}, u32[]{:S(2)}, u32[]{:S(2)}) collective-permute-start(bf16[128,128]{1,0:T(8,128)(2,1)S(1)} %get-tuple-element.33), channel_id=1, source_target_pairs={{0,2},{2,4},{4,6},{6,8},{8,10},{10,12},{12,14},{14,16},{16,18},{18... | collective-permute-start | bytes 98312 | tf_op jit(solution)/shard_map/ppermute | solution.py:21
  11.9 1.4 %collective-permute-start.1 = (bf16[128,512]{1,0:T(8,128)(2,1)S(1)}, bf16[128,512]{1,0:T(8,128)(2,1)S(1)}, u32[]{:S(2)}, u32[]{:S(2)}) collective-permute-start(bf16[128,512]{1,0:T(8,128)(2,1)S(1)} %get-tuple-element.40), channel_id=1, source_target_pairs={{0,1},{1,0},{2,3},{3,2},{4,5},{5,4},{6,7},{7,6},{8,9},{9,8},{10,11... | collective-permute-start | bytes 393224 | tf_op jit(solution)/shard_map/ppermute | solution.py:25
  14.4 22.4 %collective-permute-start.31 = (bf16[96,2048]{1,0:T(8,128)(2,1)S(1)}, bf16[96,2048]{1,0:T(8,128)(2,1)S(1)}, u32[]{:S(2)}, u32[]{:S(2)}) collective-permute-start(bf16[96,2048]{1,0:T(8,128)(2,1)S(1)} %get-tuple-element.56), channel_id=1, source_target_pairs={{0,16},{2,18},{4,20},{6,22},{8,24},{10,26},{12,28},{14,30},{16,0},... | collective-permute-start | bytes 1179656 | tf_op jit(solution)/shard_map/ppermute | solution.py:411
  17.3 10.4 %collective-permute-start.3 = (bf16[24,2048]{1,0:T(8,128)(2,1)S(1)}, bf16[24,2048]{1,0:T(8,128)(2,1)S(1)}, u32[]{:S(2)}, u32[]{:S(2)}) collective-permute-start(bf16[24,2048]{1,0:T(8,128)(2,1)S(1)} %get-tuple-element.90), channel_id=1, source_target_pairs={{0,2},{2,0},{4,6},{6,4},{8,10},{10,8},{12,14},{14,12},{16,18},{18,... | collective-permute-start | bytes 294920 | tf_op jit(solution)/shard_map/ppermute | solution.py:411
  18.7 9.1 %collective-permute-start.4 = (bf16[24,2048]{1,0:T(8,128)(2,1)S(1)}, bf16[24,2048]{1,0:T(8,128)(2,1)S(1)}, u32[]{:S(2)}, u32[]{:S(2)}) collective-permute-start(bf16[24,2048]{1,0:T(8,128)(2,1)S(1)} %get-tuple-element.89), channel_id=1, source_target_pairs={{0,4},{2,6},{4,0},{6,2},{8,12},{10,14},{12,8},{14,10},{16,20},{18,... | collective-permute-start | bytes 294920 | tf_op jit(solution)/shard_map/ppermute | solution.py:411
  20.2 7.6 %collective-permute-start.5 = (bf16[24,2048]{1,0:T(8,128)(2,1)S(1)}, bf16[24,2048]{1,0:T(8,128)(2,1)S(1)}, u32[]{:S(2)}, u32[]{:S(2)}) collective-permute-start(bf16[24,2048]{1,0:T(8,128)(2,1)S(1)} %get-tuple-element.88), channel_id=1, source_target_pairs={{0,6},{2,4},{4,2},{6,0},{8,14},{10,12},{12,10},{14,8},{16,22},{18,... | collective-permute-start | bytes 294920 | tf_op jit(solution)/shard_map/ppermute | solution.py:411
  26.1 25.7 %collective-permute-start.21 = (bf16[96,2048]{1,0:T(8,128)(2,1)S(1)}, bf16[96,2048]{1,0:T(8,128)(2,1)S(1)}, u32[]{:S(2)}, u32[]{:S(2)}) collective-permute-start(bf16[96,2048]{1,0:T(8,128)(2,1)S(1)} %get-tuple-element.53), channel_id=1, source_target_pairs={{0,8},{2,10},{4,12},{6,14},{8,0},{10,2},{12,4},{14,6},{16,24},{18,... | collective-permute-start | bytes 1179656 | tf_op jit(solution)/shard_map/ppermute | solution.py:411
  27.8 26.5 %collective-permute-start.11 = (bf16[96,2048]{1,0:T(8,128)(2,1)S(1)}, bf16[96,2048]{1,0:T(8,128)(2,1)S(1)}, u32[]{:S(2)}, u32[]{:S(2)}) collective-permute-start(bf16[96,2048]{1,0:T(8,128)(2,1)S(1)} %get-tuple-element.50), channel_id=1, source_target_pairs={{0,24},{2,26},{4,28},{6,30},{8,16},{10,18},{12,20},{14,22},{16,8},... | collective-permute-start | bytes 1179656 | tf_op jit(solution)/shard_map/ppermute | solution.py:411
  27.8 39.3 %collective-permute-start.6 = (bf16[96,2048]{1,0:T(8,128)(2,1)S(1)}, bf16[96,2048]{1,0:T(8,128)(2,1)S(1)}, u32[]{:S(2)}, u32[]{:S(2)}) collective-permute-start(bf16[96,2048]{1,0:T(8,128)(2,1)S(1)} %pad_maximum_fusion.refs_0_), channel_id=1, source_target_pairs={{0,1},{1,0},{2,3},{3,2},{4,5},{5,4},{6,7},{7,6},{8,9},{9,8},{10,11... | collective-permute-start | bytes 1179656 | tf_op jit(solution)/shard_map/ppermute | solution.py:25
  36.9 18.0 %collective-permute-start.32 = (bf16[24,2048]{1,0:T(8,128)(2,1)S(1)}, bf16[24,2048]{1,0:T(8,128)(2,1)S(1)}, u32[]{:S(2)}, u32[]{:S(2)}) collective-permute-start(bf16[24,2048]{1,0:T(8,128)(2,1)S(1)} %get-tuple-element.66), channel_id=1, source_target_pairs={{0,2},{2,0},{4,6},{6,4},{8,10},{10,8},{12,14},{14,12},{16,18},{18,... | collective-permute-start | bytes 294920 | tf_op jit(solution)/shard_map/ppermute | solution.py:411
  38.7 16.8 %collective-permute-start.33 = (bf16[24,2048]{1,0:T(8,128)(2,1)S(1)}, bf16[24,2048]{1,0:T(8,128)(2,1)S(1)}, u32[]{:S(2)}, u32[]{:S(2)}) collective-permute-start(bf16[24,2048]{1,0:T(8,128)(2,1)S(1)} %get-tuple-element.65), channel_id=1, source_target_pairs={{0,4},{2,6},{4,0},{6,2},{8,12},{10,14},{12,8},{14,10},{16,20},{18,... | collective-permute-start | bytes 294920 | tf_op jit(solution)/shard_map/ppermute | solution.py:411
  51.8 6.5 %collective-permute-start.34 = (bf16[24,2048]{1,0:T(8,128)(2,1)S(1)}, bf16[24,2048]{1,0:T(8,128)(2,1)S(1)}, u32[]{:S(2)}, u32[]{:S(2)}) collective-permute-start(bf16[24,2048]{1,0:T(8,128)(2,1)S(1)} %get-tuple-element.64), channel_id=1, source_target_pairs={{0,6},{2,4},{4,2},{6,0},{8,14},{10,12},{12,10},{14,8},{16,22},{18,... | collective-permute-start | bytes 294920 | tf_op jit(solution)/shard_map/ppermute | solution.py:411
  54.2 6.1 %collective-permute-start.22 = (bf16[24,2048]{1,0:T(8,128)(2,1)S(1)}, bf16[24,2048]{1,0:T(8,128)(2,1)S(1)}, u32[]{:S(2)}, u32[]{:S(2)}) collective-permute-start(bf16[24,2048]{1,0:T(8,128)(2,1)S(1)} %get-tuple-element.74), channel_id=1, source_target_pairs={{0,2},{2,0},{4,6},{6,4},{8,10},{10,8},{12,14},{14,12},{16,18},{18,... | collective-permute-start | bytes 294920 | tf_op jit(solution)/shard_map/ppermute | solution.py:411
  54.9 6.6 %collective-permute-start.23 = (bf16[24,2048]{1,0:T(8,128)(2,1)S(1)}, bf16[24,2048]{1,0:T(8,128)(2,1)S(1)}, u32[]{:S(2)}, u32[]{:S(2)}) collective-permute-start(bf16[24,2048]{1,0:T(8,128)(2,1)S(1)} %get-tuple-element.73), channel_id=1, source_target_pairs={{0,4},{2,6},{4,0},{6,2},{8,12},{10,14},{12,8},{14,10},{16,20},{18,... | collective-permute-start | bytes 294920 | tf_op jit(solution)/shard_map/ppermute | solution.py:411
  55.5 7.9 %collective-permute-start.24 = (bf16[24,2048]{1,0:T(8,128)(2,1)S(1)}, bf16[24,2048]{1,0:T(8,128)(2,1)S(1)}, u32[]{:S(2)}, u32[]{:S(2)}) collective-permute-start(bf16[24,2048]{1,0:T(8,128)(2,1)S(1)} %get-tuple-element.72), channel_id=1, source_target_pairs={{0,6},{2,4},{4,2},{6,0},{8,14},{10,12},{12,10},{14,8},{16,22},{18,... | collective-permute-start | bytes 294920 | tf_op jit(solution)/shard_map/ppermute | solution.py:411
  58.3 6.2 %collective-permute-start.12 = (bf16[24,2048]{1,0:T(8,128)(2,1)S(1)}, bf16[24,2048]{1,0:T(8,128)(2,1)S(1)}, u32[]{:S(2)}, u32[]{:S(2)}) collective-permute-start(bf16[24,2048]{1,0:T(8,128)(2,1)S(1)} %get-tuple-element.82), channel_id=1, source_target_pairs={{0,2},{2,0},{4,6},{6,4},{8,10},{10,8},{12,14},{14,12},{16,18},{18,... | collective-permute-start | bytes 294920 | tf_op jit(solution)/shard_map/ppermute | solution.py:411
  60.3 5.0 %collective-permute-start.13 = (bf16[24,2048]{1,0:T(8,128)(2,1)S(1)}, bf16[24,2048]{1,0:T(8,128)(2,1)S(1)}, u32[]{:S(2)}, u32[]{:S(2)}) collective-permute-start(bf16[24,2048]{1,0:T(8,128)(2,1)S(1)} %get-tuple-element.81), channel_id=1, source_target_pairs={{0,4},{2,6},{4,0},{6,2},{8,12},{10,14},{12,8},{14,10},{16,20},{18,... | collective-permute-start | bytes 294920 | tf_op jit(solution)/shard_map/ppermute | solution.py:411
  61.4 5.5 %collective-permute-start.14 = (bf16[24,2048]{1,0:T(8,128)(2,1)S(1)}, bf16[24,2048]{1,0:T(8,128)(2,1)S(1)}, u32[]{:S(2)}, u32[]{:S(2)}) collective-permute-start(bf16[24,2048]{1,0:T(8,128)(2,1)S(1)} %get-tuple-element.80), channel_id=1, source_target_pairs={{0,6},{2,4},{4,2},{6,0},{8,14},{10,12},{12,10},{14,8},{16,22},{18,... | collective-permute-start | bytes 294920 | tf_op jit(solution)/shard_map/ppermute | solution.py:411
  63.4 8.6 %collective-permute-start.35 = (bf16[96,2048]{1,0:T(8,128)(2,1)S(1)}, bf16[96,2048]{1,0:T(8,128)(2,1)S(1)}, u32[]{:S(2)}, u32[]{:S(2)}) collective-permute-start(bf16[96,2048]{1,0:T(8,128)(2,1)S(1)} %pad_maximum_fusion.3.refs_0_), channel_id=1, source_target_pairs={{0,1},{1,0},{2,3},{3,2},{4,5},{5,4},{6,7},{7,6},{8,9},{9,8},{10,11... | collective-permute-start | bytes 1179656 | tf_op jit(solution)/shard_map/ppermute | solution.py:25
  64.5 12.1 %collective-permute-start.25 = (bf16[96,2048]{1,0:T(8,128)(2,1)S(1)}, bf16[96,2048]{1,0:T(8,128)(2,1)S(1)}, u32[]{:S(2)}, u32[]{:S(2)}) collective-permute-start(bf16[96,2048]{1,0:T(8,128)(2,1)S(1)} %pad_maximum_fusion.2.refs_0_), channel_id=1, source_target_pairs={{0,1},{1,0},{2,3},{3,2},{4,5},{5,4},{6,7},{7,6},{8,9},{9,8},{10,11... | collective-permute-start | bytes 1179656 | tf_op jit(solution)/shard_map/ppermute | solution.py:25
  67.0 14.8 %collective-permute-start.15 = (bf16[96,2048]{1,0:T(8,128)(2,1)S(1)}, bf16[96,2048]{1,0:T(8,128)(2,1)S(1)}, u32[]{:S(2)}, u32[]{:S(2)}) collective-permute-start(bf16[96,2048]{1,0:T(8,128)(2,1)S(1)} %pad_maximum_fusion.1.refs_0_), channel_id=1, source_target_pairs={{0,1},{1,0},{2,3},{3,2},{4,5},{5,4},{6,7},{7,6},{8,9},{9,8},{10,11... | collective-permute-start | bytes 1179656 | tf_op jit(solution)/shard_map/ppermute | solution.py:25
  71.5 14.9 %collective-permute-start.7 = (bf16[96,2048]{1,0:T(8,128)(2,1)S(1)}, bf16[96,2048]{1,0:T(8,128)(2,1)S(1)}, u32[]{:S(2)}, u32[]{:S(2)}) collective-permute-start(bf16[96,2048]{1,0:T(8,128)(2,1)S(1)} %get-tuple-element.49), channel_id=1, source_target_pairs={{0,1},{1,0},{2,3},{3,2},{4,5},{5,4},{6,7},{7,6},{8,9},{9,8},{10,11... | collective-permute-start | bytes 1179656 | tf_op jit(solution)/shard_map/ppermute | solution.py:25
  76.5 13.9 %collective-permute-start.36 = (bf16[96,2048]{1,0:T(8,128)(2,1)S(1)}, bf16[96,2048]{1,0:T(8,128)(2,1)S(1)}, u32[]{:S(2)}, u32[]{:S(2)}) collective-permute-start(bf16[96,2048]{1,0:T(8,128)(2,1)S(1)} %get-tuple-element.58), channel_id=1, source_target_pairs={{0,1},{1,0},{2,3},{3,2},{4,5},{5,4},{6,7},{7,6},{8,9},{9,8},{10,11... | collective-permute-start | bytes 1179656 | tf_op jit(solution)/shard_map/ppermute | solution.py:25
  81.3 7.7 %collective-permute-start.26 = (bf16[96,2048]{1,0:T(8,128)(2,1)S(1)}, bf16[96,2048]{1,0:T(8,128)(2,1)S(1)}, u32[]{:S(2)}, u32[]{:S(2)}) collective-permute-start(bf16[96,2048]{1,0:T(8,128)(2,1)S(1)} %get-tuple-element.55), channel_id=1, source_target_pairs={{0,1},{1,0},{2,3},{3,2},{4,5},{5,4},{6,7},{7,6},{8,9},{9,8},{10,11... | collective-permute-start | bytes 1179656 | tf_op jit(solution)/shard_map/ppermute | solution.py:25
  86.3 39.4 %copy-start = (f32[128,2]{0,1:T(2,128)S(1)}, f32[128,2]{0,1:T(2,128)}, u32[]{:S(2)}) copy-start(f32[128,2]{0,1:T(2,128)} %param.20) | copy-start | bytes 3076
  86.3 3.9 %collective-permute-start.16 = (bf16[96,2048]{1,0:T(8,128)(2,1)S(1)}, bf16[96,2048]{1,0:T(8,128)(2,1)S(1)}, u32[]{:S(2)}, u32[]{:S(2)}) collective-permute-start(bf16[96,2048]{1,0:T(8,128)(2,1)S(1)} %get-tuple-element.52), channel_id=1, source_target_pairs={{0,1},{1,0},{2,3},{3,2},{4,5},{5,4},{6,7},{7,6},{8,9},{9,8},{10,11... | collective-permute-start | bytes 1179656 | tf_op jit(solution)/shard_map/ppermute | solution.py:25
  86.5 24.4 %collective-permute-start.10 = (bf16[24,2048]{1,0:T(8,128)(2,1)S(1)}, bf16[24,2048]{1,0:T(8,128)(2,1)S(1)}, u32[]{:S(2)}, u32[]{:S(2)}) collective-permute-start(bf16[24,2048]{1,0:T(8,128)(2,1)S(1)} %get-tuple-element.83), channel_id=1, source_target_pairs={{0,6},{2,4},{4,2},{6,0},{8,14},{10,12},{12,10},{14,8},{16,22},{18,... | collective-permute-start | bytes 294920 | tf_op jit(solution)/shard_map/ppermute | solution.py:411
  88.6 23.9 %collective-permute-start.8 = (bf16[24,2048]{1,0:T(8,128)(2,1)S(1)}, bf16[24,2048]{1,0:T(8,128)(2,1)S(1)}, u32[]{:S(2)}, u32[]{:S(2)}) collective-permute-start(bf16[24,2048]{1,0:T(8,128)(2,1)S(1)} %get-tuple-element.85), channel_id=1, source_target_pairs={{0,2},{2,0},{4,6},{6,4},{8,10},{10,8},{12,14},{14,12},{16,18},{18,... | collective-permute-start | bytes 294920 | tf_op jit(solution)/shard_map/ppermute | solution.py:411
  89.0 25.3 %collective-permute-start.9 = (bf16[24,2048]{1,0:T(8,128)(2,1)S(1)}, bf16[24,2048]{1,0:T(8,128)(2,1)S(1)}, u32[]{:S(2)}, u32[]{:S(2)}) collective-permute-start(bf16[24,2048]{1,0:T(8,128)(2,1)S(1)} %get-tuple-element.84), channel_id=1, source_target_pairs={{0,4},{2,6},{4,0},{6,2},{8,12},{10,14},{12,8},{14,10},{16,20},{18,... | collective-permute-start | bytes 294920 | tf_op jit(solution)/shard_map/ppermute | solution.py:411
  90.2 10.7 %collective-permute-start.27 = (bf16[96,2048]{1,0:T(8,128)(2,1)S(1)}, bf16[96,2048]{1,0:T(8,128)(2,1)S(1)}, u32[]{:S(2)}, u32[]{:S(2)}) collective-permute-start(bf16[96,2048]{1,0:T(8,128)(2,1)S(1)} %add_convert_fusion.1), channel_id=1, source_target_pairs={{0,8},{2,10},{4,12},{6,14},{8,0},{10,2},{12,4},{14,6},{16,24},{18,... | collective-permute-start | bytes 1179656 | tf_op jit(solution)/shard_map/ppermute | solution.py:411
  90.4 20.2 %collective-permute-start.17 = (bf16[96,2048]{1,0:T(8,128)(2,1)S(1)}, bf16[96,2048]{1,0:T(8,128)(2,1)S(1)}, u32[]{:S(2)}, u32[]{:S(2)}) collective-permute-start(bf16[96,2048]{1,0:T(8,128)(2,1)S(1)} %add_convert_fusion.2), channel_id=1, source_target_pairs={{0,24},{2,26},{4,28},{6,30},{8,16},{10,18},{12,20},{14,22},{16,8},... | collective-permute-start | bytes 1179656 | tf_op jit(solution)/shard_map/ppermute | solution.py:411
  101.0 13.6 %collective-permute-start.28 = (bf16[24,2048]{1,0:T(8,128)(2,1)S(1)}, bf16[24,2048]{1,0:T(8,128)(2,1)S(1)}, u32[]{:S(2)}, u32[]{:S(2)}) collective-permute-start(bf16[24,2048]{1,0:T(8,128)(2,1)S(1)} %get-tuple-element.69), channel_id=1, source_target_pairs={{0,2},{2,0},{4,6},{6,4},{8,10},{10,8},{12,14},{14,12},{16,18},{18,... | collective-permute-start | bytes 294920 | tf_op jit(solution)/shard_map/ppermute | solution.py:411
  110.6 7.0 %collective-permute-start.29 = (bf16[24,2048]{1,0:T(8,128)(2,1)S(1)}, bf16[24,2048]{1,0:T(8,128)(2,1)S(1)}, u32[]{:S(2)}, u32[]{:S(2)}) collective-permute-start(bf16[24,2048]{1,0:T(8,128)(2,1)S(1)} %get-tuple-element.68), channel_id=1, source_target_pairs={{0,4},{2,6},{4,0},{6,2},{8,12},{10,14},{12,8},{14,10},{16,20},{18,... | collective-permute-start | bytes 294920 | tf_op jit(solution)/shard_map/ppermute | solution.py:411
  111.0 15.7 %collective-permute-start.30 = (bf16[24,2048]{1,0:T(8,128)(2,1)S(1)}, bf16[24,2048]{1,0:T(8,128)(2,1)S(1)}, u32[]{:S(2)}, u32[]{:S(2)}) collective-permute-start(bf16[24,2048]{1,0:T(8,128)(2,1)S(1)} %get-tuple-element.67), channel_id=1, source_target_pairs={{0,6},{2,4},{4,2},{6,0},{8,14},{10,12},{12,10},{14,8},{16,22},{18,... | collective-permute-start | bytes 294920 | tf_op jit(solution)/shard_map/ppermute | solution.py:411
  112.5 7.7 %collective-permute-start.18 = (bf16[24,2048]{1,0:T(8,128)(2,1)S(1)}, bf16[24,2048]{1,0:T(8,128)(2,1)S(1)}, u32[]{:S(2)}, u32[]{:S(2)}) collective-permute-start(bf16[24,2048]{1,0:T(8,128)(2,1)S(1)} %get-tuple-element.77), channel_id=1, source_target_pairs={{0,2},{2,0},{4,6},{6,4},{8,10},{10,8},{12,14},{14,12},{16,18},{18,... | collective-permute-start | bytes 294920 | tf_op jit(solution)/shard_map/ppermute | solution.py:411
  114.2 7.5 %collective-permute-start.19 = (bf16[24,2048]{1,0:T(8,128)(2,1)S(1)}, bf16[24,2048]{1,0:T(8,128)(2,1)S(1)}, u32[]{:S(2)}, u32[]{:S(2)}) collective-permute-start(bf16[24,2048]{1,0:T(8,128)(2,1)S(1)} %get-tuple-element.76), channel_id=1, source_target_pairs={{0,4},{2,6},{4,0},{6,2},{8,12},{10,14},{12,8},{14,10},{16,20},{18,... | collective-permute-start | bytes 294920 | tf_op jit(solution)/shard_map/ppermute | solution.py:411
  114.5 8.2 %collective-permute-start.20 = (bf16[24,2048]{1,0:T(8,128)(2,1)S(1)}, bf16[24,2048]{1,0:T(8,128)(2,1)S(1)}, u32[]{:S(2)}, u32[]{:S(2)}) collective-permute-start(bf16[24,2048]{1,0:T(8,128)(2,1)S(1)} %get-tuple-element.75), channel_id=1, source_target_pairs={{0,6},{2,4},{4,2},{6,0},{8,14},{10,12},{12,10},{14,8},{16,22},{18,... | collective-permute-start | bytes 294920 | tf_op jit(solution)/shard_map/ppermute | solution.py:411
  117.7 11.3 %collective-permute-start.37 = (bf16[24,2048]{1,0:T(8,128)(2,1)S(1)}, bf16[24,2048]{1,0:T(8,128)(2,1)S(1)}, u32[]{:S(2)}, u32[]{:S(2)}) collective-permute-start(bf16[24,2048]{1,0:T(8,128)(2,1)S(1)} %get-tuple-element.62), channel_id=1, source_target_pairs={{0,16},{2,18},{4,20},{6,22},{8,24},{10,26},{12,28},{14,30},{16,0},... | collective-permute-start | bytes 294920 | tf_op jit(solution)/shard_map/ppermute | solution.py:411
  120.2 12.4 %collective-permute-start.38 = (bf16[24,2048]{1,0:T(8,128)(2,1)S(1)}, bf16[24,2048]{1,0:T(8,128)(2,1)S(1)}, u32[]{:S(2)}, u32[]{:S(2)}) collective-permute-start(bf16[24,2048]{1,0:T(8,128)(2,1)S(1)} %get-tuple-element.61), channel_id=1, source_target_pairs={{0,18},{2,16},{4,22},{6,20},{8,26},{10,24},{12,30},{14,28},{16,2},... | collective-permute-start | bytes 294920 | tf_op jit(solution)/shard_map/ppermute | solution.py:411
  121.7 13.2 %collective-permute-start.39 = (bf16[24,2048]{1,0:T(8,128)(2,1)S(1)}, bf16[24,2048]{1,0:T(8,128)(2,1)S(1)}, u32[]{:S(2)}, u32[]{:S(2)}) collective-permute-start(bf16[24,2048]{1,0:T(8,128)(2,1)S(1)} %get-tuple-element.60), channel_id=1, source_target_pairs={{0,20},{2,22},{4,16},{6,18},{8,28},{10,30},{12,24},{14,26},{16,4},... | collective-permute-start | bytes 294920 | tf_op jit(solution)/shard_map/ppermute | solution.py:411
  122.7 12.7 %collective-permute-start.40 = (bf16[24,2048]{1,0:T(8,128)(2,1)S(1)}, bf16[24,2048]{1,0:T(8,128)(2,1)S(1)}, u32[]{:S(2)}, u32[]{:S(2)}) collective-permute-start(bf16[24,2048]{1,0:T(8,128)(2,1)S(1)} %get-tuple-element.59), channel_id=1, source_target_pairs={{0,22},{2,20},{4,18},{6,16},{8,30},{10,28},{12,26},{14,24},{16,6},... | collective-permute-start | bytes 294920 | tf_op jit(solution)/shard_map/ppermute | solution.py:411
